TPU v7x, 256 devices: a 4x2x16 block of a 4x16x16 slice. The times are simulated.
256 devices in a mesh: grp: 2 (over y), ep: 32 (over z, core), tp: 4 (over x).
Axes of the slice: x: 4, y: 2, z: 16, core: 2. Of those that a mesh axis runs over, the one named last changes fastest.
The devices are a block of a 4x16x16 slice.
Arguments:
- queries: bfloat16 [32768, 512], P(('grp', 'ep'), 'tp'), parts along dimension 0, may hold values from -6 to 6
- keys: bfloat16 [32768, 512], P(('grp', 'ep'), 'tp'), parts along dimension 0, may hold values from -6 to 6
- values: bfloat16 [32768, 1024], P(('grp', 'ep'), 'tp'), parts along dimension 0, may hold values from -6 to 6
- gate: bfloat16 [32768, 1024], P(('grp', 'ep'), 'tp'), parts along dimension 0, may hold values from -6 to 6
- log_decay: float32 [32768, 8], P(('grp', 'ep'), 'tp'), parts along dimension 0, may hold values from -1 to 0, as said below
- w_out: bfloat16 [1024, 2048], P('tp'), may hold values from -0.1875 to 0.1875
- moe_input: bfloat16 [32768, 2048], P(('grp', 'ep', 'tp')), parts along dimension 0, may hold values from -40 to 40
- moe_gain: float32 [2048], replicated, may hold values from 0.1 to 1.9
- routes: int32 [32768, 2], P(('grp', 'ep', 'tp')), parts along dimension 0, may hold values from 0 to 127, all different within a row; in each aligned block of 128 rows (0 to 127, 128 to 255, ...) at most 3 rows name the same one
- route_weight: float32 [32768, 2], P(('grp', 'ep', 'tp')), parts along dimension 0, may hold values from 0.1 to 1
- expert_gate: bfloat16 [128, 2048, 512], P(('ep', 'tp')), may hold values from -0.125 to 0.125
- expert_up: bfloat16 [128, 2048, 512], P(('ep', 'tp')), may hold values from -0.125 to 0.125
- expert_down: bfloat16 [128, 512, 2048], P(('ep', 'tp')), may hold values from -0.25 to 0.25
- shared_gate: bfloat16 [2048, 512], P(None, 'tp'), may hold values from -0.125 to 0.125
- shared_up: bfloat16 [2048, 512], P(None, 'tp'), may hold values from -0.125 to 0.125
- shared_down: bfloat16 [512, 2048], P('tp'), may hold values from -0.25 to 0.25
Outputs:
- mixer_out: bfloat16 [32768, 2048], P(('grp', 'ep', 'tp')), parts along dimension 0
- moe_out: bfloat16 [32768, 2048], P(('grp', 'ep', 'tp')), parts along dimension 0
There are 2 independent parts, one for each index of `grp`. A program takes and returns all parts, laid end to end along the dimension named above; an argument that names none is the same for every part. Nothing has to cross between parts.
Inputs may be any that keep to these rules, and one draw needn't show every extreme that they name: `routes`: each row names 2 different experts; in each aligned block of 128 rows (the rows of one device) no expert is named by more than 3 rows, a bound that some block reaches. `log_decay`: below zero.
All inputs are finite; a program needn't handle non-finite values.
Results may differ from a plain program's by a relative error of at most 0.015.
Values may be sent and summed in bfloat16 or wider, within the bound.
No kernel may reach another device: no remote copies, remote signals or barrier semaphores. Data moves between devices by JAX's collectives and lax.ppermute only.
A program may use at most 128 MiB of HBM per device.

v0:
```python
import jax
import jax.numpy as jnp
from jax import lax
from jax.experimental import pallas as pl
from jax.experimental.pallas import tpu as pltpu
from jax.sharding import Mesh
from jax.sharding import PartitionSpec as P


BLOCK = 128
LANES = 128
TILE = 16
EP = ("ep_0", "ep_1")
EP_TP = ("ep_0", "ep_1", "tp")
GRP_EP = ("grp", "ep_0", "ep_1")
GRP_EP_TP = ("grp", "ep_0", "ep_1", "tp")
STATE_ROWS = 80

ROPE_BASE = 10000.0
GROUP_EPS = 1e-05
NORM_EPS = 1e-06


VMEM = pl.BlockSpec(memory_space=pltpu.VMEM)
SMEM = pl.BlockSpec(memory_space=pltpu.SMEM)
HBM = pl.BlockSpec(memory_space=pltpu.HBM)
F32 = jnp.float32
BF16 = jnp.bfloat16
MIB = 1 << 20


def call(kernel, out_shape, in_specs, out_specs, scratch, flops, moved, limit):
    return pl.pallas_call(
        kernel,
        out_shape=out_shape,
        in_specs=in_specs,
        out_specs=out_specs,
        scratch_shapes=scratch,
        compiler_params=pltpu.CompilerParams(vmem_limit_bytes=limit * MIB),
        cost_estimate=pl.CostEstimate(flops=flops, bytes_accessed=moved, transcendentals=0),
    )


def dot(a, b):
    return jnp.dot(a, b, preferred_element_type=F32)


def swap_matrix():
    side = TILE * TILE
    row = lax.broadcasted_iota(jnp.int32, (side, side), 0)
    col = lax.broadcasted_iota(jnp.int32, (side, side), 1)
    hit = (row // TILE == col % TILE) & (row % TILE == col // TILE)
    return jnp.where(hit, 1.0, 0.0).astype(BF16)


def rows_to_tiles(swap, rows):
    count = rows.shape[0] // TILE
    width = rows.shape[1] // LANES
    found = []
    for at in range(0, count, 2):
        pair = [
            jnp.concatenate(
                [
                    rows[g * TILE : (g + 1) * TILE, k * LANES : (k + 1) * LANES]
                    for k in range(width)
                ],
                axis=0,
            )
            for g in range(at, min(at + 2, count))
        ]
        out = dot(swap, jnp.concatenate(pair, axis=1)).astype(BF16)
        found += [out[:, g * LANES : (g + 1) * LANES] for g in range(len(pair))]
    return found


def prep_kernel(
    routes, x_hbm, gain_hbm, normed_hbm, outbound, places, x, gain, normed, tiles, used, sems
):
    copies = [
        pltpu.make_async_copy(x_hbm, x, sems.at[0]),
        pltpu.make_async_copy(gain_hbm, gain, sems.at[1]),
    ]
    for copy in copies:
        copy.start()
    outbound[...] = jnp.zeros_like(outbound)
    top = routes.shape[0] // x.shape[0]
    experts = used.shape[0]
    capacity = outbound.shape[0] // (experts * TILE)
    for e in range(experts):
        used[e] = 0
    for copy in copies:
        copy.wait()
    source = x[...].astype(F32)
    scale = lax.rsqrt(jnp.mean(source * source, axis=-1, keepdims=True) + NORM_EPS)
    rows = (source * scale * gain[...]).astype(BF16)
    normed[...] = rows
    keep = pltpu.make_async_copy(normed, normed_hbm, sems.at[2])
    keep.start()
    for g, tile in enumerate(rows_to_tiles(swap_matrix(), rows)):
        tiles[g * TILE * TILE : (g + 1) * TILE * TILE, :] = tile

    @pl.loop(0, x.shape[0], unroll=4)
    def _(n):
        row = tiles[pl.ds(pl.multiple_of(n * TILE, TILE), TILE), :]
        for k in range(top):
            p = n * top + k
            e = routes[p]
            rank = used[e]
            used[e] = rank + 1
            place = e * capacity + rank
            places[p] = place
            outbound[pl.ds(pl.multiple_of(place * TILE, TILE), TILE), :] = row

    keep.wait()


def expert_kernel(
    arrived_hbm,
    gate_hbm,
    up_hbm,
    down_hbm,
    out_hbm,
    gate_w,
    up_w,
    down_w,
    rows,
    arrived,
    out,
    sems,
    in_sems,
    out_sems,
):
    pieces = sems.shape[1]
    chunks = out_sems.shape[0]
    share = arrived.shape[0] // chunks
    landed = []
    for j in range(chunks):
        at = pl.ds(j * share, share)
        landed.append(pltpu.make_async_copy(arrived_hbm.at[at], arrived.at[at], in_sems.at[j]))
        landed[-1].start()
    copies = [[], [], []]
    for i, (src, dst) in enumerate(((gate_hbm, gate_w), (up_hbm, up_w), (down_hbm, down_w))):
        part = dst.shape[0] // pieces
        for j in range(pieces):
            at = pl.ds(j * part, part)
            copies[i].append(pltpu.make_async_copy(src.at[0, at], dst.at[at], sems.at[i, j]))
            copies[i][-1].start()
    swap = swap_matrix()
    side = TILE * TILE
    groups = arrived.shape[0] // side
    for at in range(0, groups, 2):
        if at * side % share == 0:
            landed[at * side // share].wait()
        pair = jnp.concatenate(
            [arrived[g * side : (g + 1) * side, :] for g in (at, at + 1)], axis=1
        )
        turned = dot(swap, pair).astype(BF16)
        for j in range(2):
            for k in range(TILE):
                rows[
                    (at + j) * TILE : (at + j + 1) * TILE, k * LANES : (k + 1) * LANES
                ] = turned[k * TILE : (k + 1) * TILE, j * LANES : (j + 1) * LANES]
    for copy in copies[0]:
        copy.wait()
    gated = jax.nn.silu(dot(rows[...], gate_w[...]))
    for copy in copies[1]:
        copy.wait()
    hidden = (gated * dot(rows[...], up_w[...])).astype(BF16)
    for copy in copies[2]:
        copy.wait()
    left = []
    step = rows.shape[0] // chunks
    for j in range(chunks):
        result = dot(hidden[j * step : (j + 1) * step, :], down_w[...]).astype(BF16)
        for g, tile in enumerate(rows_to_tiles(swap, result)):
            out[j * share + g * side : j * share + (g + 1) * side, :] = tile
        at = pl.ds(j * share, share)
        left.append(pltpu.make_async_copy(out.at[at], out_hbm.at[at], out_sems.at[j]))
        left[-1].start()
    for copy in left:
        copy.wait()


def turn_matrix():
    row = lax.broadcasted_iota(jnp.int32, (LANES, LANES), 0)
    col = lax.broadcasted_iota(jnp.int32, (LANES, LANES), 1)
    return row, col


def rotated(x, cosine, sine, half):
    row, col = turn_matrix()
    first = col % (2 * half) < half
    partner = jnp.where(first, col + half, col - half)
    turn = jnp.where(row == partner, jnp.where(first, -1.0, 1.0), 0.0).astype(BF16)
    return x.astype(F32) * cosine + dot(x, turn) * sine


def lower(size, strict=False):
    row = lax.broadcasted_iota(jnp.int32, (size, size), 0)
    col = lax.broadcasted_iota(jnp.int32, (size, size), 1)
    return row > col if strict else row >= col


def summed_f32(a, b, dims):
    return lax.dot_general(
        a, b, (dims, ((), ())), preferred_element_type=F32, precision=lax.Precision.HIGHEST
    )


def spread_heads(per_head, key_size):
    lane = lax.broadcasted_iota(jnp.int32, (per_head.shape[0], LANES), 1)
    out = per_head[:, 0:1]
    for h in range(1, per_head.shape[1]):
        out = jnp.where(lane >= h * key_size, per_head[:, h : h + 1], out)
    return out


def state_kernel(k, v, log_decay, cosine, sine, packed):
    heads = log_decay.shape[1]
    key_size = k.shape[1] // heads
    value_size = v.shape[1] // heads
    span = k.shape[0]
    k_rot = (rotated(k[...], cosine[...], sine[...], key_size // 2) * key_size ** (-0.5)).astype(
        BF16
    )
    above = jnp.where(lower(BLOCK, True), 1.0, 0.0)
    after = jnp.zeros((1, heads), F32)
    tails = [None] * (span // BLOCK)
    for b in reversed(range(span // BLOCK)):
        part = log_decay[b * BLOCK : (b + 1) * BLOCK, :]
        tails[b] = summed_f32(above, part, ((0,), (0,))) + after
        after = after + jnp.sum(part, axis=0, keepdims=True)
    tail = jnp.concatenate(tails, axis=0)
    faded = (k_rot.astype(F32) * jnp.exp(spread_heads(tail, key_size))).astype(BF16)
    state = dot(faded.T, v[...])
    for h in range(heads):
        packed[h * STATE_ROWS : h * STATE_ROWS + key_size, :] = state[
            h * key_size : (h + 1) * key_size, h * value_size : (h + 1) * value_size
        ].astype(BF16)
        whole = after[:, h : h + 1]
        high = whole.astype(BF16)
        low = (whole - high.astype(F32)).astype(BF16)
        pad = STATE_ROWS - key_size
        row = lax.broadcasted_iota(jnp.int32, (pad, LANES), 0)
        packed[h * STATE_ROWS + key_size : (h + 1) * STATE_ROWS, :] = jnp.where(
            row == 0, high.astype(F32), low.astype(F32)
        ).astype(BF16)


def retention_kernel(seat, q, k, v, gate, log_decay, cosine, sine, state_in, *rest):
    outs, gated = rest[:-1], rest[-1]
    heads = log_decay.shape[1]
    key_size = q.shape[1] // heads
    value_size = v.shape[1] // heads
    span = q.shape[0]
    q_rot = rotated(q[...], cosine[...], sine[...], key_size // 2).astype(BF16)
    k_rot = (rotated(k[...], cosine[...], sine[...], key_size // 2) * key_size ** (-0.5)).astype(
        BF16
    )
    keep = lower(BLOCK)
    ones = jnp.where(keep, 1.0, 0.0)
    lane = lax.broadcasted_iota(jnp.int32, (BLOCK, LANES), 1)
    state = state_in[...]
    for b in range(span // BLOCK):
        at = slice(b * BLOCK, (b + 1) * BLOCK)
        part = log_decay[at, :]
        column = summed_f32(ones, part, ((1,), (0,)))
        across = summed_f32(part, ones, ((0,), (1,)))
        total = column[BLOCK - 1 : BLOCK, :]
        q_part = q_rot[at, :]
        k_part = k_rot[at, :]
        v_part = v[at, :]
        lifted = q_part.astype(F32) * jnp.exp(spread_heads(column, key_size))
        tail = jnp.exp(spread_heads(total - column, key_size))
        faded = (k_part.astype(F32) * tail).astype(BF16)
        held = state.astype(BF16)
        grown = dot(faded.T, v_part)
        fade = []
        for h in range(heads):
            mine = (lane >= h * key_size) & (lane < (h + 1) * key_size)
            q_head = jnp.where(mine, q_part.astype(F32), 0.0).astype(BF16)
            scores = lax.dot_general(
                q_head, k_part, (((1,), (1,)), ((), ())), preferred_element_type=F32
            )
            gap = jnp.where(keep, column[:, h : h + 1] - across[h : h + 1, :], 0.0)
            weights = jnp.where(keep, scores * jnp.exp(gap), 0.0).astype(BF16)
            columns = slice(h * value_size, (h + 1) * value_size)
            kept = dot(weights, v_part[:, columns]) + dot(
                jnp.where(mine, lifted, 0.0).astype(BF16), held
            )
            center = jnp.mean(kept, axis=-1, keepdims=True)
            off = kept - center
            spread = jnp.mean(off * off, axis=-1, keepdims=True)
            act = jax.nn.silu(gate[at, columns].astype(F32))
            gated[at, columns] = (act * (off * lax.rsqrt(spread + GROUP_EPS))).astype(BF16)
            fade.append(
                state[h * key_size : (h + 1) * key_size, :] * jnp.exp(total[:, h : h + 1])
                + grown[h * key_size : (h + 1) * key_size, columns]
            )
        state = jnp.concatenate(fade, axis=0)
    count = len(outs)
    share = span // count
    for d in range(count):
        first = lax.rem(seat[0] + d, count) * share
        outs[d][...] = gated[pl.ds(pl.multiple_of(first, share), share), :]


def pack_kernel(core, gate_w, up_w, down_w, out):
    half = gate_w.shape[0] // 2
    first = pl.multiple_of(core[0] * half, TILE)
    out[0:half, :] = gate_w[pl.ds(first, half), :]
    out[half : 2 * half, :] = up_w[pl.ds(first, half), :]
    part = down_w.shape[0] // 2
    first = pl.multiple_of(core[0] * part, TILE)
    for k in range(down_w.shape[1] // LANES):
        at = 2 * half + k * part
        out[at : at + part, :] = down_w[pl.ds(first, part), k * LANES : (k + 1) * LANES]


def shared_kernel(core, normed, gate_w, up_w, down_w, *refs):
    count = (len(refs) - 3) // 2
    mine, theirs = refs[:count], refs[count : 2 * count]
    out, packed, down = refs[2 * count :]
    rows = normed[...]
    half = rows.shape[1] // 2
    part = down.shape[0] // 2
    hidden = jax.nn.silu(dot(rows, gate_w[...])) * dot(rows, up_w[...])
    total = dot(hidden.astype(BF16), down_w[...])
    for a, b in zip(mine, theirs):
        packed[0] = jnp.where(core[0] == 0, a[...], b[...])
        packed[1] = jnp.where(core[0] == 0, b[...], a[...])
        gated = dot(rows[:, :half], packed[0, :half]) + dot(rows[:, half:], packed[1, :half])
        up = dot(rows[:, :half], packed[0, half : 2 * half]) + dot(
            rows[:, half:], packed[1, half : 2 * half]
        )
        for c in range(2):
            for k in range(down.shape[1] // LANES):
                at = 2 * half + k * part
                down[c * part : (c + 1) * part, k * LANES : (k + 1) * LANES] = packed[
                    c, at : at + part
                ]
        hidden = (jax.nn.silu(gated) * up).astype(BF16)
        total = total + dot(hidden, down[...])
    out[...] = total


def finish_kernel(places, core, weight, *refs):
    count = (len(refs) - 11) // 3
    gated = refs[:count]
    hbm = refs[count : 3 * count + 1]
    mixer_out, moe_out, picked, rows, returned, shared, own, mine, theirs, sems = refs[
        3 * count + 1 :
    ]
    places_of = [returned, shared, own]
    places_of += [mine.at[d] for d in range(count - 1)] + [theirs.at[d] for d in range(count - 1)]
    copies = [
        pltpu.make_async_copy(a, b, sems.at[i]) for i, (a, b) in enumerate(zip(hbm, places_of))
    ]
    for copy in copies:
        copy.start()
    swap = swap_matrix()
    side = TILE * TILE
    number = moe_out.shape[0]
    top = weight.shape[1]
    copies[0].wait()

    @pl.loop(0, number, unroll=4)
    def _(n):
        for k in range(top):
            place = places[n * top + k]
            picked[k, pl.ds(pl.multiple_of(n * TILE, TILE), TILE), :] = returned[
                pl.ds(pl.multiple_of(place * TILE, TILE), TILE), :
            ]

    for k in range(top):
        for at in range(0, number // TILE, 2):
            pair = jnp.concatenate(
                [picked[k, g * side : (g + 1) * side, :] for g in (at, at + 1)], axis=1
            )
            turned = dot(swap, pair).astype(BF16)
            for j in range(2):
                for c in range(TILE):
                    rows[
                        k,
                        (at + j) * TILE : (at + j + 1) * TILE,
                        c * LANES : (c + 1) * LANES,
                    ] = turned[c * TILE : (c + 1) * TILE, j * LANES : (j + 1) * LANES]
    for copy in copies[1:]:
        copy.wait()
    total = shared[...]
    for k in range(top):
        total = total + rows[k].astype(F32) * weight[:, k : k + 1]
    moe_out[...] = total.astype(BF16)
    mixed = dot(gated[0][...], own[...])
    half = own.shape[0] // 2
    for d in range(count - 1):
        low, high = gated[d + 1][:, :half], gated[d + 1][:, half:]
        mixed = mixed + dot(jnp.where(core[0] == 0, low, high), mine[d])
        mixed = mixed + dot(jnp.where(core[0] == 0, high, low), theirs[d])
    mixer_out[...] = mixed.astype(BF16)


def moved_by(array, axis, step, around=True):
    count = lax.axis_size(axis)
    pairs = [
        (s, (s + step) % count) for s in range(count) if around or 0 <= s + step < count
    ]
    return lax.ppermute(array, axis, pairs)


def opened(packed):
    wide = packed.astype(F32)
    size = STATE_ROWS - TILE
    return wide[size : size + 1, :] + wide[size + 1 : size + 2, :], wide[:size, :]


def closed(part):
    log, state = part
    high = log.astype(BF16).astype(F32)
    row = lax.broadcasted_iota(jnp.int32, (TILE, LANES), 0)
    return jnp.concatenate([state, jnp.where(row == 0, high, log - high)], axis=0).astype(BF16)


def joined(earlier, later):
    return earlier[0] + later[0], earlier[1] * jnp.exp(later[0]) + later[1]


def picked_by(core, a, b):
    return jnp.where(core == 0, a.astype(F32), b.astype(F32)).astype(BF16)


def chip_kernel(core, own, other, out):
    mine = picked_by(core[0], own[:STATE_ROWS, :], own[STATE_ROWS:, :])
    theirs = picked_by(core[0], other[:STATE_ROWS, :], other[STATE_ROWS:, :])
    early, late = picked_by(core[0], mine, theirs), picked_by(core[0], theirs, mine)
    out[...] = closed(joined(opened(early), opened(late)))


def near_kernel(chip, far3, far2, far1, before, window):
    start = joined(joined(opened(far3[...]), opened(far2[...])), opened(far1[...]))
    before[...] = closed(start)
    window[...] = closed(joined(start, opened(chip[...])))


def far_kernel(before, far12, far8, far4, prefix):
    start = joined(joined(opened(far12[...]), opened(far8[...])), opened(far4[...]))
    prefix[...] = closed(joined(start, opened(before[...])))


def enter_kernel(core, mine, theirs, other, state):
    size = STATE_ROWS - TILE
    for h in range(other.shape[0] // STATE_ROWS):
        held = jnp.where(core[0] == h, mine[...].astype(F32), theirs[...].astype(F32))
        chip_before = opened(held)
        first = opened(other[h * STATE_ROWS : (h + 1) * STATE_ROWS, :])
        both = joined(chip_before, first)
        state[h * size : (h + 1) * size, :] = jnp.where(core[0] == 0, chip_before[1], both[1])


def small(kernel, outs, in_specs, out_specs):
    return call(kernel, outs, in_specs, out_specs, [], 100000, 100000, 2)


def per_device(
    queries,
    keys,
    values,
    gate,
    log_decay,
    w_out,
    moe_input,
    moe_gain,
    routes,
    route_weight,
    expert_gate,
    expert_up,
    expert_down,
    shared_gate,
    shared_up,
    shared_down,
):
    span = queries.shape[0]
    heads = log_decay.shape[1]
    key_size = queries.shape[1] // heads
    value_size = values.shape[1] // heads
    rows_dev, width = moe_input.shape
    top = routes.shape[1]
    n_tp = lax.axis_size("tp")
    experts = lax.axis_size(EP) * n_tp
    capacity = rows_dev * top * 3 // (2 * experts)
    hidden_size = expert_gate.shape[2]
    shared_size = shared_gate.shape[1]
    slots = experts * capacity
    tile_rows = slots * TILE

    core = lax.axis_index("ep_1").reshape(1).astype(jnp.int32)
    seat = lax.axis_index("tp").reshape(1).astype(jnp.int32)
    around = range(1, n_tp)
    half_out = w_out.shape[0] // 2
    packed_shape = jax.ShapeDtypeStruct((STATE_ROWS, value_size), BF16)

    out_half = lax.dynamic_slice_in_dim(w_out, core[0] * half_out, half_out, 0)
    out_mine = [moved_by(out_half, "tp", d) for d in around]

    normed, outbound, places = call(
        prep_kernel,
        (
            jax.ShapeDtypeStruct((rows_dev, width), BF16),
            jax.ShapeDtypeStruct((tile_rows, LANES), BF16),
            jax.ShapeDtypeStruct((rows_dev * top,), jnp.int32),
        ),
        [SMEM, HBM, HBM],
        (HBM, VMEM, SMEM),
        [
            pltpu.VMEM((rows_dev, width), BF16),
            pltpu.VMEM((1, width), F32),
            pltpu.VMEM((rows_dev, width), BF16),
            pltpu.VMEM((rows_dev * TILE, LANES), BF16),
            pltpu.SMEM((experts,), jnp.int32),
            pltpu.SemaphoreType.DMA((3,)),
        ],
        2 * rows_dev * width * 256,
        4 * rows_dev * width,
        62,
    )(routes.reshape(-1), moe_input, moe_gain.reshape(1, width))

    arrived = lax.all_to_all(
        outbound.reshape(experts, capacity * TILE, LANES),
        EP_TP,
        split_axis=0,
        concat_axis=0,
        tiled=True,
    )

    half = key_size // 2
    frequency = ROPE_BASE ** (-jnp.arange(half, dtype=F32) / half)
    spots = lax.axis_index(EP) * span + jnp.arange(span, dtype=jnp.int32)
    angles = spots.astype(F32)[:, None] * jnp.tile(frequency, LANES // half)[None, :]
    cosine = jnp.cos(angles)
    sine = jnp.sin(angles)

    own = call(
        state_kernel,
        jax.ShapeDtypeStruct((heads * STATE_ROWS, value_size), BF16),
        [VMEM] * 5,
        VMEM,
        [],
        2 * span * LANES * 512,
        4 * span * LANES * 4,
        12,
    )(keys, values, log_decay, cosine, sine)
    other = moved_by(own, "ep_1", 1)
    chip = small(chip_kernel, packed_shape, [SMEM, VMEM, VMEM], VMEM)(core, own, other)
    near = [moved_by(chip, "ep_0", d, False) for d in (3, 2, 1)]
    before, window = small(
        near_kernel, (packed_shape, packed_shape), [VMEM] * 4, (VMEM, VMEM)
    )(chip, *near)
    far = [moved_by(window, "ep_0", d, False) for d in (12, 8, 4)]
    prefix = small(far_kernel, packed_shape, [VMEM] * 4, VMEM)(before, *far)
    swapped = moved_by(prefix, "ep_1", 1)
    state_in = small(
        enter_kernel,
        jax.ShapeDtypeStruct((heads * key_size, value_size), F32),
        [SMEM] + [VMEM] * 3,
        VMEM,
    )(core, prefix, swapped, other)

    shared_half = call(
        pack_kernel,
        jax.ShapeDtypeStruct((width * 3 * shared_size // 2 // LANES, LANES), BF16),
        [SMEM] + [VMEM] * 3,
        VMEM,
        [],
        100000,
        6 * width * shared_size,
        8,
    )(core, shared_gate, shared_up, shared_down)
    shared_mine = [moved_by(shared_half, "tp", d) for d in around]
    shared_theirs = [moved_by(part, "ep_1", 1) for part in shared_mine]
    out_theirs = [moved_by(part, "ep_1", 1) for part in out_mine]
    shared_sum = call(
        shared_kernel,
        jax.ShapeDtypeStruct((rows_dev, width), F32),
        [SMEM] + [VMEM] * (4 + 2 * (n_tp - 1)),
        VMEM,
        [
            pltpu.VMEM((2,) + shared_half.shape, BF16),
            pltpu.VMEM((shared_size, width), BF16),
        ],
        2 * n_tp * rows_dev * width * shared_size * 3,
        10 * rows_dev * width * 2,
        20,
    )(core, normed, shared_gate, shared_up, shared_down, *shared_mine, *shared_theirs)

    pieces, chunks = 4, 3
    answers = call(
        expert_kernel,
        jax.ShapeDtypeStruct((tile_rows, LANES), BF16),
        [HBM] * 4,
        HBM,
        [
            pltpu.VMEM((width, hidden_size), BF16),
            pltpu.VMEM((width, hidden_size), BF16),
            pltpu.VMEM((hidden_size, width), BF16),
            pltpu.VMEM((slots, width), BF16),
            pltpu.VMEM((tile_rows, LANES), BF16),
            pltpu.VMEM((tile_rows, LANES), BF16),
            pltpu.SemaphoreType.DMA((3, pieces)),
            pltpu.SemaphoreType.DMA((chunks,)),
            pltpu.SemaphoreType.DMA((chunks,)),
        ],
        2 * slots * width * hidden_size * 3,
        3 * 2 * width * hidden_size,
        61,
    )(arrived.reshape(tile_rows, LANES), expert_gate, expert_up, expert_down)
    returned = lax.all_to_all(
        answers.reshape(experts, capacity * TILE, LANES),
        EP_TP,
        split_axis=0,
        concat_axis=0,
        tiled=True,
    )

    gated = call(
        retention_kernel,
        tuple(jax.ShapeDtypeStruct((rows_dev, heads * value_size), BF16) for _ in range(n_tp)),
        [SMEM] + [VMEM] * 8,
        (VMEM,) * n_tp,
        [pltpu.VMEM((span, heads * value_size), BF16)],
        2 * span * heads * value_size * 1000,
        10 * rows_dev * width * 2,
        20,
    )(seat, queries, keys, values, gate, log_decay, cosine, sine, state_in)
    gated = [gated[0]] + [moved_by(gated[d], "tp", d) for d in around]

    return call(
        finish_kernel,
        tuple(jax.ShapeDtypeStruct((rows_dev, width), BF16) for _ in range(2)),
        [SMEM, SMEM, VMEM] + [VMEM] * n_tp + [HBM] * (2 * n_tp + 1),
        (VMEM,) * 2,
        [
            pltpu.VMEM((top, rows_dev * TILE, LANES), BF16),
            pltpu.VMEM((top, rows_dev, width), BF16),
            pltpu.VMEM((tile_rows, LANES), BF16),
            pltpu.VMEM((rows_dev, width), F32),
            pltpu.VMEM((2 * half_out, width), BF16),
            pltpu.VMEM((n_tp - 1, half_out, width), BF16),
            pltpu.VMEM((n_tp - 1, half_out, width), BF16),
            pltpu.SemaphoreType.DMA((2 * n_tp + 1,)),
        ],
        2 * rows_dev * width * 1500,
        10 * rows_dev * width * 2,
        61,
    )(
        places,
        core,
        route_weight,
        *gated,
        returned.reshape(tile_rows, LANES),
        shared_sum,
        w_out,
        *out_mine,
        *out_theirs,
    )


def solution(mesh):
    split = Mesh(
        mesh.devices.reshape(mesh.shape["grp"], mesh.shape["ep"] // 2, 2, mesh.shape["tp"]),
        ("grp", "ep_0", "ep_1", "tp"),
    )
    return jax.shard_map(
        per_device,
        mesh=split,
        in_specs=(
            P(GRP_EP, "tp"),
            P(GRP_EP, "tp"),
            P(GRP_EP, "tp"),
            P(GRP_EP, "tp"),
            P(GRP_EP, "tp"),
            P("tp", None),
            P(GRP_EP_TP, None),
            P(),
            P(GRP_EP_TP, None),
            P(GRP_EP_TP, None),
            P(EP_TP, None, None),
            P(EP_TP, None, None),
            P(EP_TP, None, None),
            P(None, "tp"),
            P(None, "tp"),
            P("tp", None),
        ),
        out_specs=(P(GRP_EP_TP, None), P(GRP_EP_TP, None)),
        check_vma=False,
    )
```

profile of v0, /device:TPU:33, one launch (start us, length us, event | category | flops | bytes accessed | tf_op | source)
XLA Modules:
  0.0 306.2 jit_solution(12729038702010605245)
XLA Ops:
  0.6 0.8 copy.21
  2.1 4.7 %shard_map.167 = (bf16[128,2048]{1,0:T(8,128)(2,1)}, bf16[6144,128]{1,0:T(8,128)(2,1)}, s32[256]{0:T(256)}) custom-call(s32[256]{0:T(256)} %reshape.40.routes, bf16[128,2048]{1,0:T(8,128)(2,1)} %x_hbm.1, f32[1,2048]{1,0:T(1,128)} %bitcast.10), custom_call_target="tpu_custom_call" | custom-call | flops 134217728 | bytes 1048576 | tf_op jit(solution)/shard_map/pallas_call | solution.py:505
  6.8 107.0 %all_to_all.10 = bf16[128,48,128]{2,1,0:T(8,128)(2,1)} all-to-all(bf16[128,48,128]{2,1,0:T(8,128)(2,1)} %bitcast.9), channel_id=1, replica_groups=mesh['grp'=2,'ep_0'=16,'ep_1'=2,'tp'=4] {'ep_0','ep_1','tp'}, dimensions={0} | all-to-all | bytes 3145728 | tf_op jit(solution)/shard_map/all_to_all | solution.py:527
  113.9 8.1 %shard_map.174 = bf16[6144,128]{1,0:T(8,128)(2,1)} custom-call(bf16[6144,128]{1,0:T(8,128)(2,1)} %bitcast.8, bf16[1,2048,512]{2,1,0:T(8,128)(2,1)} %gate_hbm.1, bf16[1,2048,512]{2,1,0:T(8,128)(2,1)} %up_hbm.1, bf16[1,512,2048]{2,1,0:T(8,128)(2,1)} %down_hbm.1), custom_call_target="tpu_custom_call" | custom-call | flops 2415919104 | bytes 6291456 | tf_op jit(solution)/shard_map/pallas_call | solution.py:596
  122.0 9.5 %all-to-all-start.1 = ((bf16[128,48,128]{2,1,0:T(8,128)(2,1)}), bf16[128,48,128]{2,1,0:T(8,128)(2,1)}, u32[]{:S(2)}, u32[]{:S(2)}) async-start(bf16[128,48,128]{2,1,0:T(8,128)(2,1)} %bitcast.7), calls=%async_computation.1 | async-start | bytes 3145728 | tf_op jit(solution)/shard_map/all_to_all | solution.py:616
  131.7 1.6 collective-permute-start.11
  133.4 2.4 collective-permute-start.12
  135.8 1.2 collective-permute-start.13
  136.9 1.9 constant_dynamic-slice_fusion
  139.4 1.0 multiply_sine_fusion
  140.4 0.8 shard_map.168.own
  141.2 1.6 collective-permute-start
  142.9 12.1 %collective-permute-done.11.refs_0_ = bf16[3072,128]{1,0:T(8,128)(2,1)} collective-permute-done((bf16[3072,128]{1,0:T(8,128)(2,1)S(1)}, bf16[3072,128]{1,0:T(8,128)(2,1)}, u32[]{:S(2)}, u32[]{:S(2)}) %collective-permute-start.11) | collective-permute-done | bytes 786464 | tf_op jit(solution)/shard_map/ppermute | solution.py:408
  155.0 28.4 %collective-permute-start.14 = (bf16[3072,128]{1,0:T(8,128)(2,1)}, bf16[3072,128]{1,0:T(8,128)(2,1)}, u32[]{:S(2)}, u32[]{:S(2)}) collective-permute-start(bf16[3072,128]{1,0:T(8,128)(2,1)} %collective-permute-done.11.refs_0_), channel_id=1, source_target_pairs={{0,4},{4,0},{1,5},{5,1},{2,6},{6,2},{3,7},{7,3},{8,12},{12,8},{9,1... | collective-permute-start | bytes 2359304 | tf_op jit(solution)/shard_map/ppermute | solution.py:408
  184.0 1.3 collective-permute-start.1
  185.3 0.9 collective-permute-done.1.far3
  186.2 14.6 %collective-permute-start.2 = (bf16[80,128]{1,0:T(8,128)(2,1)S(1)}, bf16[80,128]{1,0:T(8,128)(2,1)S(1)}, u32[]{:S(2)}, u32[]{:S(2)}) collective-permute-start(bf16[80,128]{1,0:T(8,128)(2,1)S(1)} %shard_map.169.chip), channel_id=1, source_target_pairs={{0,16},{8,24},{16,32},{24,40},{32,48},{40,56},{48,64},{56,72},{64,... | collective-permute-start | bytes 61448 | tf_op jit(solution)/shard_map/ppermute | solution.py:408
  200.8 0.9 collective-permute-done.2.far2
  201.7 3.8 %collective-permute-start.3 = (bf16[80,128]{1,0:T(8,128)(2,1)S(1)}, bf16[80,128]{1,0:T(8,128)(2,1)S(1)}, u32[]{:S(2)}, u32[]{:S(2)}) collective-permute-start(bf16[80,128]{1,0:T(8,128)(2,1)S(1)} %shard_map.169.chip), channel_id=1, source_target_pairs={{0,8},{8,16},{16,24},{24,32},{32,40},{40,48},{48,56},{56,64},{64,7... | collective-permute-start | bytes 61448 | tf_op jit(solution)/shard_map/ppermute | solution.py:408
  205.5 0.9 collective-permute-done.3.far1
  206.4 16.7 %collective-permute-start.4 = (bf16[80,128]{1,0:T(8,128)(2,1)S(1)}, bf16[80,128]{1,0:T(8,128)(2,1)S(1)}, u32[]{:S(2)}, u32[]{:S(2)}) collective-permute-start(bf16[80,128]{1,0:T(8,128)(2,1)S(1)} %get-tuple-element.13), channel_id=1, source_target_pairs={{0,96},{8,104},{16,112},{24,120},{1,97},{9,105},{17,113},{25,121},... | collective-permute-start | bytes 61448 | tf_op jit(solution)/shard_map/ppermute | solution.py:408
  223.2 0.9 collective-permute-done.4.far12
  224.1 1.3 collective-permute-start.5
  225.4 0.9 collective-permute-done.5.far8
  226.3 13.3 %collective-permute-start.6 = (bf16[80,128]{1,0:T(8,128)(2,1)S(1)}, bf16[80,128]{1,0:T(8,128)(2,1)S(1)}, u32[]{:S(2)}, u32[]{:S(2)}) collective-permute-start(bf16[80,128]{1,0:T(8,128)(2,1)S(1)} %get-tuple-element.13), channel_id=1, source_target_pairs={{0,32},{8,40},{16,48},{24,56},{32,64},{40,72},{48,80},{56,88},{64,... | collective-permute-start | bytes 61448 | tf_op jit(solution)/shard_map/ppermute | solution.py:408
  239.6 0.9 collective-permute-done.6.far4
  241.1 5.6 %collective-permute-start.7 = (bf16[80,128]{1,0:T(8,128)(2,1)}, bf16[80,128]{1,0:T(8,128)(2,1)}, u32[]{:S(2)}, u32[]{:S(2)}) collective-permute-start(bf16[80,128]{1,0:T(8,128)(2,1)} %shard_map.171.mine), channel_id=1, source_target_pairs={{0,4},{4,0},{1,5},{5,1},{2,6},{6,2},{3,7},{7,3},{8,12},{12,8},{9,1... | collective-permute-start | bytes 61448 | tf_op jit(solution)/shard_map/ppermute | solution.py:408
  246.7 1.2 collective-permute-done.7.theirs
  247.8 0.8 copy-done.9
  248.6 0.8 shard_map.172.state_in
  249.4 0.9 copy-done.7
  250.3 0.9 copy-done.10
  251.2 2.9 shard_map.173
  256.0 2.5 collective-permute-start.10
  258.5 1.3 collective-permute-done.10.refs_3_
  259.8 2.1 collective-permute-start.18
  261.9 1.3 collective-permute-start.19
  263.2 2.1 collective-permute-start.15
  265.6 8.3 %collective-permute-done.18.refs_8_ = bf16[128,2048]{1,0:T(8,128)(2,1)} collective-permute-done((bf16[128,2048]{1,0:T(8,128)(2,1)}, bf16[128,2048]{1,0:T(8,128)(2,1)}, u32[]{:S(2)}, u32[]{:S(2)}) %collective-permute-start.18) | collective-permute-done | bytes 524320 | tf_op jit(solution)/shard_map/ppermute | solution.py:408
  273.9 2.1 collective-permute-start.20
  276.0 10.3 %collective-permute-done.19.refs_9_ = bf16[128,2048]{1,0:T(8,128)(2,1)} collective-permute-done((bf16[128,2048]{1,0:T(8,128)(2,1)}, bf16[128,2048]{1,0:T(8,128)(2,1)}, u32[]{:S(2)}, u32[]{:S(2)}) %collective-permute-start.19) | collective-permute-done | bytes 524320 | tf_op jit(solution)/shard_map/ppermute | solution.py:408
  286.3 1.6 collective-permute-start.21
  287.9 0.7 copy.24.weight
  288.9 3.2 %collective-permute-start.9 = (bf16[128,256]{1,0:T(8,128)(2,1)}, bf16[128,256]{1,0:T(8,128)(2,1)S(1)}, u32[]{:S(2)}, u32[]{:S(2)}) collective-permute-start(bf16[128,256]{1,0:T(8,128)(2,1)} %copy-done.12), channel_id=1, source_target_pairs={{0,2},{1,3},{2,0},{3,1},{4,6},{5,7},{6,4},{7,5},{8,10},{9,11},{10,... | collective-permute-start | bytes 196616 | tf_op jit(solution)/shard_map/ppermute | solution.py:408
  292.1 1.0 copy-done.5
  293.2 5.0 %shard_map.176.refs_5_ = f32[128,2048]{1,0:T(8,128)S(1)} custom-call(s32[1]{0:T(128)} %bitcast.1.core, bf16[128,2048]{1,0:T(8,128)(2,1)S(1)} %copy-done.5, bf16[2048,128]{1,0:T(8,128)(2,1)S(1)} %copy-done.1, bf16[2048,128]{1,0:T(8,128)(2,1)S(1)} %copy-done.2, bf16[128,2048]{1,0:T(8,128)(2,1)S(1)} %copy-done.3, ...), custom_call_target="tpu_custom_call" | custom-call | flops 805306368 | bytes 5242880 | tf_op jit(solution)/shard_map/pallas_call | solution.py:581
  298.2 1.0 copy-done
  299.8 6.2 %shard_map.177 = (bf16[128,2048]{1,0:T(8,128)(2,1)}, bf16[128,2048]{1,0:T(8,128)(2,1)}) custom-call(s32[256]{0:T(256)} %get-tuple-element.11.places, s32[1]{0:T(128)} %bitcast.1.core, f32[128,2]{1,0:T(8,128)} %copy.24.weight, bf16[128,256]{1,0:T(8,128)(2,1)} %copy-done.11, bf16[128,256]{1,0:T(8,128)(2,1)} %copy-done.15, bf16[128,256]{1,0:T(8,128)(2,1)} %copy-done.16, ...), custom_call_target="tpu_custom_call" | custom-call | flops 786432000 | bytes 5242880 | tf_op jit(solution)/shard_map/pallas_call | solution.py:636
  (60 shorter events, 5.8 us)
Async XLA Ops:
  122.0 9.6 %copy-start.1 = (bf16[2048,128]{1,0:T(8,128)(2,1)S(1)}, bf16[2048,128]{1,0:T(8,128)(2,1)}, u32[]{:S(2)}) copy-start(bf16[2048,128]{1,0:T(8,128)(2,1)} %gate_w.3) | copy-start | bytes 1572868
  122.0 9.6 %copy-start.2 = (bf16[2048,128]{1,0:T(8,128)(2,1)S(1)}, bf16[2048,128]{1,0:T(8,128)(2,1)}, u32[]{:S(2)}) copy-start(bf16[2048,128]{1,0:T(8,128)(2,1)} %up_w.3) | copy-start | bytes 1572868
  122.0 9.6 %copy-start.3 = (bf16[128,2048]{1,0:T(8,128)(2,1)S(1)}, bf16[128,2048]{1,0:T(8,128)(2,1)}, u32[]{:S(2)}) copy-start(bf16[128,2048]{1,0:T(8,128)(2,1)} %down_w.3) | copy-start | bytes 1572868
  122.0 177.2 %all-to-all-start.1 = ((bf16[128,48,128]{2,1,0:T(8,128)(2,1)}), bf16[128,48,128]{2,1,0:T(8,128)(2,1)}, u32[]{:S(2)}, u32[]{:S(2)}) async-start(bf16[128,48,128]{2,1,0:T(8,128)(2,1)} %bitcast.7), calls=%async_computation.1 | async-start | bytes 3145728 | tf_op jit(solution)/shard_map/all_to_all | solution.py:616
  131.6 7.6 %copy-start.17 = (f32[512,2]{0,1:T(2,128)S(1)}, f32[512,2]{0,1:T(2,128)}, u32[]{:S(2)}) copy-start(f32[512,2]{0,1:T(2,128)} %param.20) | copy-start | bytes 12292
  131.6 8.8 %copy-start.4 = (bf16[512,256]{1,0:T(8,128)(2,1)S(1)}, bf16[512,256]{1,0:T(8,128)(2,1)}, u32[]{:S(2)}) copy-start(bf16[512,256]{1,0:T(8,128)(2,1)} %v.3) | copy-start | bytes 786436
  131.6 8.8 %copy-start.6 = (bf16[512,128]{1,0:T(8,128)(2,1)S(1)}, bf16[512,128]{1,0:T(8,128)(2,1)}, u32[]{:S(2)}) copy-start(bf16[512,128]{1,0:T(8,128)(2,1)} %k.3) | copy-start | bytes 393220
  131.7 23.3 %collective-permute-start.11 = (bf16[3072,128]{1,0:T(8,128)(2,1)S(1)}, bf16[3072,128]{1,0:T(8,128)(2,1)}, u32[]{:S(2)}, u32[]{:S(2)}) collective-permute-start(bf16[3072,128]{1,0:T(8,128)(2,1)S(1)} %shard_map.175), channel_id=1, source_target_pairs={{0,1},{1,2},{2,3},{3,0},{4,5},{5,6},{6,7},{7,4},{8,9},{9,10},{10,1... | collective-permute-start | bytes 2359304 | tf_op jit(solution)/shard_map/ppermute | solution.py:408
  133.4 129.8 %collective-permute-start.12 = (bf16[3072,128]{1,0:T(8,128)(2,1)S(1)}, bf16[3072,128]{1,0:T(8,128)(2,1)}, u32[]{:S(2)}, u32[]{:S(2)}) collective-permute-start(bf16[3072,128]{1,0:T(8,128)(2,1)S(1)} %shard_map.175), channel_id=1, source_target_pairs={{0,2},{1,3},{2,0},{3,1},{4,6},{5,7},{6,4},{7,5},{8,10},{9,11},{10,... | collective-permute-start | bytes 2359304 | tf_op jit(solution)/shard_map/ppermute | solution.py:408
  135.8 129.5 %collective-permute-start.13 = (bf16[3072,128]{1,0:T(8,128)(2,1)S(1)}, bf16[3072,128]{1,0:T(8,128)(2,1)}, u32[]{:S(2)}, u32[]{:S(2)}) collective-permute-start(bf16[3072,128]{1,0:T(8,128)(2,1)S(1)} %shard_map.175), channel_id=1, source_target_pairs={{0,3},{1,0},{2,1},{3,2},{4,7},{5,4},{6,5},{7,6},{8,11},{9,8},{10,9... | collective-permute-start | bytes 2359304 | tf_op jit(solution)/shard_map/ppermute | solution.py:408
  138.8 123.1 %collective-permute-start.17 = (bf16[128,2048]{1,0:T(8,128)(2,1)}, bf16[128,2048]{1,0:T(8,128)(2,1)}, u32[]{:S(2)}, u32[]{:S(2)}) collective-permute-start(bf16[128,2048]{1,0:T(8,128)(2,1)} %constant_dynamic-slice_fusion), channel_id=1, source_target_pairs={{0,1},{1,2},{2,3},{3,0},{4,5},{5,6},{6,7},{7,4},{8,9},{9,10},{10,1... | collective-permute-start | bytes 1572872 | tf_op jit(solution)/shard_map/ppermute | solution.py:408
  140.4 147.5 %copy-start.18 = (f32[128,2]{0,1:T(2,128)S(1)}, f32[128,2]{0,1:T(2,128)}, u32[]{:S(2)}) copy-start(f32[128,2]{0,1:T(2,128)} %param.25) | copy-start | bytes 3076
  141.2 42.2 %collective-permute-start = (bf16[160,128]{1,0:T(8,128)(2,1)S(1)}, bf16[160,128]{1,0:T(8,128)(2,1)S(1)}, u32[]{:S(2)}, u32[]{:S(2)}) collective-permute-start(bf16[160,128]{1,0:T(8,128)(2,1)S(1)} %shard_map.168.own), channel_id=1, source_target_pairs={{0,4},{4,0},{1,5},{5,1},{2,6},{6,2},{3,7},{7,3},{8,12},{12,8},{9,1... | collective-permute-start | bytes 122888 | tf_op jit(solution)/shard_map/ppermute | solution.py:408
  155.0 132.9 %collective-permute-start.14 = (bf16[3072,128]{1,0:T(8,128)(2,1)}, bf16[3072,128]{1,0:T(8,128)(2,1)}, u32[]{:S(2)}, u32[]{:S(2)}) collective-permute-start(bf16[3072,128]{1,0:T(8,128)(2,1)} %collective-permute-done.11.refs_0_), channel_id=1, source_target_pairs={{0,4},{4,0},{1,5},{5,1},{2,6},{6,2},{3,7},{7,3},{8,12},{12,8},{9,1... | collective-permute-start | bytes 2359304 | tf_op jit(solution)/shard_map/ppermute | solution.py:408
  183.4 0.6 copy-start.8
  184.0 2.2 collective-permute-start.1
  186.2 15.5 %collective-permute-start.2 = (bf16[80,128]{1,0:T(8,128)(2,1)S(1)}, bf16[80,128]{1,0:T(8,128)(2,1)S(1)}, u32[]{:S(2)}, u32[]{:S(2)}) collective-permute-start(bf16[80,128]{1,0:T(8,128)(2,1)S(1)} %shard_map.169.chip), channel_id=1, source_target_pairs={{0,16},{8,24},{16,32},{24,40},{32,48},{40,56},{48,64},{56,72},{64,... | collective-permute-start | bytes 61448 | tf_op jit(solution)/shard_map/ppermute | solution.py:408
  201.7 4.7 %collective-permute-start.3 = (bf16[80,128]{1,0:T(8,128)(2,1)S(1)}, bf16[80,128]{1,0:T(8,128)(2,1)S(1)}, u32[]{:S(2)}, u32[]{:S(2)}) collective-permute-start(bf16[80,128]{1,0:T(8,128)(2,1)S(1)} %shard_map.169.chip), channel_id=1, source_target_pairs={{0,8},{8,16},{16,24},{24,32},{32,40},{40,48},{48,56},{56,64},{64,7... | collective-permute-start | bytes 61448 | tf_op jit(solution)/shard_map/ppermute | solution.py:408
  206.4 17.6 %collective-permute-start.4 = (bf16[80,128]{1,0:T(8,128)(2,1)S(1)}, bf16[80,128]{1,0:T(8,128)(2,1)S(1)}, u32[]{:S(2)}, u32[]{:S(2)}) collective-permute-start(bf16[80,128]{1,0:T(8,128)(2,1)S(1)} %get-tuple-element.13), channel_id=1, source_target_pairs={{0,96},{8,104},{16,112},{24,120},{1,97},{9,105},{17,113},{25,121},... | collective-permute-start | bytes 61448 | tf_op jit(solution)/shard_map/ppermute | solution.py:408
  224.1 2.2 collective-permute-start.5
  226.3 14.2 %collective-permute-start.6 = (bf16[80,128]{1,0:T(8,128)(2,1)S(1)}, bf16[80,128]{1,0:T(8,128)(2,1)S(1)}, u32[]{:S(2)}, u32[]{:S(2)}) collective-permute-start(bf16[80,128]{1,0:T(8,128)(2,1)S(1)} %get-tuple-element.13), channel_id=1, source_target_pairs={{0,32},{8,40},{16,48},{24,56},{32,64},{40,72},{48,80},{56,88},{64,... | collective-permute-start | bytes 61448 | tf_op jit(solution)/shard_map/ppermute | solution.py:408
  241.1 6.8 %collective-permute-start.7 = (bf16[80,128]{1,0:T(8,128)(2,1)}, bf16[80,128]{1,0:T(8,128)(2,1)}, u32[]{:S(2)}, u32[]{:S(2)}) collective-permute-start(bf16[80,128]{1,0:T(8,128)(2,1)} %shard_map.171.mine), channel_id=1, source_target_pairs={{0,4},{4,0},{1,5},{5,1},{2,6},{6,2},{3,7},{7,3},{8,12},{12,8},{9,1... | collective-permute-start | bytes 61448 | tf_op jit(solution)/shard_map/ppermute | solution.py:408
  247.8 0.8 copy-start.9
  249.4 1.0 copy-start.7
  250.3 0.9 copy-start.10
  254.1 0.6 copy-start.11
  254.8 0.6 copy-start.12
  255.4 0.6 copy-start.13
  256.0 3.8 %collective-permute-start.10 = (bf16[128,256]{1,0:T(8,128)(2,1)S(1)}, bf16[128,256]{1,0:T(8,128)(2,1)S(1)}, u32[]{:S(2)}, u32[]{:S(2)}) collective-permute-start(bf16[128,256]{1,0:T(8,128)(2,1)S(1)} %get-tuple-element.17), channel_id=1, source_target_pairs={{0,3},{1,0},{2,1},{3,2},{4,7},{5,4},{6,5},{7,6},{8,11},{9,8},{10,9... | collective-permute-start | bytes 196616 | tf_op jit(solution)/shard_map/ppermute | solution.py:408
  259.8 38.4 %copy-start.14 = (bf16[128,256]{1,0:T(8,128)(2,1)}, bf16[128,256]{1,0:T(8,128)(2,1)S(1)}, u32[]{:S(2)}) copy-start(bf16[128,256]{1,0:T(8,128)(2,1)S(1)} %collective-permute-done.10.refs_3_) | copy-start | bytes 196612
  259.8 14.1 %collective-permute-start.18 = (bf16[128,2048]{1,0:T(8,128)(2,1)}, bf16[128,2048]{1,0:T(8,128)(2,1)}, u32[]{:S(2)}, u32[]{:S(2)}) collective-permute-start(bf16[128,2048]{1,0:T(8,128)(2,1)} %constant_dynamic-slice_fusion), channel_id=1, source_target_pairs={{0,2},{1,3},{2,0},{3,1},{4,6},{5,7},{6,4},{7,5},{8,10},{9,11},{10,... | collective-permute-start | bytes 1572872 | tf_op jit(solution)/shard_map/ppermute | solution.py:408
  261.9 24.4 %collective-permute-start.19 = (bf16[128,2048]{1,0:T(8,128)(2,1)}, bf16[128,2048]{1,0:T(8,128)(2,1)}, u32[]{:S(2)}, u32[]{:S(2)}) collective-permute-start(bf16[128,2048]{1,0:T(8,128)(2,1)} %constant_dynamic-slice_fusion), channel_id=1, source_target_pairs={{0,3},{1,0},{2,1},{3,2},{4,7},{5,4},{6,5},{7,6},{8,11},{9,8},{10,9... | collective-permute-start | bytes 1572872 | tf_op jit(solution)/shard_map/ppermute | solution.py:408
  263.2 25.4 %collective-permute-start.15 = (bf16[3072,128]{1,0:T(8,128)(2,1)}, bf16[3072,128]{1,0:T(8,128)(2,1)S(1)}, u32[]{:S(2)}, u32[]{:S(2)}) collective-permute-start(bf16[3072,128]{1,0:T(8,128)(2,1)} %collective-permute-done.12.refs_1_), channel_id=1, source_target_pairs={{0,4},{4,0},{1,5},{5,1},{2,6},{6,2},{3,7},{7,3},{8,12},{12,8},{9,1... | collective-permute-start | bytes 2359304 | tf_op jit(solution)/shard_map/ppermute | solution.py:408
  265.3 23.7 %collective-permute-start.16 = (bf16[3072,128]{1,0:T(8,128)(2,1)}, bf16[3072,128]{1,0:T(8,128)(2,1)S(1)}, u32[]{:S(2)}, u32[]{:S(2)}) collective-permute-start(bf16[3072,128]{1,0:T(8,128)(2,1)} %collective-permute-done.13.refs_2_), channel_id=1, source_target_pairs={{0,4},{4,0},{1,5},{5,1},{2,6},{6,2},{3,7},{7,3},{8,12},{12,8},{9,1... | collective-permute-start | bytes 2359304 | tf_op jit(solution)/shard_map/ppermute | solution.py:408
  273.9 25.3 %collective-permute-start.20 = (bf16[128,2048]{1,0:T(8,128)(2,1)}, bf16[128,2048]{1,0:T(8,128)(2,1)}, u32[]{:S(2)}, u32[]{:S(2)}) collective-permute-start(bf16[128,2048]{1,0:T(8,128)(2,1)} %collective-permute-done.17.refs_7_), channel_id=1, source_target_pairs={{0,4},{4,0},{1,5},{5,1},{2,6},{6,2},{3,7},{7,3},{8,12},{12,8},{9,1... | collective-permute-start | bytes 1572872 | tf_op jit(solution)/shard_map/ppermute | solution.py:408
  286.3 12.9 %collective-permute-start.21 = (bf16[128,2048]{1,0:T(8,128)(2,1)}, bf16[128,2048]{1,0:T(8,128)(2,1)}, u32[]{:S(2)}, u32[]{:S(2)}) collective-permute-start(bf16[128,2048]{1,0:T(8,128)(2,1)} %collective-permute-done.18.refs_8_), channel_id=1, source_target_pairs={{0,4},{4,0},{1,5},{5,1},{2,6},{6,2},{3,7},{7,3},{8,12},{12,8},{9,1... | collective-permute-start | bytes 1572872 | tf_op jit(solution)/shard_map/ppermute | solution.py:408
  287.9 11.4 %collective-permute-start.22 = (bf16[128,2048]{1,0:T(8,128)(2,1)}, bf16[128,2048]{1,0:T(8,128)(2,1)}, u32[]{:S(2)}, u32[]{:S(2)}) collective-permute-start(bf16[128,2048]{1,0:T(8,128)(2,1)} %collective-permute-done.19.refs_9_), channel_id=1, source_target_pairs={{0,4},{4,0},{1,5},{5,1},{2,6},{6,2},{3,7},{7,3},{8,12},{12,8},{9,1... | collective-permute-start | bytes 1572872 | tf_op jit(solution)/shard_map/ppermute | solution.py:408
  288.6 10.6 %collective-permute-start.8 = (bf16[128,256]{1,0:T(8,128)(2,1)}, bf16[128,256]{1,0:T(8,128)(2,1)S(1)}, u32[]{:S(2)}, u32[]{:S(2)}) collective-permute-start(bf16[128,256]{1,0:T(8,128)(2,1)} %copy-done.13), channel_id=1, source_target_pairs={{0,1},{1,2},{2,3},{3,0},{4,5},{5,6},{6,7},{7,4},{8,9},{9,10},{10,1... | collective-permute-start | bytes 196616 | tf_op jit(solution)/shard_map/ppermute | solution.py:408
  288.9 10.2 %collective-permute-start.9 = (bf16[128,256]{1,0:T(8,128)(2,1)}, bf16[128,256]{1,0:T(8,128)(2,1)S(1)}, u32[]{:S(2)}, u32[]{:S(2)}) collective-permute-start(bf16[128,256]{1,0:T(8,128)(2,1)} %copy-done.12), channel_id=1, source_target_pairs={{0,2},{1,3},{2,0},{3,1},{4,6},{5,7},{6,4},{7,5},{8,10},{9,11},{10,... | collective-permute-start | bytes 196616 | tf_op jit(solution)/shard_map/ppermute | solution.py:408
  292.1 1.0 copy-start.5
  298.2 1.0 copy-start
  299.2 0.6 copy-start.15
  299.2 0.6 copy-start.16
where the time goes:
time: 307 us; the launch traced here: 306 us
  starting transfers between devices  117 us (38%)
  blocking collectives  107 us (35%)
  waiting for transfers between devices  38.7 us (13%)
  Pallas kernels  29.2 us (10%)
  local copies, waits for them, and re-layouts  12.1 us (4%)
    ppermute x23, starting transfers between devices, moved_by(): return lax.ppermute(array, axis, pairs)  108 us
    all_to_all x1, blocking collectives, per_device(): lax.all_to_all(outbound.reshape(experts, capacity * TILE, LANES), EP_TP,...  107 us
    ppermute x23, waiting for transfers between devices, moved_by(): return lax.ppermute(array, axis, pairs)  38.7 us
    all_to_all x1, starting transfers between devices, per_device(): lax.all_to_all(answers.reshape(experts, capacity * TILE, LANES), EP_TP, s...  9.53 us
    unnamed x41, local copies, waits for them, and re-layouts  9.38 us
    pallas_call x1, Pallas kernels, per_device(): call(expert_kernel, jax.ShapeDtypeStruct((tile_rows, LANES), BF16), [HBM]...  8.09 us
    pallas_call x1, Pallas kernels, per_device(): call(finish_kernel, tuple((jax.ShapeDtypeStruct((rows_dev, width), BF16)...  6.15 us
  transfers between devices with their start and end apart: 24, of which 11 were waited for; matrix products, arithmetic and copies ran while one was open for 1% of the time, Pallas kernels for 3%

commit v1 on v0

--- a/solution.py
+++ b/solution.py
@@ -36,7 +36,7 @@
         in_specs=in_specs,
         out_specs=out_specs,
         scratch_shapes=scratch,
-        compiler_params=pltpu.CompilerParams(vmem_limit_bytes=limit * MIB),
+        compiler_params=pltpu.CompilerParams(vmem_limit_bytes=int(limit * MIB)),
         cost_estimate=pl.CostEstimate(flops=flops, bytes_accessed=moved, transcendentals=0),
     )
 
@@ -83,11 +83,20 @@
     for copy in copies:
         copy.start()
     outbound[...] = jnp.zeros_like(outbound)
-    top = routes.shape[0] // x.shape[0]
+    top, number = routes.shape
     experts = used.shape[0]
     capacity = outbound.shape[0] // (experts * TILE)
     for e in range(experts):
         used[e] = 0
+
+    @pl.loop(0, number, unroll=8)
+    def _(n):
+        for k in range(top):
+            e = routes[k, n]
+            rank = used[e]
+            used[e] = rank + 1
+            places[k, n] = e * capacity + rank
+
     for copy in copies:
         copy.wait()
     source = x[...].astype(F32)
@@ -99,17 +108,12 @@
     for g, tile in enumerate(rows_to_tiles(swap_matrix(), rows)):
         tiles[g * TILE * TILE : (g + 1) * TILE * TILE, :] = tile
 
-    @pl.loop(0, x.shape[0], unroll=4)
+    @pl.loop(0, number, unroll=8)
     def _(n):
         row = tiles[pl.ds(pl.multiple_of(n * TILE, TILE), TILE), :]
         for k in range(top):
-            p = n * top + k
-            e = routes[p]
-            rank = used[e]
-            used[e] = rank + 1
-            place = e * capacity + rank
-            places[p] = place
-            outbound[pl.ds(pl.multiple_of(place * TILE, TILE), TILE), :] = row
+            at = pl.multiple_of(places[k, n] * TILE, TILE)
+            outbound[pl.ds(at, TILE), :] = row
 
     keep.wait()
 
@@ -216,7 +220,7 @@
 
 
 def state_kernel(k, v, log_decay, cosine, sine, packed):
-    heads = log_decay.shape[1]
+    heads = log_decay.shape[0]
     key_size = k.shape[1] // heads
     value_size = v.shape[1] // heads
     span = k.shape[0]
@@ -227,9 +231,9 @@
     after = jnp.zeros((1, heads), F32)
     tails = [None] * (span // BLOCK)
     for b in reversed(range(span // BLOCK)):
-        part = log_decay[b * BLOCK : (b + 1) * BLOCK, :]
-        tails[b] = summed_f32(above, part, ((0,), (0,))) + after
-        after = after + jnp.sum(part, axis=0, keepdims=True)
+        part = log_decay[:, b * BLOCK : (b + 1) * BLOCK]
+        tails[b] = summed_f32(above, part, ((0,), (1,))) + after
+        after = after + summed_f32(jnp.ones((1, BLOCK), F32), part, ((1,), (1,)))
     tail = jnp.concatenate(tails, axis=0)
     faded = (k_rot.astype(F32) * jnp.exp(spread_heads(tail, key_size))).astype(BF16)
     state = dot(faded.T, v[...])
@@ -247,9 +251,9 @@
         ).astype(BF16)
 
 
-def retention_kernel(seat, q, k, v, gate, log_decay, cosine, sine, state_in, *rest):
-    outs, gated = rest[:-1], rest[-1]
-    heads = log_decay.shape[1]
+def retention_kernel(seat, q, k, v, gate, log_decay, cosine, sine, state_in, w_out, *rest):
+    own, *outs, gated = rest
+    heads = log_decay.shape[0]
     key_size = q.shape[1] // heads
     value_size = v.shape[1] // heads
     span = q.shape[0]
@@ -263,9 +267,9 @@
     state = state_in[...]
     for b in range(span // BLOCK):
         at = slice(b * BLOCK, (b + 1) * BLOCK)
-        part = log_decay[at, :]
-        column = summed_f32(ones, part, ((1,), (0,)))
-        across = summed_f32(part, ones, ((0,), (1,)))
+        part = log_decay[:, at]
+        column = summed_f32(ones, part, ((1,), (1,)))
+        across = summed_f32(part, ones, ((1,), (1,)))
         total = column[BLOCK - 1 : BLOCK, :]
         q_part = q_rot[at, :]
         k_part = k_rot[at, :]
@@ -298,76 +302,104 @@
                 + grown[h * key_size : (h + 1) * key_size, columns]
             )
         state = jnp.concatenate(fade, axis=0)
-    count = len(outs)
+    count = len(outs) + 1
     share = span // count
     for d in range(count):
         first = lax.rem(seat[0] + d, count) * share
-        outs[d][...] = gated[pl.ds(pl.multiple_of(first, share), share), :]
-
-
-def pack_kernel(core, gate_w, up_w, down_w, out):
-    half = gate_w.shape[0] // 2
-    first = pl.multiple_of(core[0] * half, TILE)
-    out[0:half, :] = gate_w[pl.ds(first, half), :]
-    out[half : 2 * half, :] = up_w[pl.ds(first, half), :]
-    part = down_w.shape[0] // 2
-    first = pl.multiple_of(core[0] * part, TILE)
-    for k in range(down_w.shape[1] // LANES):
-        at = 2 * half + k * part
-        out[at : at + part, :] = down_w[pl.ds(first, part), k * LANES : (k + 1) * LANES]
-
-
-def shared_kernel(core, normed, gate_w, up_w, down_w, *refs):
-    count = (len(refs) - 3) // 2
-    mine, theirs = refs[:count], refs[count : 2 * count]
-    out, packed, down = refs[2 * count :]
+        part = gated[pl.ds(pl.multiple_of(first, share), share), :]
+        if d == 0:
+            own[...] = dot(part, w_out[...]).astype(BF16)
+        else:
+            outs[d - 1][...] = part
+
+
+def pack_kernel(core, gate_w, up_w, down_w, w_out, whole, half, out_half):
+    def fill(to, first, depth, cut, thin):
+        to[0:depth, :] = gate_w[pl.ds(first, depth), :]
+        to[depth : 2 * depth, :] = up_w[pl.ds(first, depth), :]
+        for k in range(down_w.shape[1] // LANES):
+            at = 2 * depth + k * thin
+            to[at : at + thin, :] = down_w[pl.ds(cut, thin), k * LANES : (k + 1) * LANES]
+
+    depth, thin = gate_w.shape[0], down_w.shape[0]
+    fill(whole, 0, depth, 0, thin)
+    at = pl.multiple_of(core[0] * (depth // 2), TILE)
+    cut = pl.multiple_of(core[0] * (thin // 2), TILE)
+    fill(half, at, depth // 2, cut, thin // 2)
+    share = out_half.shape[0]
+    out_half[...] = w_out[pl.ds(pl.multiple_of(core[0] * share, TILE), share), :]
+
+
+def shared_kernel(core, normed, own, near, near_other, mine, theirs, out, packed, down):
     rows = normed[...]
-    half = rows.shape[1] // 2
-    part = down.shape[0] // 2
-    hidden = jax.nn.silu(dot(rows, gate_w[...])) * dot(rows, up_w[...])
-    total = dot(hidden.astype(BF16), down_w[...])
-    for a, b in zip(mine, theirs):
-        packed[0] = jnp.where(core[0] == 0, a[...], b[...])
-        packed[1] = jnp.where(core[0] == 0, b[...], a[...])
-        gated = dot(rows[:, :half], packed[0, :half]) + dot(rows[:, half:], packed[1, :half])
-        up = dot(rows[:, :half], packed[0, half : 2 * half]) + dot(
-            rows[:, half:], packed[1, half : 2 * half]
-        )
-        for c in range(2):
-            for k in range(down.shape[1] // LANES):
-                at = 2 * half + k * part
-                down[c * part : (c + 1) * part, k * LANES : (k + 1) * LANES] = packed[
-                    c, at : at + part
-                ]
-        hidden = (jax.nn.silu(gated) * up).astype(BF16)
-        total = total + dot(hidden, down[...])
-    out[...] = total
-
-
-def finish_kernel(places, core, weight, *refs):
-    count = (len(refs) - 11) // 3
-    gated = refs[:count]
-    hbm = refs[count : 3 * count + 1]
-    mixer_out, moe_out, picked, rows, returned, shared, own, mine, theirs, sems = refs[
-        3 * count + 1 :
-    ]
-    places_of = [returned, shared, own]
-    places_of += [mine.at[d] for d in range(count - 1)] + [theirs.at[d] for d in range(count - 1)]
-    copies = [
-        pltpu.make_async_copy(a, b, sems.at[i]) for i, (a, b) in enumerate(zip(hbm, places_of))
-    ]
+    depth = rows.shape[1]
+    total = None
+    for part in (own, near, near_other):
+        hidden = jax.nn.silu(dot(rows, part[0:depth, :])) * dot(rows, part[depth : 2 * depth, :])
+        thin = down.shape[0]
+        for k in range(down.shape[1] // LANES):
+            at = 2 * depth + k * thin
+            down[:, k * LANES : (k + 1) * LANES] = part[at : at + thin, :]
+        product = dot(hidden.astype(BF16), down[...])
+        total = product if total is None else total + product
+    packed[0] = jnp.where(core[0] == 0, mine[...], theirs[...])
+    packed[1] = jnp.where(core[0] == 0, theirs[...], mine[...])
+    half = depth // 2
+    thin = down.shape[0] // 2
+    gated = dot(rows[:, :half], packed[0, :half]) + dot(rows[:, half:], packed[1, :half])
+    up = dot(rows[:, :half], packed[0, half:depth]) + dot(rows[:, half:], packed[1, half:depth])
+    for c in range(2):
+        for k in range(down.shape[1] // LANES):
+            at = depth + k * thin
+            down[c * thin : (c + 1) * thin, k * LANES : (k + 1) * LANES] = packed[c, at : at + thin]
+    hidden = (jax.nn.silu(gated) * up).astype(BF16)
+    out[...] = total + dot(hidden, down[...])
+
+
+def finish_kernel(
+    places,
+    core,
+    returned,
+    weight,
+    own,
+    gated_left,
+    gated_right,
+    gated_far,
+    shared_hbm,
+    near_hbm,
+    other_hbm,
+    mine_hbm,
+    theirs_hbm,
+    mixer_out,
+    moe_out,
+    picked,
+    rows,
+    shared,
+    near,
+    other,
+    far,
+    sems,
+):
+    share = far.shape[1]
+    pairs = (
+        (shared_hbm, shared),
+        (near_hbm, near),
+        (other_hbm, other),
+        (mine_hbm, far.at[0]),
+        (theirs_hbm, far.at[1]),
+    )
+    copies = [pltpu.make_async_copy(a, b, sems.at[i]) for i, (a, b) in enumerate(pairs)]
     for copy in copies:
         copy.start()
     swap = swap_matrix()
     side = TILE * TILE
     number = moe_out.shape[0]
     top = weight.shape[1]
-    copies[0].wait()
-
-    @pl.loop(0, number, unroll=4)
+
+    @pl.loop(0, number, unroll=8)
     def _(n):
         for k in range(top):
-            place = places[n * top + k]
+            place = places[k, n]
             picked[k, pl.ds(pl.multiple_of(n * TILE, TILE), TILE), :] = returned[
                 pl.ds(pl.multiple_of(place * TILE, TILE), TILE), :
             ]
@@ -385,18 +417,20 @@
                         (at + j) * TILE : (at + j + 1) * TILE,
                         c * LANES : (c + 1) * LANES,
                     ] = turned[c * TILE : (c + 1) * TILE, j * LANES : (j + 1) * LANES]
-    for copy in copies[1:]:
+    for copy in copies:
         copy.wait()
     total = shared[...]
     for k in range(top):
         total = total + rows[k].astype(F32) * weight[:, k : k + 1]
     moe_out[...] = total.astype(BF16)
-    mixed = dot(gated[0][...], own[...])
-    half = own.shape[0] // 2
-    for d in range(count - 1):
-        low, high = gated[d + 1][:, :half], gated[d + 1][:, half:]
-        mixed = mixed + dot(jnp.where(core[0] == 0, low, high), mine[d])
-        mixed = mixed + dot(jnp.where(core[0] == 0, high, low), theirs[d])
+    first = core[0] == 0
+    left, right, across = gated_left[...], gated_right[...], gated_far[...]
+    mixed = own[...].astype(F32)
+    mixed = mixed + dot(jnp.where(first, left, right), near[...])
+    mixed = mixed + dot(jnp.where(first, right, left), other[...])
+    low, high = across[:, :share], across[:, share:]
+    mixed = mixed + dot(jnp.where(first, low, high), far[0])
+    mixed = mixed + dot(jnp.where(first, high, low), far[1])
     mixer_out[...] = mixed.astype(BF16)
 
 
@@ -406,6 +440,13 @@
         (s, (s + step) % count) for s in range(count) if around or 0 <= s + step < count
     ]
     return lax.ppermute(array, axis, pairs)
+
+
+def outward(array):
+    count = lax.axis_size("tp")
+    pairs = [(s, (s + 1) % count) for s in range(count)]
+    pairs += [(count + s, count + (s - 1) % count) for s in range(count)]
+    return lax.ppermute(array, ("ep_1", "tp"), pairs)
 
 
 def opened(packed):
@@ -499,15 +540,14 @@
     half_out = w_out.shape[0] // 2
     packed_shape = jax.ShapeDtypeStruct((STATE_ROWS, value_size), BF16)
 
-    out_half = lax.dynamic_slice_in_dim(w_out, core[0] * half_out, half_out, 0)
-    out_mine = [moved_by(out_half, "tp", d) for d in around]
+    out_near = outward(w_out)
 
     normed, outbound, places = call(
         prep_kernel,
         (
             jax.ShapeDtypeStruct((rows_dev, width), BF16),
             jax.ShapeDtypeStruct((tile_rows, LANES), BF16),
-            jax.ShapeDtypeStruct((rows_dev * top,), jnp.int32),
+            jax.ShapeDtypeStruct((top, rows_dev), jnp.int32),
         ),
         [SMEM, HBM, HBM],
         (HBM, VMEM, SMEM),
@@ -522,7 +562,7 @@
         2 * rows_dev * width * 256,
         4 * rows_dev * width,
         62,
-    )(routes.reshape(-1), moe_input, moe_gain.reshape(1, width))
+    )(routes.T, moe_input, moe_gain.reshape(1, width))
 
     arrived = lax.all_to_all(
         outbound.reshape(experts, capacity * TILE, LANES),
@@ -548,7 +588,7 @@
         2 * span * LANES * 512,
         4 * span * LANES * 4,
         12,
-    )(keys, values, log_decay, cosine, sine)
+    )(keys, values, log_decay.T, cosine, sine)
     other = moved_by(own, "ep_1", 1)
     chip = small(chip_kernel, packed_shape, [SMEM, VMEM, VMEM], VMEM)(core, own, other)
     near = [moved_by(chip, "ep_0", d, False) for d in (3, 2, 1)]
@@ -565,23 +605,31 @@
         VMEM,
     )(core, prefix, swapped, other)
 
-    shared_half = call(
+    pack_rows = width * 3 * shared_size // LANES
+    shared_own, shared_half, out_half = call(
         pack_kernel,
-        jax.ShapeDtypeStruct((width * 3 * shared_size // 2 // LANES, LANES), BF16),
-        [SMEM] + [VMEM] * 3,
-        VMEM,
+        (
+            jax.ShapeDtypeStruct((pack_rows, LANES), BF16),
+            jax.ShapeDtypeStruct((pack_rows // 2, LANES), BF16),
+            jax.ShapeDtypeStruct((half_out, width), BF16),
+        ),
+        [SMEM] + [VMEM] * 4,
+        (VMEM,) * 3,
         [],
         100000,
         6 * width * shared_size,
-        8,
-    )(core, shared_gate, shared_up, shared_down)
-    shared_mine = [moved_by(shared_half, "tp", d) for d in around]
-    shared_theirs = [moved_by(part, "ep_1", 1) for part in shared_mine]
-    out_theirs = [moved_by(part, "ep_1", 1) for part in out_mine]
+        16,
+    )(core, shared_gate, shared_up, shared_down, w_out)
+    shared_near = outward(shared_own)
+    shared_mine = moved_by(shared_half, "tp", 2)
+    out_mine = moved_by(out_half, "tp", 2)
+    shared_other, shared_theirs, out_other, out_theirs = [
+        moved_by(part, "ep_1", 1) for part in (shared_near, shared_mine, out_near, out_mine)
+    ]
     shared_sum = call(
         shared_kernel,
         jax.ShapeDtypeStruct((rows_dev, width), F32),
-        [SMEM] + [VMEM] * (4 + 2 * (n_tp - 1)),
+        [SMEM] + [VMEM] * 6,
         VMEM,
         [
             pltpu.VMEM((2,) + shared_half.shape, BF16),
@@ -590,7 +638,7 @@
         2 * n_tp * rows_dev * width * shared_size * 3,
         10 * rows_dev * width * 2,
         20,
-    )(core, normed, shared_gate, shared_up, shared_down, *shared_mine, *shared_theirs)
+    )(core, normed, shared_own, shared_near, shared_other, shared_mine, shared_theirs)
 
     pieces, chunks = 4, 3
     answers = call(
@@ -611,7 +659,7 @@
         ],
         2 * slots * width * hidden_size * 3,
         3 * 2 * width * hidden_size,
-        61,
+        62,
     )(arrived.reshape(tile_rows, LANES), expert_gate, expert_up, expert_down)
     returned = lax.all_to_all(
         answers.reshape(experts, capacity * TILE, LANES),
@@ -621,46 +669,50 @@
         tiled=True,
     )
 
-    gated = call(
+    gated_shape = jax.ShapeDtypeStruct((rows_dev, heads * value_size), BF16)
+    own_mixed, *gated = call(
         retention_kernel,
-        tuple(jax.ShapeDtypeStruct((rows_dev, heads * value_size), BF16) for _ in range(n_tp)),
-        [SMEM] + [VMEM] * 8,
+        (jax.ShapeDtypeStruct((rows_dev, width), BF16),) + (gated_shape,) * (n_tp - 1),
+        [SMEM] + [VMEM] * 9,
         (VMEM,) * n_tp,
         [pltpu.VMEM((span, heads * value_size), BF16)],
         2 * span * heads * value_size * 1000,
         10 * rows_dev * width * 2,
         20,
-    )(seat, queries, keys, values, gate, log_decay, cosine, sine, state_in)
-    gated = [gated[0]] + [moved_by(gated[d], "tp", d) for d in around]
+    )(seat, queries, keys, values, gate, log_decay.T, cosine, sine, state_in, w_out)
+    gated_left, gated_far, gated_right = [moved_by(gated[d - 1], "tp", d) for d in around]
 
     return call(
         finish_kernel,
         tuple(jax.ShapeDtypeStruct((rows_dev, width), BF16) for _ in range(2)),
-        [SMEM, SMEM, VMEM] + [VMEM] * n_tp + [HBM] * (2 * n_tp + 1),
+        [SMEM, SMEM] + [VMEM] * 6 + [HBM] * 5,
         (VMEM,) * 2,
         [
             pltpu.VMEM((top, rows_dev * TILE, LANES), BF16),
             pltpu.VMEM((top, rows_dev, width), BF16),
-            pltpu.VMEM((tile_rows, LANES), BF16),
             pltpu.VMEM((rows_dev, width), F32),
             pltpu.VMEM((2 * half_out, width), BF16),
-            pltpu.VMEM((n_tp - 1, half_out, width), BF16),
-            pltpu.VMEM((n_tp - 1, half_out, width), BF16),
-            pltpu.SemaphoreType.DMA((2 * n_tp + 1,)),
+            pltpu.VMEM((2 * half_out, width), BF16),
+            pltpu.VMEM((2, half_out, width), BF16),
+            pltpu.SemaphoreType.DMA((5,)),
         ],
         2 * rows_dev * width * 1500,
         10 * rows_dev * width * 2,
-        61,
+        28,
     )(
         places,
         core,
+        returned.reshape(tile_rows, LANES),
         route_weight,
-        *gated,
-        returned.reshape(tile_rows, LANES),
+        own_mixed,
+        gated_left,
+        gated_right,
+        gated_far,
         shared_sum,
-        w_out,
-        *out_mine,
-        *out_theirs,
+        out_near,
+        out_other,
+        out_mine,
+        out_theirs,
     )
 
 

time: 307 us -> 288 us (0.938)
  starting transfers between devices: 117 us -> 68.6 us
  waiting for transfers between devices: 38.7 us -> 73.4 us
  local copies, waits for them, and re-layouts: 12.1 us -> 8.33 us
    ppermute x0 -> x2, waiting for transfers between devices: none -> 65.8 us  [outward(): return lax.ppermute(array, ('ep_1', 'tp'), pairs)]
    ppermute x23 -> x17, starting transfers between devices: 108 us -> 56 us  [moved_by(): return lax.ppermute(array, axis, pairs)]
    ppermute x23 -> x17, waiting for transfers between devices: 38.7 us -> 7.55 us  [moved_by(): return lax.ppermute(array, axis, pairs)]
    ppermute x0 -> x2, starting transfers between devices: none -> 3.14 us  [outward(): return lax.ppermute(array, ('ep_1', 'tp'), pairs)]
    unnamed x41 -> x39, local copies, waits for them, and re-layouts: 9.38 us -> 8.24 us
  transfers between devices with their start and end apart: 24 -> 20, of which waited for: 11 -> 10; matrix products, arithmetic and copies ran while one was open for 1% -> 1% of each run, Pallas kernels for 3% -> 4%
where the time goes in v1:
time: 288 us
  blocking collectives  107 us (37%)
  waiting for transfers between devices  73.4 us (25%)
  starting transfers between devices  68.6 us (24%)
  Pallas kernels  28.4 us (10%)
  local copies, waits for them, and re-layouts  8.33 us (3%)
    all_to_all x1, blocking collectives, per_device(): lax.all_to_all(outbound.reshape(experts, capacity * TILE, LANES), EP_TP,...  107 us
    ppermute x2, waiting for transfers between devices, outward(): return lax.ppermute(array, ('ep_1', 'tp'), pairs)  65.8 us
    ppermute x17, starting transfers between devices, moved_by(): return lax.ppermute(array, axis, pairs)  56 us
    all_to_all x1, starting transfers between devices, per_device(): lax.all_to_all(answers.reshape(experts, capacity * TILE, LANES), EP_TP, s...  9.48 us
    unnamed x39, local copies, waits for them, and re-layouts  8.24 us
    pallas_call x1, Pallas kernels, per_device(): call(expert_kernel, jax.ShapeDtypeStruct((tile_rows, LANES), BF16), [HBM]...  8.1 us
    ppermute x17, waiting for transfers between devices, moved_by(): return lax.ppermute(array, axis, pairs)  7.55 us
  transfers between devices with their start and end apart: 20, of which 10 were waited for; matrix products, arithmetic and copies ran while one was open for 1% of the time, Pallas kernels for 4%

profile of v1, /device:TPU:33, one launch (start us, length us, event | category | flops | bytes accessed | tf_op | source)
XLA Modules:
  0.0 287.8 jit_solution(10135999460539685482)
XLA Ops:
  0.6 4.6 %shard_map.167 = (bf16[128,2048]{1,0:T(8,128)(2,1)}, bf16[6144,128]{1,0:T(8,128)(2,1)}, s32[2,128]{1,0:T(2,128)}) custom-call(s32[2,128]{1,0:T(2,128)} %bitcast.16, bf16[128,2048]{1,0:T(8,128)(2,1)} %x_hbm.1, f32[1,2048]{1,0:T(1,128)} %bitcast.15), custom_call_target="tpu_custom_call" | custom-call | flops 134217728 | bytes 1048576 | tf_op jit(solution)/shard_map/pallas_call | solution.py:545
  5.3 107.0 %all_to_all.10 = bf16[128,48,128]{2,1,0:T(8,128)(2,1)} all-to-all(bf16[128,48,128]{2,1,0:T(8,128)(2,1)} %bitcast.14), channel_id=1, replica_groups=mesh['grp'=2,'ep_0'=16,'ep_1'=2,'tp'=4] {'ep_0','ep_1','tp'}, dimensions={0} | all-to-all | bytes 3145728 | tf_op jit(solution)/shard_map/all_to_all | solution.py:567
  112.3 8.1 %shard_map.168 = bf16[6144,128]{1,0:T(8,128)(2,1)} custom-call(bf16[6144,128]{1,0:T(8,128)(2,1)} %bitcast.13, bf16[1,2048,512]{2,1,0:T(8,128)(2,1)} %gate_hbm.1, bf16[1,2048,512]{2,1,0:T(8,128)(2,1)} %up_hbm.1, bf16[1,512,2048]{2,1,0:T(8,128)(2,1)} %down_hbm.1), custom_call_target="tpu_custom_call" | custom-call | flops 2415919104 | bytes 6291456 | tf_op jit(solution)/shard_map/pallas_call | solution.py:644
  120.4 9.5 %all-to-all-start.1 = ((bf16[128,48,128]{2,1,0:T(8,128)(2,1)}), bf16[128,48,128]{2,1,0:T(8,128)(2,1)S(1)}, u32[]{:S(2)}, u32[]{:S(2)}) async-start(bf16[128,48,128]{2,1,0:T(8,128)(2,1)} %bitcast.12), calls=%async_computation.1 | async-start | bytes 3145728 | tf_op jit(solution)/shard_map/all_to_all | solution.py:664
  129.9 1.0 copy-done.8
  131.0 1.0 copy-done.9
  132.0 1.1 shard_map.175
  133.1 2.6 collective-permute-start.11
  135.7 1.2 copy-done.1
  136.8 0.6 collective-permute-start.15
  137.4 0.1 collective-permute-start.13
  137.5 31.9 %collective-permute-done.11.near = bf16[6144,128]{1,0:T(8,128)(2,1)} collective-permute-done((bf16[6144,128]{1,0:T(8,128)(2,1)S(1)}, bf16[6144,128]{1,0:T(8,128)(2,1)}, u32[]{:S(2)}, u32[]{:S(2)}) %collective-permute-start.11) | collective-permute-done | bytes 1572896 | tf_op jit(solution)/shard_map/ppermute | solution.py:449
  169.4 3.6 %collective-permute-start.12 = (bf16[6144,128]{1,0:T(8,128)(2,1)}, bf16[6144,128]{1,0:T(8,128)(2,1)}, u32[]{:S(2)}, u32[]{:S(2)}) collective-permute-start(bf16[6144,128]{1,0:T(8,128)(2,1)} %collective-permute-done.11.near), channel_id=1, source_target_pairs={{0,4},{4,0},{1,5},{5,1},{2,6},{6,2},{3,7},{7,3},{8,12},{12,8},{9,1... | collective-permute-start | bytes 4718600 | tf_op jit(solution)/shard_map/ppermute | solution.py:442
  173.1 33.9 %collective-permute-done.15.near_hbm = bf16[256,2048]{1,0:T(8,128)(2,1)} collective-permute-done((bf16[256,2048]{1,0:T(8,128)(2,1)S(1)}, bf16[256,2048]{1,0:T(8,128)(2,1)}, u32[]{:S(2)}, u32[]{:S(2)}) %collective-permute-start.15) | collective-permute-done | bytes 1048608 | tf_op jit(solution)/shard_map/ppermute | solution.py:449
  207.0 4.1 %collective-permute-start.16 = (bf16[256,2048]{1,0:T(8,128)(2,1)}, bf16[256,2048]{1,0:T(8,128)(2,1)}, u32[]{:S(2)}, u32[]{:S(2)}) collective-permute-start(bf16[256,2048]{1,0:T(8,128)(2,1)} %collective-permute-done.15.near_hbm), channel_id=1, source_target_pairs={{0,4},{4,0},{1,5},{5,1},{2,6},{6,2},{3,7},{7,3},{8,12},{12,8},{9,1... | collective-permute-start | bytes 3145736 | tf_op jit(solution)/shard_map/ppermute | solution.py:442
  211.2 0.6 collective-permute-start.18
  211.8 1.0 multiply_sine_fusion
  212.8 0.8 shard_map.169.own
  213.7 0.2 collective-permute-start
  213.8 1.8 collective-permute-done.other
  215.6 0.6 copy-done.13
  216.2 3.1 %collective-permute-start.1 = (bf16[80,128]{1,0:T(8,128)(2,1)S(1)}, bf16[80,128]{1,0:T(8,128)(2,1)S(1)}, u32[]{:S(2)}, u32[]{:S(2)}) collective-permute-start(bf16[80,128]{1,0:T(8,128)(2,1)S(1)} %shard_map.170.chip), channel_id=1, source_target_pairs={{0,24},{8,32},{16,40},{24,48},{32,56},{40,64},{48,72},{56,80},{64,... | collective-permute-start | bytes 61448 | tf_op jit(solution)/shard_map/ppermute | solution.py:442
  219.3 0.9 collective-permute-done.1.far3
  220.2 5.2 %collective-permute-start.2 = (bf16[80,128]{1,0:T(8,128)(2,1)S(1)}, bf16[80,128]{1,0:T(8,128)(2,1)S(1)}, u32[]{:S(2)}, u32[]{:S(2)}) collective-permute-start(bf16[80,128]{1,0:T(8,128)(2,1)S(1)} %shard_map.170.chip), channel_id=1, source_target_pairs={{0,16},{8,24},{16,32},{24,40},{32,48},{40,56},{48,64},{56,72},{64,... | collective-permute-start | bytes 61448 | tf_op jit(solution)/shard_map/ppermute | solution.py:442
  225.4 0.9 collective-permute-done.2.far2
  226.3 3.0 %collective-permute-start.3 = (bf16[80,128]{1,0:T(8,128)(2,1)S(1)}, bf16[80,128]{1,0:T(8,128)(2,1)S(1)}, u32[]{:S(2)}, u32[]{:S(2)}) collective-permute-start(bf16[80,128]{1,0:T(8,128)(2,1)S(1)} %shard_map.170.chip), channel_id=1, source_target_pairs={{0,8},{8,16},{16,24},{24,32},{32,40},{40,48},{48,56},{56,64},{64,7... | collective-permute-start | bytes 61448 | tf_op jit(solution)/shard_map/ppermute | solution.py:442
  229.3 0.9 collective-permute-done.3.far1
  230.2 11.8 %collective-permute-start.4 = (bf16[80,128]{1,0:T(8,128)(2,1)S(1)}, bf16[80,128]{1,0:T(8,128)(2,1)S(1)}, u32[]{:S(2)}, u32[]{:S(2)}) collective-permute-start(bf16[80,128]{1,0:T(8,128)(2,1)S(1)} %get-tuple-element.17), channel_id=1, source_target_pairs={{0,96},{8,104},{16,112},{24,120},{1,97},{9,105},{17,113},{25,121},... | collective-permute-start | bytes 61448 | tf_op jit(solution)/shard_map/ppermute | solution.py:442
  242.0 0.9 collective-permute-done.4.far12
  242.9 4.1 %collective-permute-start.5 = (bf16[80,128]{1,0:T(8,128)(2,1)S(1)}, bf16[80,128]{1,0:T(8,128)(2,1)S(1)}, u32[]{:S(2)}, u32[]{:S(2)}) collective-permute-start(bf16[80,128]{1,0:T(8,128)(2,1)S(1)} %get-tuple-element.17), channel_id=1, source_target_pairs={{0,64},{8,72},{16,80},{24,88},{32,96},{40,104},{48,112},{56,120},{... | collective-permute-start | bytes 61448 | tf_op jit(solution)/shard_map/ppermute | solution.py:442
  246.9 0.9 collective-permute-done.5.far8
  247.8 10.5 %collective-permute-start.6 = (bf16[80,128]{1,0:T(8,128)(2,1)S(1)}, bf16[80,128]{1,0:T(8,128)(2,1)S(1)}, u32[]{:S(2)}, u32[]{:S(2)}) collective-permute-start(bf16[80,128]{1,0:T(8,128)(2,1)S(1)} %get-tuple-element.17), channel_id=1, source_target_pairs={{0,32},{8,40},{16,48},{24,56},{32,64},{40,72},{48,80},{56,88},{64,... | collective-permute-start | bytes 61448 | tf_op jit(solution)/shard_map/ppermute | solution.py:442
  258.3 0.9 collective-permute-done.6.far4
  259.2 0.6 shard_map.172.mine
  259.9 6.6 %collective-permute-start.7 = (bf16[80,128]{1,0:T(8,128)(2,1)}, bf16[80,128]{1,0:T(8,128)(2,1)}, u32[]{:S(2)}, u32[]{:S(2)}) collective-permute-start(bf16[80,128]{1,0:T(8,128)(2,1)} %shard_map.172.mine), channel_id=1, source_target_pairs={{0,4},{4,0},{1,5},{5,1},{2,6},{6,2},{3,7},{7,3},{8,12},{12,8},{9,1... | collective-permute-start | bytes 61448 | tf_op jit(solution)/shard_map/ppermute | solution.py:442
  266.4 0.7 copy.18.weight
  267.2 0.4 collective-permute-done.7.theirs
  267.6 1.0 copy-done.14
  268.6 0.8 shard_map.173.state_in
  269.4 0.9 copy-done.12
  270.3 0.9 copy-done.15
  271.2 3.1 %shard_map.174 = (bf16[128,2048]{1,0:T(8,128)(2,1)S(1)}, bf16[128,256]{1,0:T(8,128)(2,1)S(1)}, bf16[128,256]{1,0:T(8,128)(2,1)S(1)}, bf16[128,256]{1,0:T(8,128)(2,1)S(1)}) custom-call(s32[1]{0:T(128)} %bitcast.7.seat, bf16[512,128]{1,0:T(8,128)(2,1)S(1)} %copy-done.15, bf16[512,128]{1,0:T(8,128)(2,1)S(1)} %copy-done.10, bf16[512,256]{1,0:T(8,128)(2,1)S(1)} %copy-done.3, ...), custom_call_target="tpu_custom_call" | custom-call | flops 262144000 | bytes 5242880 | tf_op jit(solution)/shard_map/pallas_call | solution.py:673
  274.4 0.8 copy-done.5
  275.1 0.5 collective-permute-start.10
  275.7 1.7 collective-permute-start.8
  277.3 1.0 collective-permute-start.9
  278.4 4.8 %shard_map.176.shared_hbm = f32[128,2048]{1,0:T(8,128)S(1)} custom-call(s32[1]{0:T(128)} %bitcast.2.core, bf16[128,2048]{1,0:T(8,128)(2,1)S(1)} %copy-done.4, bf16[6144,128]{1,0:T(8,128)(2,1)S(1)} %copy-done.2, bf16[6144,128]{1,0:T(8,128)(2,1)} %collective-permute-done.11.near, bf16[6144,128]{1,0:T(8,128)(2,1)} %collective-permute-done.12.near_other, ...), custom_call_target="tpu_custom_call" | custom-call | flops 805306368 | bytes 5242880 | tf_op jit(solution)/shard_map/pallas_call | solution.py:629
  283.3 4.3 %shard_map.177 = (bf16[128,2048]{1,0:T(8,128)(2,1)}, bf16[128,2048]{1,0:T(8,128)(2,1)}) custom-call(s32[2,128]{1,0:T(2,128)S(1)} %copy-done.17, s32[1]{0:T(128)} %bitcast.2.core, bf16[6144,128]{1,0:T(8,128)(2,1)S(1)} %bitcast.9, f32[128,2]{1,0:T(8,128)S(1)} %copy-done.11, bf16[128,2048]{1,0:T(8,128)(2,1)S(1)} %copy-done.6, ...), custom_call_target="tpu_custom_call" | custom-call | flops 786432000 | bytes 5242880 | tf_op jit(solution)/shard_map/pallas_call | solution.py:685
  (48 shorter events, 0.3 us)
Async XLA Ops:
  120.4 9.5 %copy-start = (bf16[256,2048]{1,0:T(8,128)(2,1)S(1)}, bf16[256,2048]{1,0:T(8,128)(2,1)}, u32[]{:S(2)}) copy-start(bf16[256,2048]{1,0:T(8,128)(2,1)} %w_out.3) | copy-start | bytes 3145732
  120.4 9.5 %copy-start.7 = (bf16[2048,128]{1,0:T(8,128)(2,1)S(1)}, bf16[2048,128]{1,0:T(8,128)(2,1)}, u32[]{:S(2)}) copy-start(bf16[2048,128]{1,0:T(8,128)(2,1)} %gate_w.1) | copy-start | bytes 1572868
  120.4 162.9 %all-to-all-start.1 = ((bf16[128,48,128]{2,1,0:T(8,128)(2,1)}), bf16[128,48,128]{2,1,0:T(8,128)(2,1)S(1)}, u32[]{:S(2)}, u32[]{:S(2)}) async-start(bf16[128,48,128]{2,1,0:T(8,128)(2,1)} %bitcast.12), calls=%async_computation.1 | async-start | bytes 3145728 | tf_op jit(solution)/shard_map/all_to_all | solution.py:664
  129.9 1.0 copy-start.8
  131.0 1.0 copy-start.9
  132.0 80.8 %copy-start.3 = (bf16[512,256]{1,0:T(8,128)(2,1)S(1)}, bf16[512,256]{1,0:T(8,128)(2,1)}, u32[]{:S(2)}) copy-start(bf16[512,256]{1,0:T(8,128)(2,1)} %v.3) | copy-start | bytes 786436
  132.0 80.8 %copy-start.10 = (bf16[512,128]{1,0:T(8,128)(2,1)S(1)}, bf16[512,128]{1,0:T(8,128)(2,1)}, u32[]{:S(2)}) copy-start(bf16[512,128]{1,0:T(8,128)(2,1)} %k.3) | copy-start | bytes 393220
  132.0 80.8 %copy-start.16 = (f32[512,2]{0,1:T(2,128)S(1)}, f32[512,2]{0,1:T(2,128)}, u32[]{:S(2)}) copy-start(f32[512,2]{0,1:T(2,128)} %param.20) | copy-start | bytes 12292
  132.0 134.4 %copy-start.18 = (f32[128,2]{0,1:T(2,128)S(1)}, f32[128,2]{0,1:T(2,128)}, u32[]{:S(2)}) copy-start(f32[128,2]{0,1:T(2,128)} %param.25) | copy-start | bytes 3076
  133.1 36.4 %collective-permute-start.11 = (bf16[6144,128]{1,0:T(8,128)(2,1)S(1)}, bf16[6144,128]{1,0:T(8,128)(2,1)}, u32[]{:S(2)}, u32[]{:S(2)}) collective-permute-start(bf16[6144,128]{1,0:T(8,128)(2,1)S(1)} %get-tuple-element.23.own), channel_id=1, source_target_pairs={{0,1},{1,2},{2,3},{3,0},{4,7},{5,4},{6,5},{7,6},{8,9},{9,10},{10,1... | collective-permute-start | bytes 4718600 | tf_op jit(solution)/shard_map/ppermute | solution.py:449
  135.7 1.2 copy-start.1
  136.8 70.1 %collective-permute-start.15 = (bf16[256,2048]{1,0:T(8,128)(2,1)S(1)}, bf16[256,2048]{1,0:T(8,128)(2,1)}, u32[]{:S(2)}, u32[]{:S(2)}) collective-permute-start(bf16[256,2048]{1,0:T(8,128)(2,1)S(1)} %copy-done), channel_id=1, source_target_pairs={{0,1},{1,2},{2,3},{3,0},{4,7},{5,4},{6,5},{7,6},{8,9},{9,10},{10,1... | collective-permute-start | bytes 3145736 | tf_op jit(solution)/shard_map/ppermute | solution.py:449
  137.4 73.7 %collective-permute-start.13 = (bf16[3072,128]{1,0:T(8,128)(2,1)S(1)}, bf16[3072,128]{1,0:T(8,128)(2,1)}, u32[]{:S(2)}, u32[]{:S(2)}) collective-permute-start(bf16[3072,128]{1,0:T(8,128)(2,1)S(1)} %get-tuple-element.24), channel_id=1, source_target_pairs={{0,2},{1,3},{2,0},{3,1},{4,6},{5,7},{6,4},{7,5},{8,10},{9,11},{10,... | collective-permute-start | bytes 2359304 | tf_op jit(solution)/shard_map/ppermute | solution.py:442
  169.4 107.9 %collective-permute-start.12 = (bf16[6144,128]{1,0:T(8,128)(2,1)}, bf16[6144,128]{1,0:T(8,128)(2,1)}, u32[]{:S(2)}, u32[]{:S(2)}) collective-permute-start(bf16[6144,128]{1,0:T(8,128)(2,1)} %collective-permute-done.11.near), channel_id=1, source_target_pairs={{0,4},{4,0},{1,5},{5,1},{2,6},{6,2},{3,7},{7,3},{8,12},{12,8},{9,1... | collective-permute-start | bytes 4718600 | tf_op jit(solution)/shard_map/ppermute | solution.py:442
  173.1 38.1 %collective-permute-start.17 = (bf16[128,2048]{1,0:T(8,128)(2,1)}, bf16[128,2048]{1,0:T(8,128)(2,1)}, u32[]{:S(2)}, u32[]{:S(2)}) collective-permute-start(bf16[128,2048]{1,0:T(8,128)(2,1)} %get-tuple-element.25), channel_id=1, source_target_pairs={{0,2},{1,3},{2,0},{3,1},{4,6},{5,7},{6,4},{7,5},{8,10},{9,11},{10,... | collective-permute-start | bytes 1572872 | tf_op jit(solution)/shard_map/ppermute | solution.py:442
  207.0 76.3 %collective-permute-start.16 = (bf16[256,2048]{1,0:T(8,128)(2,1)}, bf16[256,2048]{1,0:T(8,128)(2,1)}, u32[]{:S(2)}, u32[]{:S(2)}) collective-permute-start(bf16[256,2048]{1,0:T(8,128)(2,1)} %collective-permute-done.15.near_hbm), channel_id=1, source_target_pairs={{0,4},{4,0},{1,5},{5,1},{2,6},{6,2},{3,7},{7,3},{8,12},{12,8},{9,1... | collective-permute-start | bytes 3145736 | tf_op jit(solution)/shard_map/ppermute | solution.py:442
  211.1 64.6 %collective-permute-start.14 = (bf16[3072,128]{1,0:T(8,128)(2,1)}, bf16[3072,128]{1,0:T(8,128)(2,1)}, u32[]{:S(2)}, u32[]{:S(2)}) collective-permute-start(bf16[3072,128]{1,0:T(8,128)(2,1)} %collective-permute-done.13.mine), channel_id=1, source_target_pairs={{0,4},{4,0},{1,5},{5,1},{2,6},{6,2},{3,7},{7,3},{8,12},{12,8},{9,1... | collective-permute-start | bytes 2359304 | tf_op jit(solution)/shard_map/ppermute | solution.py:442
  211.2 72.1 %collective-permute-start.18 = (bf16[128,2048]{1,0:T(8,128)(2,1)}, bf16[128,2048]{1,0:T(8,128)(2,1)}, u32[]{:S(2)}, u32[]{:S(2)}) collective-permute-start(bf16[128,2048]{1,0:T(8,128)(2,1)} %collective-permute-done.17.mine_hbm), channel_id=1, source_target_pairs={{0,4},{4,0},{1,5},{5,1},{2,6},{6,2},{3,7},{7,3},{8,12},{12,8},{9,1... | collective-permute-start | bytes 1572872 | tf_op jit(solution)/shard_map/ppermute | solution.py:442
  213.7 1.9 collective-permute-start
  215.6 0.6 copy-start.13
  216.2 4.0 %collective-permute-start.1 = (bf16[80,128]{1,0:T(8,128)(2,1)S(1)}, bf16[80,128]{1,0:T(8,128)(2,1)S(1)}, u32[]{:S(2)}, u32[]{:S(2)}) collective-permute-start(bf16[80,128]{1,0:T(8,128)(2,1)S(1)} %shard_map.170.chip), channel_id=1, source_target_pairs={{0,24},{8,32},{16,40},{24,48},{32,56},{40,64},{48,72},{56,80},{64,... | collective-permute-start | bytes 61448 | tf_op jit(solution)/shard_map/ppermute | solution.py:442
  220.2 6.1 %collective-permute-start.2 = (bf16[80,128]{1,0:T(8,128)(2,1)S(1)}, bf16[80,128]{1,0:T(8,128)(2,1)S(1)}, u32[]{:S(2)}, u32[]{:S(2)}) collective-permute-start(bf16[80,128]{1,0:T(8,128)(2,1)S(1)} %shard_map.170.chip), channel_id=1, source_target_pairs={{0,16},{8,24},{16,32},{24,40},{32,48},{40,56},{48,64},{56,72},{64,... | collective-permute-start | bytes 61448 | tf_op jit(solution)/shard_map/ppermute | solution.py:442
  226.3 3.9 %collective-permute-start.3 = (bf16[80,128]{1,0:T(8,128)(2,1)S(1)}, bf16[80,128]{1,0:T(8,128)(2,1)S(1)}, u32[]{:S(2)}, u32[]{:S(2)}) collective-permute-start(bf16[80,128]{1,0:T(8,128)(2,1)S(1)} %shard_map.170.chip), channel_id=1, source_target_pairs={{0,8},{8,16},{16,24},{24,32},{32,40},{40,48},{48,56},{56,64},{64,7... | collective-permute-start | bytes 61448 | tf_op jit(solution)/shard_map/ppermute | solution.py:442
  230.2 12.7 %collective-permute-start.4 = (bf16[80,128]{1,0:T(8,128)(2,1)S(1)}, bf16[80,128]{1,0:T(8,128)(2,1)S(1)}, u32[]{:S(2)}, u32[]{:S(2)}) collective-permute-start(bf16[80,128]{1,0:T(8,128)(2,1)S(1)} %get-tuple-element.17), channel_id=1, source_target_pairs={{0,96},{8,104},{16,112},{24,120},{1,97},{9,105},{17,113},{25,121},... | collective-permute-start | bytes 61448 | tf_op jit(solution)/shard_map/ppermute | solution.py:442
  242.9 5.0 %collective-permute-start.5 = (bf16[80,128]{1,0:T(8,128)(2,1)S(1)}, bf16[80,128]{1,0:T(8,128)(2,1)S(1)}, u32[]{:S(2)}, u32[]{:S(2)}) collective-permute-start(bf16[80,128]{1,0:T(8,128)(2,1)S(1)} %get-tuple-element.17), channel_id=1, source_target_pairs={{0,64},{8,72},{16,80},{24,88},{32,96},{40,104},{48,112},{56,120},{... | collective-permute-start | bytes 61448 | tf_op jit(solution)/shard_map/ppermute | solution.py:442
  247.8 11.4 %collective-permute-start.6 = (bf16[80,128]{1,0:T(8,128)(2,1)S(1)}, bf16[80,128]{1,0:T(8,128)(2,1)S(1)}, u32[]{:S(2)}, u32[]{:S(2)}) collective-permute-start(bf16[80,128]{1,0:T(8,128)(2,1)S(1)} %get-tuple-element.17), channel_id=1, source_target_pairs={{0,32},{8,40},{16,48},{24,56},{32,64},{40,72},{48,80},{56,88},{64,... | collective-permute-start | bytes 61448 | tf_op jit(solution)/shard_map/ppermute | solution.py:442
  259.9 7.8 %collective-permute-start.7 = (bf16[80,128]{1,0:T(8,128)(2,1)}, bf16[80,128]{1,0:T(8,128)(2,1)}, u32[]{:S(2)}, u32[]{:S(2)}) collective-permute-start(bf16[80,128]{1,0:T(8,128)(2,1)} %shard_map.172.mine), channel_id=1, source_target_pairs={{0,4},{4,0},{1,5},{5,1},{2,6},{6,2},{3,7},{7,3},{8,12},{12,8},{9,1... | collective-permute-start | bytes 61448 | tf_op jit(solution)/shard_map/ppermute | solution.py:442
  267.2 11.2 %copy-start.2 = (bf16[6144,128]{1,0:T(8,128)(2,1)S(1)}, bf16[6144,128]{1,0:T(8,128)(2,1)}, u32[]{:S(2)}) copy-start(bf16[6144,128]{1,0:T(8,128)(2,1)} %copy-done.1) | copy-start | bytes 4718596
  267.2 11.2 %copy-start.4 = (bf16[128,2048]{1,0:T(8,128)(2,1)S(1)}, bf16[128,2048]{1,0:T(8,128)(2,1)}, u32[]{:S(2)}) copy-start(bf16[128,2048]{1,0:T(8,128)(2,1)} %get-tuple-element.22.normed) | copy-start | bytes 1572868
  267.6 1.0 copy-start.14
  269.3 1.0 copy-start.12
  270.3 0.9 copy-start.15
  274.3 0.8 copy-start.5
  275.1 8.1 %collective-permute-start.10 = (bf16[128,256]{1,0:T(8,128)(2,1)S(1)}, bf16[128,256]{1,0:T(8,128)(2,1)S(1)}, u32[]{:S(2)}, u32[]{:S(2)}) collective-permute-start(bf16[128,256]{1,0:T(8,128)(2,1)S(1)} %get-tuple-element.21), channel_id=1, source_target_pairs={{0,2},{1,3},{2,0},{3,1},{4,6},{5,7},{6,4},{7,5},{8,10},{9,11},{10,... | collective-permute-start | bytes 196616 | tf_op jit(solution)/shard_map/ppermute | solution.py:442
  275.7 7.6 %collective-permute-start.8 = (bf16[128,256]{1,0:T(8,128)(2,1)S(1)}, bf16[128,256]{1,0:T(8,128)(2,1)S(1)}, u32[]{:S(2)}, u32[]{:S(2)}) collective-permute-start(bf16[128,256]{1,0:T(8,128)(2,1)S(1)} %get-tuple-element.19), channel_id=1, source_target_pairs={{0,1},{1,2},{2,3},{3,0},{4,5},{5,6},{6,7},{7,4},{8,9},{9,10},{10,1... | collective-permute-start | bytes 196616 | tf_op jit(solution)/shard_map/ppermute | solution.py:442
  277.3 5.9 %collective-permute-start.9 = (bf16[128,256]{1,0:T(8,128)(2,1)S(1)}, bf16[128,256]{1,0:T(8,128)(2,1)S(1)}, u32[]{:S(2)}, u32[]{:S(2)}) collective-permute-start(bf16[128,256]{1,0:T(8,128)(2,1)S(1)} %get-tuple-element.20), channel_id=1, source_target_pairs={{0,3},{1,0},{2,1},{3,2},{4,7},{5,4},{6,5},{7,6},{8,11},{9,8},{10,9... | collective-permute-start | bytes 196616 | tf_op jit(solution)/shard_map/ppermute | solution.py:442
  278.3 4.9 %copy-start.6 = (bf16[128,2048]{1,0:T(8,128)(2,1)S(1)}, bf16[128,2048]{1,0:T(8,128)(2,1)}, u32[]{:S(2)}) copy-start(bf16[128,2048]{1,0:T(8,128)(2,1)} %copy-done.5) | copy-start | bytes 1572868
  278.4 4.9 %copy-start.11 = (f32[128,2]{1,0:T(8,128)S(1)}, f32[128,2]{1,0:T(8,128)}, u32[]{:S(2)}) copy-start(f32[128,2]{1,0:T(8,128)} %copy.18.weight) | copy-start | bytes 3076
  278.4 4.9 %copy-start.17 = (s32[2,128]{1,0:T(2,128)S(1)}, s32[2,128]{1,0:T(2,128)}, u32[]{:S(2)}) copy-start(s32[2,128]{1,0:T(2,128)} %get-tuple-element.14.places) | copy-start | bytes 3076

commit v2 on v1

--- a/solution.py
+++ b/solution.py
@@ -10,10 +10,11 @@
 BLOCK = 128
 LANES = 128
 TILE = 16
-EP = ("ep_0", "ep_1")
-EP_TP = ("ep_0", "ep_1", "tp")
-GRP_EP = ("grp", "ep_0", "ep_1")
-GRP_EP_TP = ("grp", "ep_0", "ep_1", "tp")
+CHIPS = 4
+EP = ("ep_hi", "ep_lo", "ep_1")
+EP_TP = EP + ("tp",)
+GRP_EP = ("grp",) + EP
+GRP_EP_TP = ("grp",) + EP_TP
 STATE_ROWS = 80
 
 ROPE_BASE = 10000.0
@@ -45,32 +46,8 @@
     return jnp.dot(a, b, preferred_element_type=F32)
 
 
-def swap_matrix():
-    side = TILE * TILE
-    row = lax.broadcasted_iota(jnp.int32, (side, side), 0)
-    col = lax.broadcasted_iota(jnp.int32, (side, side), 1)
-    hit = (row // TILE == col % TILE) & (row % TILE == col // TILE)
-    return jnp.where(hit, 1.0, 0.0).astype(BF16)
-
-
-def rows_to_tiles(swap, rows):
-    count = rows.shape[0] // TILE
-    width = rows.shape[1] // LANES
-    found = []
-    for at in range(0, count, 2):
-        pair = [
-            jnp.concatenate(
-                [
-                    rows[g * TILE : (g + 1) * TILE, k * LANES : (k + 1) * LANES]
-                    for k in range(width)
-                ],
-                axis=0,
-            )
-            for g in range(at, min(at + 2, count))
-        ]
-        out = dot(swap, jnp.concatenate(pair, axis=1)).astype(BF16)
-        found += [out[:, g * LANES : (g + 1) * LANES] for g in range(len(pair))]
-    return found
+def column(c):
+    return slice(c * LANES, (c + 1) * LANES)
 
 
 def prep_kernel(
@@ -105,12 +82,13 @@
     normed[...] = rows
     keep = pltpu.make_async_copy(normed, normed_hbm, sems.at[2])
     keep.start()
-    for g, tile in enumerate(rows_to_tiles(swap_matrix(), rows)):
-        tiles[g * TILE * TILE : (g + 1) * TILE * TILE, :] = tile
+    wide = rows.astype(F32)
+    for c in range(TILE):
+        tiles[pl.ds(c, number, stride=TILE), :] = wide[:, column(c)]
 
     @pl.loop(0, number, unroll=8)
     def _(n):
-        row = tiles[pl.ds(pl.multiple_of(n * TILE, TILE), TILE), :]
+        row = tiles[pl.ds(pl.multiple_of(n * TILE, TILE), TILE), :].astype(BF16)
         for k in range(top):
             at = pl.multiple_of(places[k, n] * TILE, TILE)
             outbound[pl.ds(at, TILE), :] = row
@@ -129,6 +107,7 @@
     down_w,
     rows,
     arrived,
+    wide,
     out,
     sems,
     in_sems,
@@ -149,21 +128,15 @@
             at = pl.ds(j * part, part)
             copies[i].append(pltpu.make_async_copy(src.at[0, at], dst.at[at], sems.at[i, j]))
             copies[i][-1].start()
-    swap = swap_matrix()
-    side = TILE * TILE
-    groups = arrived.shape[0] // side
-    for at in range(0, groups, 2):
-        if at * side % share == 0:
-            landed[at * side // share].wait()
-        pair = jnp.concatenate(
-            [arrived[g * side : (g + 1) * side, :] for g in (at, at + 1)], axis=1
-        )
-        turned = dot(swap, pair).astype(BF16)
-        for j in range(2):
-            for k in range(TILE):
-                rows[
-                    (at + j) * TILE : (at + j + 1) * TILE, k * LANES : (k + 1) * LANES
-                ] = turned[k * TILE : (k + 1) * TILE, j * LANES : (j + 1) * LANES]
+    depth = share // TILE
+    for j in range(chunks):
+        landed[j].wait()
+        at = slice(j * share, (j + 1) * share)
+        wide[at, :] = arrived[at, :].astype(F32)
+        for c in range(TILE):
+            rows[j * depth : (j + 1) * depth, column(c)] = wide[
+                pl.ds(j * share + c, depth, stride=TILE), :
+            ].astype(BF16)
     for copy in copies[0]:
         copy.wait()
     gated = jax.nn.silu(dot(rows[...], gate_w[...]))
@@ -172,12 +145,15 @@
     hidden = (gated * dot(rows[...], up_w[...])).astype(BF16)
     for copy in copies[2]:
         copy.wait()
+    count = rows.shape[0]
+    step = 4 * LANES
+    for at in range(0, down_w.shape[1], step):
+        result = dot(hidden, down_w[:, at : at + step])
+        for c in range(step // LANES):
+            wide[pl.ds(at // LANES + c, count, stride=TILE), :] = result[:, column(c)]
     left = []
-    step = rows.shape[0] // chunks
     for j in range(chunks):
-        result = dot(hidden[j * step : (j + 1) * step, :], down_w[...]).astype(BF16)
-        for g, tile in enumerate(rows_to_tiles(swap, result)):
-            out[j * share + g * side : j * share + (g + 1) * side, :] = tile
+        out[j * share : (j + 1) * share, :] = wide[j * share : (j + 1) * share, :].astype(BF16)
         at = pl.ds(j * share, share)
         left.append(pltpu.make_async_copy(out.at[at], out_hbm.at[at], out_sems.at[j]))
         left[-1].start()
@@ -373,7 +349,6 @@
     mixer_out,
     moe_out,
     picked,
-    rows,
     shared,
     near,
     other,
@@ -391,8 +366,6 @@
     copies = [pltpu.make_async_copy(a, b, sems.at[i]) for i, (a, b) in enumerate(pairs)]
     for copy in copies:
         copy.start()
-    swap = swap_matrix()
-    side = TILE * TILE
     number = moe_out.shape[0]
     top = weight.shape[1]
 
@@ -402,27 +375,16 @@
             place = places[k, n]
             picked[k, pl.ds(pl.multiple_of(n * TILE, TILE), TILE), :] = returned[
                 pl.ds(pl.multiple_of(place * TILE, TILE), TILE), :
-            ]
-
-    for k in range(top):
-        for at in range(0, number // TILE, 2):
-            pair = jnp.concatenate(
-                [picked[k, g * side : (g + 1) * side, :] for g in (at, at + 1)], axis=1
-            )
-            turned = dot(swap, pair).astype(BF16)
-            for j in range(2):
-                for c in range(TILE):
-                    rows[
-                        k,
-                        (at + j) * TILE : (at + j + 1) * TILE,
-                        c * LANES : (c + 1) * LANES,
-                    ] = turned[c * TILE : (c + 1) * TILE, j * LANES : (j + 1) * LANES]
-    for copy in copies:
+            ].astype(F32)
+
+    copies[0].wait()
+    for c in range(TILE):
+        total = shared[:, column(c)]
+        for k in range(top):
+            total = total + picked[k, pl.ds(c, number, stride=TILE), :] * weight[:, k : k + 1]
+        moe_out[:, column(c)] = total.astype(BF16)
+    for copy in copies[1:]:
         copy.wait()
-    total = shared[...]
-    for k in range(top):
-        total = total + rows[k].astype(F32) * weight[:, k : k + 1]
-    moe_out[...] = total.astype(BF16)
     first = core[0] == 0
     left, right, across = gated_left[...], gated_right[...], gated_far[...]
     mixed = own[...].astype(F32)
@@ -434,12 +396,9 @@
     mixer_out[...] = mixed.astype(BF16)
 
 
-def moved_by(array, axis, step, around=True):
+def moved_by(array, axis, step):
     count = lax.axis_size(axis)
-    pairs = [
-        (s, (s + step) % count) for s in range(count) if around or 0 <= s + step < count
-    ]
-    return lax.ppermute(array, axis, pairs)
+    return lax.ppermute(array, axis, [(s, (s + step) % count) for s in range(count)])
 
 
 def outward(array):
@@ -477,14 +436,32 @@
     out[...] = closed(joined(opened(early), opened(late)))
 
 
-def near_kernel(chip, far3, far2, far1, before, window):
-    start = joined(joined(opened(far3[...]), opened(far2[...])), opened(far1[...]))
+def near_kernel(seat, chip, *refs):
+    *near, before, window = refs
+    count = len(near) + 1
+    found = [chip[...].astype(F32)] + [part[...].astype(F32) for part in near]
+    start = whole = None
+    for p in range(count):
+        back = lax.rem(seat[0] + count - p, count)
+        part = found[0]
+        for d in range(1, count):
+            part = jnp.where(back == d, found[d], part)
+        item = opened(part)
+        early = opened(jnp.where(seat[0] > p, part, 0.0))
+        start = early if start is None else joined(start, early)
+        whole = item if whole is None else joined(whole, item)
     before[...] = closed(start)
-    window[...] = closed(joined(start, opened(chip[...])))
-
-
-def far_kernel(before, far12, far8, far4, prefix):
-    start = joined(joined(opened(far12[...]), opened(far8[...])), opened(far4[...]))
+    packed = closed(whole)
+    for p in range(window.shape[0] // STATE_ROWS):
+        window[p * STATE_ROWS : (p + 1) * STATE_ROWS, :] = packed
+
+
+def far_kernel(seat, before, window, prefix):
+    start = None
+    for p in range(window.shape[0] // STATE_ROWS):
+        part = window[p * STATE_ROWS : (p + 1) * STATE_ROWS, :].astype(F32)
+        early = opened(jnp.where(seat[0] > p, part, 0.0))
+        start = early if start is None else joined(start, early)
     prefix[...] = closed(joined(start, opened(before[...])))
 
 
@@ -555,7 +532,7 @@
             pltpu.VMEM((rows_dev, width), BF16),
             pltpu.VMEM((1, width), F32),
             pltpu.VMEM((rows_dev, width), BF16),
-            pltpu.VMEM((rows_dev * TILE, LANES), BF16),
+            pltpu.VMEM((rows_dev * TILE, LANES), F32),
             pltpu.SMEM((experts,), jnp.int32),
             pltpu.SemaphoreType.DMA((3,)),
         ],
@@ -591,12 +568,24 @@
     )(keys, values, log_decay.T, cosine, sine)
     other = moved_by(own, "ep_1", 1)
     chip = small(chip_kernel, packed_shape, [SMEM, VMEM, VMEM], VMEM)(core, own, other)
-    near = [moved_by(chip, "ep_0", d, False) for d in (3, 2, 1)]
+    low_seat = lax.axis_index("ep_lo").reshape(1).astype(jnp.int32)
+    high_seat = lax.axis_index("ep_hi").reshape(1).astype(jnp.int32)
+    groups = lax.axis_size("ep_hi")
+    near = [moved_by(chip, "ep_lo", d) for d in range(1, lax.axis_size("ep_lo"))]
+    window_shape = jax.ShapeDtypeStruct((groups * STATE_ROWS, value_size), BF16)
     before, window = small(
-        near_kernel, (packed_shape, packed_shape), [VMEM] * 4, (VMEM, VMEM)
-    )(chip, *near)
-    far = [moved_by(window, "ep_0", d, False) for d in (12, 8, 4)]
-    prefix = small(far_kernel, packed_shape, [VMEM] * 4, VMEM)(before, *far)
+        near_kernel, (packed_shape, window_shape), [SMEM] + [VMEM] * (1 + len(near)), (VMEM, VMEM)
+    )(low_seat, chip, *near)
+    far = lax.all_to_all(
+        window.reshape(groups, STATE_ROWS, value_size),
+        "ep_hi",
+        split_axis=0,
+        concat_axis=0,
+        tiled=True,
+    )
+    prefix = small(far_kernel, packed_shape, [SMEM] + [VMEM] * 2, VMEM)(
+        high_seat, before, far.reshape(groups * STATE_ROWS, value_size)
+    )
     swapped = moved_by(prefix, "ep_1", 1)
     state_in = small(
         enter_kernel,
@@ -652,6 +641,7 @@
             pltpu.VMEM((hidden_size, width), BF16),
             pltpu.VMEM((slots, width), BF16),
             pltpu.VMEM((tile_rows, LANES), BF16),
+            pltpu.VMEM((tile_rows, LANES), F32),
             pltpu.VMEM((tile_rows, LANES), BF16),
             pltpu.SemaphoreType.DMA((3, pieces)),
             pltpu.SemaphoreType.DMA((chunks,)),
@@ -688,8 +678,7 @@
         [SMEM, SMEM] + [VMEM] * 6 + [HBM] * 5,
         (VMEM,) * 2,
         [
-            pltpu.VMEM((top, rows_dev * TILE, LANES), BF16),
-            pltpu.VMEM((top, rows_dev, width), BF16),
+            pltpu.VMEM((top, rows_dev * TILE, LANES), F32),
             pltpu.VMEM((rows_dev, width), F32),
             pltpu.VMEM((2 * half_out, width), BF16),
             pltpu.VMEM((2 * half_out, width), BF16),
@@ -718,8 +707,10 @@
 
 def solution(mesh):
     split = Mesh(
-        mesh.devices.reshape(mesh.shape["grp"], mesh.shape["ep"] // 2, 2, mesh.shape["tp"]),
-        ("grp", "ep_0", "ep_1", "tp"),
+        mesh.devices.reshape(
+            mesh.shape["grp"], mesh.shape["ep"] // (2 * CHIPS), CHIPS, 2, mesh.shape["tp"]
+        ),
+        GRP_EP_TP,
     )
     return jax.shard_map(
         per_device,

time: 288 us -> 253 us (0.88)
  blocking collectives: 107 us -> 0 us
  waiting for transfers between devices: 73.4 us -> 138 us
  starting transfers between devices: 68.6 us -> 72.2 us
  local copies, waits for them, and re-layouts: 8.33 us -> 11.6 us
    all_to_all x1 -> x0, blocking collectives: 107 us -> none  [per_device(): lax.all_to_all(outbound.reshape(experts, capacity * TILE, LANES), EP_TP,...]
    ppermute x17 -> x14, waiting for transfers between devices: 7.55 us -> 59.9 us  [moved_by(): lax.ppermute(array, axis, [(s, (s + step) % count) for s in range(count)])]
    ppermute x17 -> x14, starting transfers between devices: 56 us -> 17.4 us  [moved_by(): lax.ppermute(array, axis, [(s, (s + step) % count) for s in range(count)])]
    all_to_all x0 -> x2, starting transfers between devices: none -> 36.7 us  [the longest x1 31.1 us: per_device(): lax.all_to_all(outbound.reshape(experts, capacity * TILE, LANES), EP_TP,...]
    all_to_all x0 -> x2, waiting for transfers between devices: none -> 12.6 us  [the longest x1 8.37 us: per_device(): lax.all_to_all(outbound.reshape(experts, capacity * TILE, LANES), EP_TP,...]
    all_to_all x1, starting transfers between devices: 9.48 us -> 14.8 us  [per_device(): lax.all_to_all(answers.reshape(experts, capacity * TILE, LANES), EP_TP, s...]
    unnamed x39 -> x49, local copies, waits for them, and re-layouts: 8.24 us -> 11.5 us
  transfers between devices with their start and end apart: 20 -> 19, of which waited for: 10 -> 9; matrix products, arithmetic and copies ran while one was open for 1% -> 1% of each run, Pallas kernels for 4% -> 8%
where the time goes in v2:
time: 253 us; the launch traced here: 252 us
  waiting for transfers between devices  138 us (55%)
  starting transfers between devices  72.2 us (29%)
  Pallas kernels  28.2 us (11%)
  local copies, waits for them, and re-layouts  11.6 us (5%)
    ppermute x2, waiting for transfers between devices, outward(): return lax.ppermute(array, ('ep_1', 'tp'), pairs)  65.6 us
    ppermute x14, waiting for transfers between devices, moved_by(): lax.ppermute(array, axis, [(s, (s + step) % count) for s in range(count)])  59.9 us
    all_to_all x1, starting transfers between devices, per_device(): lax.all_to_all(outbound.reshape(experts, capacity * TILE, LANES), EP_TP,...  31.1 us
    ppermute x14, starting transfers between devices, moved_by(): lax.ppermute(array, axis, [(s, (s + step) % count) for s in range(count)])  17.4 us
    all_to_all x1, starting transfers between devices, per_device(): lax.all_to_all(answers.reshape(experts, capacity * TILE, LANES), EP_TP, s...  14.8 us
    unnamed x49, local copies, waits for them, and re-layouts  11.5 us
    pallas_call x1, Pallas kernels, per_device(): call(expert_kernel, jax.ShapeDtypeStruct((tile_rows, LANES), BF16), [HBM]...  8.39 us
    all_to_all x1, waiting for transfers between devices, per_device(): lax.all_to_all(outbound.reshape(experts, capacity * TILE, LANES), EP_TP,...  8.37 us
  transfers between devices with their start and end apart: 19, of which 9 were waited for; matrix products, arithmetic and copies ran while one was open for 1% of the time, Pallas kernels for 8%

profile of v2, /device:TPU:33, one launch (start us, length us, event | category | flops | bytes accessed | tf_op | source)
XLA Modules:
  0.0 252.1 jit_solution(12919228313420696161)
XLA Ops:
  0.6 4.6 %shard_map.167 = (bf16[128,2048]{1,0:T(8,128)(2,1)}, bf16[6144,128]{1,0:T(8,128)(2,1)}, s32[2,128]{1,0:T(2,128)}) custom-call(s32[2,128]{1,0:T(2,128)} %bitcast.21, bf16[128,2048]{1,0:T(8,128)(2,1)} %x_hbm.1, f32[1,2048]{1,0:T(1,128)} %bitcast.20), custom_call_target="tpu_custom_call" | custom-call | flops 134217728 | bytes 1048576 | tf_op jit(solution)/shard_map/pallas_call | solution.py:522
  5.2 31.1 %all-to-all-start = ((bf16[128,48,128]{2,1,0:T(8,128)(2,1)}), bf16[128,48,128]{2,1,0:T(8,128)(2,1)S(1)}, u32[]{:S(2)}, u32[]{:S(2)}) async-start(bf16[128,48,128]{2,1,0:T(8,128)(2,1)} %bitcast.19), calls=%async_computation | async-start | bytes 3145728 | tf_op jit(solution)/shard_map/all_to_all | solution.py:544
  36.4 0.1 mul.28
  36.5 1.0 multiply_sine_fusion
  37.5 0.8 shard_map.169.own
  38.4 2.7 %collective-permute-start = (bf16[160,128]{1,0:T(8,128)(2,1)S(1)}, bf16[160,128]{1,0:T(8,128)(2,1)S(1)}, u32[]{:S(2)}, u32[]{:S(2)}) collective-permute-start(bf16[160,128]{1,0:T(8,128)(2,1)S(1)} %shard_map.169.own), channel_id=1, source_target_pairs={{0,4},{4,0},{1,5},{5,1},{2,6},{6,2},{3,7},{7,3},{8,12},{12,8},{9,1... | collective-permute-start | bytes 122888 | tf_op jit(solution)/shard_map/ppermute | solution.py:401
  41.1 0.9 collective-permute-done.other
  42.0 0.6 copy-done.15
  42.6 1.4 collective-permute-start.2
  44.0 1.9 collective-permute-start.3
  45.8 55.1 %collective-permute-done.1.refs_0_ = bf16[80,128]{1,0:T(8,128)(2,1)S(1)} collective-permute-done((bf16[80,128]{1,0:T(8,128)(2,1)S(1)}, bf16[80,128]{1,0:T(8,128)(2,1)S(1)}, u32[]{:S(2)}, u32[]{:S(2)}) %collective-permute-start.1) | collective-permute-done | bytes 20512 | tf_op jit(solution)/shard_map/ppermute | solution.py:401
  100.9 0.9 collective-permute-done.2.refs_1_
  101.8 0.5 collective-permute-done.3.refs_2_
  102.3 0.7 shard_map.171
  103.0 0.6 copy-done.18
  103.6 8.4 %all-to-all-done = bf16[128,48,128]{2,1,0:T(8,128)(2,1)S(1)} async-done(((bf16[128,48,128]{2,1,0:T(8,128)(2,1)}), bf16[128,48,128]{2,1,0:T(8,128)(2,1)S(1)}, u32[]{:S(2)}, u32[]{:S(2)}) %all-to-all-start) | async-done | bytes 1572896 | tf_op jit(solution)/shard_map/all_to_all | solution.py:544
  112.0 1.1 copy-done.22
  113.1 5.6 %all-to-all-start.2 = ((bf16[4,80,128]{2,1,0:T(8,128)(2,1)}), bf16[4,80,128]{2,1,0:T(8,128)(2,1)S(1)}, u32[]{:S(2)}, u32[]{:S(2)}) async-start(bf16[4,80,128]{2,1,0:T(8,128)(2,1)} %bitcast.11), calls=%async_computation.2 | async-start | bytes 163840 | tf_op jit(solution)/shard_map/all_to_all | solution.py:579
  118.7 8.4 %shard_map.168 = bf16[6144,128]{1,0:T(8,128)(2,1)} custom-call(bf16[6144,128]{1,0:T(8,128)(2,1)} %bitcast.18, bf16[1,2048,512]{2,1,0:T(8,128)(2,1)} %gate_hbm.1, bf16[1,2048,512]{2,1,0:T(8,128)(2,1)} %up_hbm.1, bf16[1,512,2048]{2,1,0:T(8,128)(2,1)} %down_hbm.1), custom_call_target="tpu_custom_call" | custom-call | flops 2415919104 | bytes 6291456 | tf_op jit(solution)/shard_map/pallas_call | solution.py:633
  127.1 4.2 %all-to-all-done.2 = bf16[4,80,128]{2,1,0:T(8,128)(2,1)S(1)} async-done(((bf16[4,80,128]{2,1,0:T(8,128)(2,1)}), bf16[4,80,128]{2,1,0:T(8,128)(2,1)S(1)}, u32[]{:S(2)}, u32[]{:S(2)}) %all-to-all-start.2) | async-done | bytes 81952 | tf_op jit(solution)/shard_map/all_to_all | solution.py:579
  131.3 0.6 copy-done.11
  132.0 14.8 %all-to-all-start.1 = ((bf16[128,48,128]{2,1,0:T(8,128)(2,1)}), bf16[128,48,128]{2,1,0:T(8,128)(2,1)S(1)}, u32[]{:S(2)}, u32[]{:S(2)}) async-start(bf16[128,48,128]{2,1,0:T(8,128)(2,1)} %bitcast.17), calls=%async_computation.1 | async-start | bytes 3145728 | tf_op jit(solution)/shard_map/all_to_all | solution.py:654
  146.8 1.0 copy-done.7
  147.9 1.0 copy-done.8
  148.9 1.0 copy-done.9
  150.0 0.3 shard_map.175
  150.2 2.7 %collective-permute-start.8 = (bf16[6144,128]{1,0:T(8,128)(2,1)S(1)}, bf16[6144,128]{1,0:T(8,128)(2,1)}, u32[]{:S(2)}, u32[]{:S(2)}) collective-permute-start(bf16[6144,128]{1,0:T(8,128)(2,1)S(1)} %get-tuple-element.23.own), channel_id=1, source_target_pairs={{0,1},{1,2},{2,3},{3,0},{4,7},{5,4},{6,5},{7,6},{8,9},{9,10},{10,1... | collective-permute-start | bytes 4718600 | tf_op jit(solution)/shard_map/ppermute | solution.py:408
  152.9 1.2 copy-done.1
  154.1 0.6 collective-permute-start.12
  154.7 0.1 collective-permute-start.10
  154.8 31.9 %collective-permute-done.8.near = bf16[6144,128]{1,0:T(8,128)(2,1)} collective-permute-done((bf16[6144,128]{1,0:T(8,128)(2,1)S(1)}, bf16[6144,128]{1,0:T(8,128)(2,1)}, u32[]{:S(2)}, u32[]{:S(2)}) %collective-permute-start.8) | collective-permute-done | bytes 1572896 | tf_op jit(solution)/shard_map/ppermute | solution.py:408
  186.7 3.9 %collective-permute-start.9 = (bf16[6144,128]{1,0:T(8,128)(2,1)}, bf16[6144,128]{1,0:T(8,128)(2,1)}, u32[]{:S(2)}, u32[]{:S(2)}) collective-permute-start(bf16[6144,128]{1,0:T(8,128)(2,1)} %collective-permute-done.8.near), channel_id=1, source_target_pairs={{0,4},{4,0},{1,5},{5,1},{2,6},{6,2},{3,7},{7,3},{8,12},{12,8},{9,1... | collective-permute-start | bytes 4718600 | tf_op jit(solution)/shard_map/ppermute | solution.py:401
  190.6 33.6 %collective-permute-done.12.near_hbm = bf16[256,2048]{1,0:T(8,128)(2,1)} collective-permute-done((bf16[256,2048]{1,0:T(8,128)(2,1)S(1)}, bf16[256,2048]{1,0:T(8,128)(2,1)}, u32[]{:S(2)}, u32[]{:S(2)}) %collective-permute-start.12) | collective-permute-done | bytes 1048608 | tf_op jit(solution)/shard_map/ppermute | solution.py:408
  224.2 4.1 %collective-permute-start.13 = (bf16[256,2048]{1,0:T(8,128)(2,1)}, bf16[256,2048]{1,0:T(8,128)(2,1)}, u32[]{:S(2)}, u32[]{:S(2)}) collective-permute-start(bf16[256,2048]{1,0:T(8,128)(2,1)} %collective-permute-done.12.near_hbm), channel_id=1, source_target_pairs={{0,4},{4,0},{1,5},{5,1},{2,6},{6,2},{3,7},{7,3},{8,12},{12,8},{9,1... | collective-permute-start | bytes 3145736 | tf_op jit(solution)/shard_map/ppermute | solution.py:401
  228.3 0.5 collective-permute-start.15
  228.9 0.6 shard_map.172.mine
  229.5 0.1 collective-permute-start.4
  229.6 0.7 copy.18.weight
  230.4 2.5 collective-permute-done.4.theirs
  232.9 0.8 copy-done.16
  233.6 0.8 shard_map.173.state_in
  234.4 0.9 copy-done.14
  235.4 0.9 copy-done.17
  236.3 3.1 %shard_map.174 = (bf16[128,2048]{1,0:T(8,128)(2,1)S(1)}, bf16[128,256]{1,0:T(8,128)(2,1)S(1)}, bf16[128,256]{1,0:T(8,128)(2,1)S(1)}, bf16[128,256]{1,0:T(8,128)(2,1)S(1)}) custom-call(s32[1]{0:T(128)} %bitcast.7.seat, bf16[512,128]{1,0:T(8,128)(2,1)S(1)} %copy-done.17, bf16[512,128]{1,0:T(8,128)(2,1)S(1)} %copy-done.10, bf16[512,256]{1,0:T(8,128)(2,1)S(1)} %copy-done.3, ...), custom_call_target="tpu_custom_call" | custom-call | flops 262144000 | bytes 5242880 | tf_op jit(solution)/shard_map/pallas_call | solution.py:663
  239.4 0.8 copy-done.5
  240.2 2.7 %collective-permute-start.6 = (bf16[128,256]{1,0:T(8,128)(2,1)S(1)}, bf16[128,256]{1,0:T(8,128)(2,1)S(1)}, u32[]{:S(2)}, u32[]{:S(2)}) collective-permute-start(bf16[128,256]{1,0:T(8,128)(2,1)S(1)} %get-tuple-element.20), channel_id=1, source_target_pairs={{0,3},{1,0},{2,1},{3,2},{4,7},{5,4},{6,5},{7,6},{8,11},{9,8},{10,9... | collective-permute-start | bytes 196616 | tf_op jit(solution)/shard_map/ppermute | solution.py:401
  243.0 4.8 %shard_map.176.shared_hbm = f32[128,2048]{1,0:T(8,128)S(1)} custom-call(s32[1]{0:T(128)} %bitcast.2.core, bf16[128,2048]{1,0:T(8,128)(2,1)S(1)} %copy-done.4, bf16[6144,128]{1,0:T(8,128)(2,1)S(1)} %copy-done.2, bf16[6144,128]{1,0:T(8,128)(2,1)} %collective-permute-done.8.near, bf16[6144,128]{1,0:T(8,128)(2,1)} %collective-permute-done.9.near_other, ...), custom_call_target="tpu_custom_call" | custom-call | flops 805306368 | bytes 5242880 | tf_op jit(solution)/shard_map/pallas_call | solution.py:618
  247.9 4.0 %shard_map.177 = (bf16[128,2048]{1,0:T(8,128)(2,1)}, bf16[128,2048]{1,0:T(8,128)(2,1)}) custom-call(s32[2,128]{1,0:T(2,128)S(1)} %copy-done.21, s32[1]{0:T(128)} %bitcast.2.core, bf16[6144,128]{1,0:T(8,128)(2,1)S(1)} %bitcast.13, f32[128,2]{1,0:T(8,128)S(1)} %copy-done.13, bf16[128,2048]{1,0:T(8,128)(2,1)S(1)} %copy-done.6, ...), custom_call_target="tpu_custom_call" | custom-call | flops 786432000 | bytes 5242880 | tf_op jit(solution)/shard_map/pallas_call | solution.py:675
  (55 shorter events, 0.2 us)
Async XLA Ops:
  5.2 32.3 %copy-start.3 = (bf16[512,256]{1,0:T(8,128)(2,1)S(1)}, bf16[512,256]{1,0:T(8,128)(2,1)}, u32[]{:S(2)}) copy-start(bf16[512,256]{1,0:T(8,128)(2,1)} %v.3) | copy-start | bytes 786436
  5.2 32.3 %copy-start.10 = (bf16[512,128]{1,0:T(8,128)(2,1)S(1)}, bf16[512,128]{1,0:T(8,128)(2,1)}, u32[]{:S(2)}) copy-start(bf16[512,128]{1,0:T(8,128)(2,1)} %k.3) | copy-start | bytes 393220
  5.2 32.3 %copy-start.20 = (f32[512,2]{0,1:T(2,128)S(1)}, f32[512,2]{0,1:T(2,128)}, u32[]{:S(2)}) copy-start(f32[512,2]{0,1:T(2,128)} %param.20) | copy-start | bytes 12292
  5.2 106.8 %all-to-all-start = ((bf16[128,48,128]{2,1,0:T(8,128)(2,1)}), bf16[128,48,128]{2,1,0:T(8,128)(2,1)S(1)}, u32[]{:S(2)}, u32[]{:S(2)}) async-start(bf16[128,48,128]{2,1,0:T(8,128)(2,1)} %bitcast.19), calls=%async_computation | async-start | bytes 3145728 | tf_op jit(solution)/shard_map/all_to_all | solution.py:544
  38.4 3.6 %collective-permute-start = (bf16[160,128]{1,0:T(8,128)(2,1)S(1)}, bf16[160,128]{1,0:T(8,128)(2,1)S(1)}, u32[]{:S(2)}, u32[]{:S(2)}) collective-permute-start(bf16[160,128]{1,0:T(8,128)(2,1)S(1)} %shard_map.169.own), channel_id=1, source_target_pairs={{0,4},{4,0},{1,5},{5,1},{2,6},{6,2},{3,7},{7,3},{8,12},{12,8},{9,1... | collective-permute-start | bytes 122888 | tf_op jit(solution)/shard_map/ppermute | solution.py:401
  42.0 0.6 copy-start.15
  42.6 58.4 %collective-permute-start.1 = (bf16[80,128]{1,0:T(8,128)(2,1)S(1)}, bf16[80,128]{1,0:T(8,128)(2,1)S(1)}, u32[]{:S(2)}, u32[]{:S(2)}) collective-permute-start(bf16[80,128]{1,0:T(8,128)(2,1)S(1)} %shard_map.170.chip), channel_id=1, source_target_pairs={{0,8},{8,16},{16,24},{24,0},{1,9},{9,17},{17,25},{25,1},{2,10},{10... | collective-permute-start | bytes 61448 | tf_op jit(solution)/shard_map/ppermute | solution.py:401
  42.6 59.3 %collective-permute-start.2 = (bf16[80,128]{1,0:T(8,128)(2,1)S(1)}, bf16[80,128]{1,0:T(8,128)(2,1)S(1)}, u32[]{:S(2)}, u32[]{:S(2)}) collective-permute-start(bf16[80,128]{1,0:T(8,128)(2,1)S(1)} %shard_map.170.chip), channel_id=1, source_target_pairs={{0,16},{8,24},{16,0},{24,8},{1,17},{9,25},{17,1},{25,9},{2,18},{10... | collective-permute-start | bytes 61448 | tf_op jit(solution)/shard_map/ppermute | solution.py:401
  44.0 58.4 %collective-permute-start.3 = (bf16[80,128]{1,0:T(8,128)(2,1)S(1)}, bf16[80,128]{1,0:T(8,128)(2,1)S(1)}, u32[]{:S(2)}, u32[]{:S(2)}) collective-permute-start(bf16[80,128]{1,0:T(8,128)(2,1)S(1)} %shard_map.170.chip), channel_id=1, source_target_pairs={{0,24},{8,0},{16,8},{24,16},{1,25},{9,1},{17,9},{25,17},{2,26},{10... | collective-permute-start | bytes 61448 | tf_op jit(solution)/shard_map/ppermute | solution.py:401
  103.0 0.6 copy-start.18
  112.0 1.1 copy-start.22
  113.1 18.2 %all-to-all-start.2 = ((bf16[4,80,128]{2,1,0:T(8,128)(2,1)}), bf16[4,80,128]{2,1,0:T(8,128)(2,1)S(1)}, u32[]{:S(2)}, u32[]{:S(2)}) async-start(bf16[4,80,128]{2,1,0:T(8,128)(2,1)} %bitcast.11), calls=%async_computation.2 | async-start | bytes 163840 | tf_op jit(solution)/shard_map/all_to_all | solution.py:579
  131.3 0.6 copy-start.11
  132.0 14.9 %copy-start = (bf16[256,2048]{1,0:T(8,128)(2,1)S(1)}, bf16[256,2048]{1,0:T(8,128)(2,1)}, u32[]{:S(2)}) copy-start(bf16[256,2048]{1,0:T(8,128)(2,1)} %w_out.3) | copy-start | bytes 3145732
  132.0 115.9 %all-to-all-start.1 = ((bf16[128,48,128]{2,1,0:T(8,128)(2,1)}), bf16[128,48,128]{2,1,0:T(8,128)(2,1)S(1)}, u32[]{:S(2)}, u32[]{:S(2)}) async-start(bf16[128,48,128]{2,1,0:T(8,128)(2,1)} %bitcast.17), calls=%async_computation.1 | async-start | bytes 3145728 | tf_op jit(solution)/shard_map/all_to_all | solution.py:654
  146.8 1.0 copy-start.7
  147.9 1.0 copy-start.8
  148.9 1.0 copy-start.9
  150.0 78.9 %copy-start.12 = (bf16[4,80,128]{2,1,0:T(8,128)(2,1)S(1)}, bf16[4,80,128]{2,1,0:T(8,128)(2,1)}, u32[]{:S(2)}) copy-start(bf16[4,80,128]{2,1,0:T(8,128)(2,1)} %copy-done.11) | copy-start | bytes 245764
  150.0 78.9 %copy-start.19 = (bf16[80,128]{1,0:T(8,128)(2,1)S(1)}, bf16[80,128]{1,0:T(8,128)(2,1)}, u32[]{:S(2)}) copy-start(bf16[80,128]{1,0:T(8,128)(2,1)} %copy-done.18) | copy-start | bytes 61444
  150.0 79.7 %copy-start.23 = (f32[128,2]{0,1:T(2,128)S(1)}, f32[128,2]{0,1:T(2,128)}, u32[]{:S(2)}) copy-start(f32[128,2]{0,1:T(2,128)} %param.25) | copy-start | bytes 3076
  150.2 36.5 %collective-permute-start.8 = (bf16[6144,128]{1,0:T(8,128)(2,1)S(1)}, bf16[6144,128]{1,0:T(8,128)(2,1)}, u32[]{:S(2)}, u32[]{:S(2)}) collective-permute-start(bf16[6144,128]{1,0:T(8,128)(2,1)S(1)} %get-tuple-element.23.own), channel_id=1, source_target_pairs={{0,1},{1,2},{2,3},{3,0},{4,7},{5,4},{6,5},{7,6},{8,9},{9,10},{10,1... | collective-permute-start | bytes 4718600 | tf_op jit(solution)/shard_map/ppermute | solution.py:408
  152.9 1.2 copy-start.1
  154.1 70.1 %collective-permute-start.12 = (bf16[256,2048]{1,0:T(8,128)(2,1)S(1)}, bf16[256,2048]{1,0:T(8,128)(2,1)}, u32[]{:S(2)}, u32[]{:S(2)}) collective-permute-start(bf16[256,2048]{1,0:T(8,128)(2,1)S(1)} %copy-done), channel_id=1, source_target_pairs={{0,1},{1,2},{2,3},{3,0},{4,7},{5,4},{6,5},{7,6},{8,9},{9,10},{10,1... | collective-permute-start | bytes 3145736 | tf_op jit(solution)/shard_map/ppermute | solution.py:408
  154.7 73.7 %collective-permute-start.10 = (bf16[3072,128]{1,0:T(8,128)(2,1)S(1)}, bf16[3072,128]{1,0:T(8,128)(2,1)}, u32[]{:S(2)}, u32[]{:S(2)}) collective-permute-start(bf16[3072,128]{1,0:T(8,128)(2,1)S(1)} %get-tuple-element.24), channel_id=1, source_target_pairs={{0,2},{1,3},{2,0},{3,1},{4,6},{5,7},{6,4},{7,5},{8,10},{9,11},{10,... | collective-permute-start | bytes 2359304 | tf_op jit(solution)/shard_map/ppermute | solution.py:401
  186.7 56.2 %collective-permute-start.9 = (bf16[6144,128]{1,0:T(8,128)(2,1)}, bf16[6144,128]{1,0:T(8,128)(2,1)}, u32[]{:S(2)}, u32[]{:S(2)}) collective-permute-start(bf16[6144,128]{1,0:T(8,128)(2,1)} %collective-permute-done.8.near), channel_id=1, source_target_pairs={{0,4},{4,0},{1,5},{5,1},{2,6},{6,2},{3,7},{7,3},{8,12},{12,8},{9,1... | collective-permute-start | bytes 4718600 | tf_op jit(solution)/shard_map/ppermute | solution.py:401
  190.6 37.8 %collective-permute-start.14 = (bf16[128,2048]{1,0:T(8,128)(2,1)S(1)}, bf16[128,2048]{1,0:T(8,128)(2,1)}, u32[]{:S(2)}, u32[]{:S(2)}) collective-permute-start(bf16[128,2048]{1,0:T(8,128)(2,1)S(1)} %get-tuple-element.25), channel_id=1, source_target_pairs={{0,2},{1,3},{2,0},{3,1},{4,6},{5,7},{6,4},{7,5},{8,10},{9,11},{10,... | collective-permute-start | bytes 1572872 | tf_op jit(solution)/shard_map/ppermute | solution.py:401
  224.2 23.6 %collective-permute-start.13 = (bf16[256,2048]{1,0:T(8,128)(2,1)}, bf16[256,2048]{1,0:T(8,128)(2,1)}, u32[]{:S(2)}, u32[]{:S(2)}) collective-permute-start(bf16[256,2048]{1,0:T(8,128)(2,1)} %collective-permute-done.12.near_hbm), channel_id=1, source_target_pairs={{0,4},{4,0},{1,5},{5,1},{2,6},{6,2},{3,7},{7,3},{8,12},{12,8},{9,1... | collective-permute-start | bytes 3145736 | tf_op jit(solution)/shard_map/ppermute | solution.py:401
  228.3 11.9 %collective-permute-start.11 = (bf16[3072,128]{1,0:T(8,128)(2,1)}, bf16[3072,128]{1,0:T(8,128)(2,1)}, u32[]{:S(2)}, u32[]{:S(2)}) collective-permute-start(bf16[3072,128]{1,0:T(8,128)(2,1)} %collective-permute-done.10.mine), channel_id=1, source_target_pairs={{0,4},{4,0},{1,5},{5,1},{2,6},{6,2},{3,7},{7,3},{8,12},{12,8},{9,1... | collective-permute-start | bytes 2359304 | tf_op jit(solution)/shard_map/ppermute | solution.py:401
  228.3 19.5 %collective-permute-start.15 = (bf16[128,2048]{1,0:T(8,128)(2,1)}, bf16[128,2048]{1,0:T(8,128)(2,1)}, u32[]{:S(2)}, u32[]{:S(2)}) collective-permute-start(bf16[128,2048]{1,0:T(8,128)(2,1)} %collective-permute-done.14.mine_hbm), channel_id=1, source_target_pairs={{0,4},{4,0},{1,5},{5,1},{2,6},{6,2},{3,7},{7,3},{8,12},{12,8},{9,1... | collective-permute-start | bytes 1572872 | tf_op jit(solution)/shard_map/ppermute | solution.py:401
  229.5 3.4 %collective-permute-start.4 = (bf16[80,128]{1,0:T(8,128)(2,1)}, bf16[80,128]{1,0:T(8,128)(2,1)}, u32[]{:S(2)}, u32[]{:S(2)}) collective-permute-start(bf16[80,128]{1,0:T(8,128)(2,1)} %shard_map.172.mine), channel_id=1, source_target_pairs={{0,4},{4,0},{1,5},{5,1},{2,6},{6,2},{3,7},{7,3},{8,12},{12,8},{9,1... | collective-permute-start | bytes 61448 | tf_op jit(solution)/shard_map/ppermute | solution.py:401
  230.4 12.5 %copy-start.2 = (bf16[6144,128]{1,0:T(8,128)(2,1)S(1)}, bf16[6144,128]{1,0:T(8,128)(2,1)}, u32[]{:S(2)}) copy-start(bf16[6144,128]{1,0:T(8,128)(2,1)} %copy-done.1) | copy-start | bytes 4718596
  230.4 12.5 %copy-start.4 = (bf16[128,2048]{1,0:T(8,128)(2,1)S(1)}, bf16[128,2048]{1,0:T(8,128)(2,1)}, u32[]{:S(2)}) copy-start(bf16[128,2048]{1,0:T(8,128)(2,1)} %get-tuple-element.22.normed) | copy-start | bytes 1572868
  232.9 0.8 copy-start.16
  234.4 1.0 copy-start.14
  235.4 0.9 copy-start.17
  239.4 0.8 copy-start.5
  240.2 7.6 %collective-permute-start.5 = (bf16[128,256]{1,0:T(8,128)(2,1)S(1)}, bf16[128,256]{1,0:T(8,128)(2,1)S(1)}, u32[]{:S(2)}, u32[]{:S(2)}) collective-permute-start(bf16[128,256]{1,0:T(8,128)(2,1)S(1)} %get-tuple-element.19), channel_id=1, source_target_pairs={{0,1},{1,2},{2,3},{3,0},{4,5},{5,6},{6,7},{7,4},{8,9},{9,10},{10,1... | collective-permute-start | bytes 196616 | tf_op jit(solution)/shard_map/ppermute | solution.py:401
  240.2 7.6 %collective-permute-start.6 = (bf16[128,256]{1,0:T(8,128)(2,1)S(1)}, bf16[128,256]{1,0:T(8,128)(2,1)S(1)}, u32[]{:S(2)}, u32[]{:S(2)}) collective-permute-start(bf16[128,256]{1,0:T(8,128)(2,1)S(1)} %get-tuple-element.20), channel_id=1, source_target_pairs={{0,3},{1,0},{2,1},{3,2},{4,7},{5,4},{6,5},{7,6},{8,11},{9,8},{10,9... | collective-permute-start | bytes 196616 | tf_op jit(solution)/shard_map/ppermute | solution.py:401
  242.9 4.9 %collective-permute-start.7 = (bf16[128,256]{1,0:T(8,128)(2,1)S(1)}, bf16[128,256]{1,0:T(8,128)(2,1)S(1)}, u32[]{:S(2)}, u32[]{:S(2)}) collective-permute-start(bf16[128,256]{1,0:T(8,128)(2,1)S(1)} %get-tuple-element.21), channel_id=1, source_target_pairs={{0,2},{1,3},{2,0},{3,1},{4,6},{5,7},{6,4},{7,5},{8,10},{9,11},{10,... | collective-permute-start | bytes 196616 | tf_op jit(solution)/shard_map/ppermute | solution.py:401
  242.9 4.9 %copy-start.6 = (bf16[128,2048]{1,0:T(8,128)(2,1)S(1)}, bf16[128,2048]{1,0:T(8,128)(2,1)}, u32[]{:S(2)}) copy-start(bf16[128,2048]{1,0:T(8,128)(2,1)} %copy-done.5) | copy-start | bytes 1572868
  242.9 4.9 %copy-start.13 = (f32[128,2]{1,0:T(8,128)S(1)}, f32[128,2]{1,0:T(8,128)}, u32[]{:S(2)}) copy-start(f32[128,2]{1,0:T(8,128)} %copy.18.weight) | copy-start | bytes 3076
  242.9 4.9 %copy-start.21 = (s32[2,128]{1,0:T(2,128)S(1)}, s32[2,128]{1,0:T(2,128)}, u32[]{:S(2)}) copy-start(s32[2,128]{1,0:T(2,128)} %get-tuple-element.14.places) | copy-start | bytes 3076

commit v3 on v2

--- a/solution.py
+++ b/solution.py
@@ -44,6 +44,34 @@
 
 def dot(a, b):
     return jnp.dot(a, b, preferred_element_type=F32)
+
+
+def swap_matrix():
+    side = TILE * TILE
+    row = lax.broadcasted_iota(jnp.int32, (side, side), 0)
+    col = lax.broadcasted_iota(jnp.int32, (side, side), 1)
+    hit = (row // TILE == col % TILE) & (row % TILE == col // TILE)
+    return jnp.where(hit, 1.0, 0.0).astype(BF16)
+
+
+def rows_to_tiles(swap, rows):
+    count = rows.shape[0] // TILE
+    width = rows.shape[1] // LANES
+    found = []
+    for at in range(0, count, 2):
+        pair = [
+            jnp.concatenate(
+                [
+                    rows[g * TILE : (g + 1) * TILE, k * LANES : (k + 1) * LANES]
+                    for k in range(width)
+                ],
+                axis=0,
+            )
+            for g in range(at, min(at + 2, count))
+        ]
+        out = dot(swap, jnp.concatenate(pair, axis=1)).astype(BF16)
+        found += [out[:, g * LANES : (g + 1) * LANES] for g in range(len(pair))]
+    return found
 
 
 def column(c):
@@ -107,7 +135,6 @@
     down_w,
     rows,
     arrived,
-    wide,
     out,
     sems,
     in_sems,
@@ -127,16 +154,23 @@
         for j in range(pieces):
             at = pl.ds(j * part, part)
             copies[i].append(pltpu.make_async_copy(src.at[0, at], dst.at[at], sems.at[i, j]))
-            copies[i][-1].start()
-    depth = share // TILE
-    for j in range(chunks):
-        landed[j].wait()
-        at = slice(j * share, (j + 1) * share)
-        wide[at, :] = arrived[at, :].astype(F32)
-        for c in range(TILE):
-            rows[j * depth : (j + 1) * depth, column(c)] = wide[
-                pl.ds(j * share + c, depth, stride=TILE), :
-            ].astype(BF16)
+    swap = swap_matrix()
+    side = TILE * TILE
+    groups = arrived.shape[0] // side
+    for at in range(0, groups, 2):
+        if at * side % share == 0:
+            landed[at * side // share].wait()
+            for copy in copies[at * side // share]:
+                copy.start()
+        pair = jnp.concatenate(
+            [arrived[g * side : (g + 1) * side, :] for g in (at, at + 1)], axis=1
+        )
+        turned = dot(swap, pair).astype(BF16)
+        for j in range(2):
+            for k in range(TILE):
+                rows[
+                    (at + j) * TILE : (at + j + 1) * TILE, k * LANES : (k + 1) * LANES
+                ] = turned[k * TILE : (k + 1) * TILE, j * LANES : (j + 1) * LANES]
     for copy in copies[0]:
         copy.wait()
     gated = jax.nn.silu(dot(rows[...], gate_w[...]))
@@ -145,15 +179,13 @@
     hidden = (gated * dot(rows[...], up_w[...])).astype(BF16)
     for copy in copies[2]:
         copy.wait()
-    count = rows.shape[0]
-    step = 4 * LANES
-    for at in range(0, down_w.shape[1], step):
-        result = dot(hidden, down_w[:, at : at + step])
-        for c in range(step // LANES):
-            wide[pl.ds(at // LANES + c, count, stride=TILE), :] = result[:, column(c)]
     left = []
+    step = rows.shape[0] // chunks
+    for at in range(0, down_w.shape[1], 4 * LANES):
+        rows[:, at : at + 4 * LANES] = dot(hidden, down_w[:, at : at + 4 * LANES]).astype(BF16)
     for j in range(chunks):
-        out[j * share : (j + 1) * share, :] = wide[j * share : (j + 1) * share, :].astype(BF16)
+        for g, tile in enumerate(rows_to_tiles(swap, rows[j * step : (j + 1) * step, :])):
+            out[j * share + g * side : j * share + (g + 1) * side, :] = tile
         at = pl.ds(j * share, share)
         left.append(pltpu.make_async_copy(out.at[at], out_hbm.at[at], out_sems.at[j]))
         left[-1].start()
@@ -451,16 +483,14 @@
         start = early if start is None else joined(start, early)
         whole = item if whole is None else joined(whole, item)
     before[...] = closed(start)
-    packed = closed(whole)
-    for p in range(window.shape[0] // STATE_ROWS):
-        window[p * STATE_ROWS : (p + 1) * STATE_ROWS, :] = packed
-
-
-def far_kernel(seat, before, window, prefix):
+    window[...] = closed(whole)
+
+
+def far_kernel(seat, before, *refs):
+    *far, prefix = refs
     start = None
-    for p in range(window.shape[0] // STATE_ROWS):
-        part = window[p * STATE_ROWS : (p + 1) * STATE_ROWS, :].astype(F32)
-        early = opened(jnp.where(seat[0] > p, part, 0.0))
+    for d in range(len(far), 0, -1):
+        early = opened(jnp.where(seat[0] >= d, far[d - 1][...].astype(F32), 0.0))
         start = early if start is None else joined(start, early)
     prefix[...] = closed(joined(start, opened(before[...])))
 
@@ -570,21 +600,13 @@
     chip = small(chip_kernel, packed_shape, [SMEM, VMEM, VMEM], VMEM)(core, own, other)
     low_seat = lax.axis_index("ep_lo").reshape(1).astype(jnp.int32)
     high_seat = lax.axis_index("ep_hi").reshape(1).astype(jnp.int32)
-    groups = lax.axis_size("ep_hi")
     near = [moved_by(chip, "ep_lo", d) for d in range(1, lax.axis_size("ep_lo"))]
-    window_shape = jax.ShapeDtypeStruct((groups * STATE_ROWS, value_size), BF16)
     before, window = small(
-        near_kernel, (packed_shape, window_shape), [SMEM] + [VMEM] * (1 + len(near)), (VMEM, VMEM)
+        near_kernel, (packed_shape, packed_shape), [SMEM] + [VMEM] * (1 + len(near)), (VMEM, VMEM)
     )(low_seat, chip, *near)
-    far = lax.all_to_all(
-        window.reshape(groups, STATE_ROWS, value_size),
-        "ep_hi",
-        split_axis=0,
-        concat_axis=0,
-        tiled=True,
-    )
-    prefix = small(far_kernel, packed_shape, [SMEM] + [VMEM] * 2, VMEM)(
-        high_seat, before, far.reshape(groups * STATE_ROWS, value_size)
+    far = [moved_by(window, "ep_hi", d) for d in range(1, lax.axis_size("ep_hi"))]
+    prefix = small(far_kernel, packed_shape, [SMEM] + [VMEM] * (1 + len(far)), VMEM)(
+        high_seat, before, *far
     )
     swapped = moved_by(prefix, "ep_1", 1)
     state_in = small(
@@ -641,7 +663,6 @@
             pltpu.VMEM((hidden_size, width), BF16),
             pltpu.VMEM((slots, width), BF16),
             pltpu.VMEM((tile_rows, LANES), BF16),
-            pltpu.VMEM((tile_rows, LANES), F32),
             pltpu.VMEM((tile_rows, LANES), BF16),
             pltpu.SemaphoreType.DMA((3, pieces)),
             pltpu.SemaphoreType.DMA((chunks,)),

time: 253 us -> 280 us (1.11)
  blocking collectives: 0 us -> 107 us
  waiting for transfers between devices: 138 us -> 87.9 us
  starting transfers between devices: 72.2 us -> 46.7 us
  local copies, waits for them, and re-layouts: 11.6 us -> 8.33 us
    all_to_all x0 -> x1, blocking collectives: none -> 107 us  [per_device(): lax.all_to_all(outbound.reshape(experts, capacity * TILE, LANES), EP_TP,...]
    ppermute x14 -> x17, waiting for transfers between devices: 59.9 us -> 22.1 us  [moved_by(): lax.ppermute(array, axis, [(s, (s + step) % count) for s in range(count)])]
    all_to_all x2 -> x0, starting transfers between devices: 36.7 us -> none  [the longest x1 31.1 us: per_device(): lax.all_to_all(outbound.reshape(experts, capacity * TILE, LANES), EP_TP,...]
    ppermute x14 -> x17, starting transfers between devices: 17.4 us -> 34.1 us  [moved_by(): lax.ppermute(array, axis, [(s, (s + step) % count) for s in range(count)])]
    all_to_all x2 -> x0, waiting for transfers between devices: 12.6 us -> none  [the longest x1 8.37 us: per_device(): lax.all_to_all(outbound.reshape(experts, capacity * TILE, LANES), EP_TP,...]
    all_to_all x1, starting transfers between devices: 14.8 us -> 9.48 us  [per_device(): lax.all_to_all(answers.reshape(experts, capacity * TILE, LANES), EP_TP, s...]
    unnamed x49 -> x39, local copies, waits for them, and re-layouts: 11.5 us -> 8.24 us
  transfers between devices with their start and end apart: 19 -> 20, of which waited for: 9 -> 10; matrix products, arithmetic and copies ran while one was open for 1% -> 1% of each run, Pallas kernels for 8% -> 4%
where the time goes in v3:
time: 280 us; the launch traced here: 279 us
  blocking collectives  107 us (38%)
  waiting for transfers between devices  87.9 us (31%)
  starting transfers between devices  46.7 us (17%)
  Pallas kernels  27.1 us (10%)
  local copies, waits for them, and re-layouts  8.33 us (3%)
    all_to_all x1, blocking collectives, per_device(): lax.all_to_all(outbound.reshape(experts, capacity * TILE, LANES), EP_TP,...  107 us
    ppermute x2, waiting for transfers between devices, outward(): return lax.ppermute(array, ('ep_1', 'tp'), pairs)  65.8 us
    ppermute x17, starting transfers between devices, moved_by(): lax.ppermute(array, axis, [(s, (s + step) % count) for s in range(count)])  34.1 us
    ppermute x17, waiting for transfers between devices, moved_by(): lax.ppermute(array, axis, [(s, (s + step) % count) for s in range(count)])  22.1 us
    all_to_all x1, starting transfers between devices, per_device(): lax.all_to_all(answers.reshape(experts, capacity * TILE, LANES), EP_TP, s...  9.48 us
    unnamed x39, local copies, waits for them, and re-layouts  8.24 us
    pallas_call x1, Pallas kernels, per_device(): call(expert_kernel, jax.ShapeDtypeStruct((tile_rows, LANES), BF16), [HBM]...  7.13 us
  transfers between devices with their start and end apart: 20, of which 10 were waited for; matrix products, arithmetic and copies ran while one was open for 1% of the time, Pallas kernels for 4%

profile of v3, /device:TPU:33, one launch (start us, length us, event | category | flops | bytes accessed | tf_op | source)
XLA Modules:
  0.0 279.1 jit_solution(11659702096412255405)
XLA Ops:
  0.6 4.6 %shard_map.167 = (bf16[128,2048]{1,0:T(8,128)(2,1)}, bf16[6144,128]{1,0:T(8,128)(2,1)}, s32[2,128]{1,0:T(2,128)}) custom-call(s32[2,128]{1,0:T(2,128)} %bitcast.18, bf16[128,2048]{1,0:T(8,128)(2,1)} %x_hbm.1, f32[1,2048]{1,0:T(1,128)} %bitcast.17), custom_call_target="tpu_custom_call" | custom-call | flops 134217728 | bytes 1048576 | tf_op jit(solution)/shard_map/pallas_call | solution.py:552
  5.2 107.0 %all_to_all.10 = bf16[128,48,128]{2,1,0:T(8,128)(2,1)} all-to-all(bf16[128,48,128]{2,1,0:T(8,128)(2,1)} %bitcast.16), channel_id=1, replica_groups=mesh['grp'=2,'ep_hi'=4,'ep_lo'=4,'ep_1'=2,'tp'=4] {'ep_hi','ep_lo','ep_1..., dimensions={0} | all-to-all | bytes 3145728 | tf_op jit(solution)/shard_map/all_to_all | solution.py:574
  112.2 7.1 %shard_map.168 = bf16[6144,128]{1,0:T(8,128)(2,1)} custom-call(bf16[6144,128]{1,0:T(8,128)(2,1)} %bitcast.15, bf16[1,2048,512]{2,1,0:T(8,128)(2,1)} %gate_hbm.1, bf16[1,2048,512]{2,1,0:T(8,128)(2,1)} %up_hbm.1, bf16[1,512,2048]{2,1,0:T(8,128)(2,1)} %down_hbm.1), custom_call_target="tpu_custom_call" | custom-call | flops 2415919104 | bytes 6291456 | tf_op jit(solution)/shard_map/pallas_call | solution.py:655
  119.4 0.0 copy-start.7
  119.4 9.5 %all-to-all-start.1 = ((bf16[128,48,128]{2,1,0:T(8,128)(2,1)}), bf16[128,48,128]{2,1,0:T(8,128)(2,1)S(1)}, u32[]{:S(2)}, u32[]{:S(2)}) async-start(bf16[128,48,128]{2,1,0:T(8,128)(2,1)} %bitcast.14), calls=%async_computation.1 | async-start | bytes 3145728 | tf_op jit(solution)/shard_map/all_to_all | solution.py:675
  128.9 1.0 copy-done.8
  130.0 1.0 copy-done.9
  131.0 1.1 shard_map.175
  132.1 2.6 collective-permute-start.11
  134.6 1.2 copy-done.1
  135.8 0.6 collective-permute-start.15
  136.4 0.1 collective-permute-start.13
  136.5 31.9 %collective-permute-done.11.near = bf16[6144,128]{1,0:T(8,128)(2,1)} collective-permute-done((bf16[6144,128]{1,0:T(8,128)(2,1)S(1)}, bf16[6144,128]{1,0:T(8,128)(2,1)}, u32[]{:S(2)}, u32[]{:S(2)}) %collective-permute-start.11) | collective-permute-done | bytes 1572896 | tf_op jit(solution)/shard_map/ppermute | solution.py:440
  168.4 3.6 %collective-permute-start.12 = (bf16[6144,128]{1,0:T(8,128)(2,1)}, bf16[6144,128]{1,0:T(8,128)(2,1)}, u32[]{:S(2)}, u32[]{:S(2)}) collective-permute-start(bf16[6144,128]{1,0:T(8,128)(2,1)} %collective-permute-done.11.near), channel_id=1, source_target_pairs={{0,4},{4,0},{1,5},{5,1},{2,6},{6,2},{3,7},{7,3},{8,12},{12,8},{9,1... | collective-permute-start | bytes 4718600 | tf_op jit(solution)/shard_map/ppermute | solution.py:433
  172.1 33.9 %collective-permute-done.15.near_hbm = bf16[256,2048]{1,0:T(8,128)(2,1)} collective-permute-done((bf16[256,2048]{1,0:T(8,128)(2,1)S(1)}, bf16[256,2048]{1,0:T(8,128)(2,1)}, u32[]{:S(2)}, u32[]{:S(2)}) %collective-permute-start.15) | collective-permute-done | bytes 1048608 | tf_op jit(solution)/shard_map/ppermute | solution.py:440
  205.9 4.1 %collective-permute-start.16 = (bf16[256,2048]{1,0:T(8,128)(2,1)}, bf16[256,2048]{1,0:T(8,128)(2,1)}, u32[]{:S(2)}, u32[]{:S(2)}) collective-permute-start(bf16[256,2048]{1,0:T(8,128)(2,1)} %collective-permute-done.15.near_hbm), channel_id=1, source_target_pairs={{0,4},{4,0},{1,5},{5,1},{2,6},{6,2},{3,7},{7,3},{8,12},{12,8},{9,1... | collective-permute-start | bytes 3145736 | tf_op jit(solution)/shard_map/ppermute | solution.py:433
  210.1 0.1 mul.28
  210.2 0.6 collective-permute-start.18
  210.8 1.0 multiply_sine_fusion
  211.8 0.8 shard_map.169.own
  212.7 0.2 collective-permute-start
  212.8 1.8 collective-permute-done.other
  214.6 0.6 copy-done.13
  215.2 4.4 %collective-permute-done.1.refs_0_ = bf16[80,128]{1,0:T(8,128)(2,1)S(1)} collective-permute-done((bf16[80,128]{1,0:T(8,128)(2,1)S(1)}, bf16[80,128]{1,0:T(8,128)(2,1)S(1)}, u32[]{:S(2)}, u32[]{:S(2)}) %collective-permute-start.1) | collective-permute-done | bytes 20512 | tf_op jit(solution)/shard_map/ppermute | solution.py:433
  219.6 3.5 %collective-permute-done.2.refs_1_ = bf16[80,128]{1,0:T(8,128)(2,1)S(1)} collective-permute-done((bf16[80,128]{1,0:T(8,128)(2,1)S(1)}, bf16[80,128]{1,0:T(8,128)(2,1)S(1)}, u32[]{:S(2)}, u32[]{:S(2)}) %collective-permute-start.2) | collective-permute-done | bytes 20512 | tf_op jit(solution)/shard_map/ppermute | solution.py:433
  223.2 2.6 collective-permute-done.3.refs_2_
  225.8 0.1 shard_map.171
  225.9 3.4 %collective-permute-start.4 = (bf16[80,128]{1,0:T(8,128)(2,1)S(1)}, bf16[80,128]{1,0:T(8,128)(2,1)S(1)}, u32[]{:S(2)}, u32[]{:S(2)}) collective-permute-start(bf16[80,128]{1,0:T(8,128)(2,1)S(1)} %get-tuple-element.17), channel_id=1, source_target_pairs={{0,32},{32,64},{64,96},{96,0},{1,33},{33,65},{65,97},{97,1},{2,34}... | collective-permute-start | bytes 61448 | tf_op jit(solution)/shard_map/ppermute | solution.py:433
  229.3 3.3 %collective-permute-done.4.refs_0_ = bf16[80,128]{1,0:T(8,128)(2,1)S(1)} collective-permute-done((bf16[80,128]{1,0:T(8,128)(2,1)S(1)}, bf16[80,128]{1,0:T(8,128)(2,1)S(1)}, u32[]{:S(2)}, u32[]{:S(2)}) %collective-permute-start.4) | collective-permute-done | bytes 20512 | tf_op jit(solution)/shard_map/ppermute | solution.py:433
  232.5 7.9 %collective-permute-start.5 = (bf16[80,128]{1,0:T(8,128)(2,1)S(1)}, bf16[80,128]{1,0:T(8,128)(2,1)S(1)}, u32[]{:S(2)}, u32[]{:S(2)}) collective-permute-start(bf16[80,128]{1,0:T(8,128)(2,1)S(1)} %get-tuple-element.17), channel_id=1, source_target_pairs={{0,64},{32,96},{64,0},{96,32},{1,65},{33,97},{65,1},{97,33},{2,66}... | collective-permute-start | bytes 61448 | tf_op jit(solution)/shard_map/ppermute | solution.py:433
  240.5 3.4 %collective-permute-done.5.refs_1_ = bf16[80,128]{1,0:T(8,128)(2,1)S(1)} collective-permute-done((bf16[80,128]{1,0:T(8,128)(2,1)S(1)}, bf16[80,128]{1,0:T(8,128)(2,1)S(1)}, u32[]{:S(2)}, u32[]{:S(2)}) %collective-permute-start.5) | collective-permute-done | bytes 20512 | tf_op jit(solution)/shard_map/ppermute | solution.py:433
  243.9 3.9 %collective-permute-start.6 = (bf16[80,128]{1,0:T(8,128)(2,1)S(1)}, bf16[80,128]{1,0:T(8,128)(2,1)S(1)}, u32[]{:S(2)}, u32[]{:S(2)}) collective-permute-start(bf16[80,128]{1,0:T(8,128)(2,1)S(1)} %get-tuple-element.17), channel_id=1, source_target_pairs={{0,96},{32,0},{64,32},{96,64},{1,97},{33,1},{65,33},{97,65},{2,98}... | collective-permute-start | bytes 61448 | tf_op jit(solution)/shard_map/ppermute | solution.py:433
  247.8 2.6 collective-permute-done.6.refs_2_
  250.4 0.6 shard_map.172.mine
  251.0 7.5 %collective-permute-start.7 = (bf16[80,128]{1,0:T(8,128)(2,1)}, bf16[80,128]{1,0:T(8,128)(2,1)}, u32[]{:S(2)}, u32[]{:S(2)}) collective-permute-start(bf16[80,128]{1,0:T(8,128)(2,1)} %shard_map.172.mine), channel_id=1, source_target_pairs={{0,4},{4,0},{1,5},{5,1},{2,6},{6,2},{3,7},{7,3},{8,12},{12,8},{9,1... | collective-permute-start | bytes 61448 | tf_op jit(solution)/shard_map/ppermute | solution.py:433
  258.5 0.7 copy.18.weight
  259.3 0.4 collective-permute-done.7.theirs
  259.7 1.0 copy-done.14
  260.7 0.8 shard_map.173.state_in
  261.5 0.0 copy-start.12
  261.5 0.9 copy-done.12
  262.4 0.9 copy-done.15
  263.3 3.1 %shard_map.174 = (bf16[128,2048]{1,0:T(8,128)(2,1)S(1)}, bf16[128,256]{1,0:T(8,128)(2,1)S(1)}, bf16[128,256]{1,0:T(8,128)(2,1)S(1)}, bf16[128,256]{1,0:T(8,128)(2,1)S(1)}) custom-call(s32[1]{0:T(128)} %bitcast.7.seat, bf16[512,128]{1,0:T(8,128)(2,1)S(1)} %copy-done.15, bf16[512,128]{1,0:T(8,128)(2,1)S(1)} %copy-done.10, bf16[512,256]{1,0:T(8,128)(2,1)S(1)} %copy-done.3, ...), custom_call_target="tpu_custom_call" | custom-call | flops 262144000 | bytes 5242880 | tf_op jit(solution)/shard_map/pallas_call | solution.py:684
  266.5 0.8 copy-done.5
  267.3 0.4 collective-permute-start.8
  267.6 2.3 collective-permute-start.9
  270.0 4.8 %shard_map.176.shared_hbm = f32[128,2048]{1,0:T(8,128)S(1)} custom-call(s32[1]{0:T(128)} %bitcast.2.core, bf16[128,2048]{1,0:T(8,128)(2,1)S(1)} %copy-done.4, bf16[6144,128]{1,0:T(8,128)(2,1)S(1)} %copy-done.2, bf16[6144,128]{1,0:T(8,128)(2,1)} %collective-permute-done.11.near, bf16[6144,128]{1,0:T(8,128)(2,1)} %collective-permute-done.12.near_other, ...), custom_call_target="tpu_custom_call" | custom-call | flops 805306368 | bytes 5242880 | tf_op jit(solution)/shard_map/pallas_call | solution.py:640
  274.9 4.0 %shard_map.177 = (bf16[128,2048]{1,0:T(8,128)(2,1)}, bf16[128,2048]{1,0:T(8,128)(2,1)}) custom-call(s32[2,128]{1,0:T(2,128)S(1)} %copy-done.17, s32[1]{0:T(128)} %bitcast.2.core, bf16[6144,128]{1,0:T(8,128)(2,1)S(1)} %bitcast.11, f32[128,2]{1,0:T(8,128)S(1)} %copy-done.11, bf16[128,2048]{1,0:T(8,128)(2,1)S(1)} %copy-done.6, ...), custom_call_target="tpu_custom_call" | custom-call | flops 786432000 | bytes 5242880 | tf_op jit(solution)/shard_map/pallas_call | solution.py:696
  (48 shorter events, 0.1 us)
Async XLA Ops:
  119.4 9.5 %copy-start = (bf16[256,2048]{1,0:T(8,128)(2,1)S(1)}, bf16[256,2048]{1,0:T(8,128)(2,1)}, u32[]{:S(2)}) copy-start(bf16[256,2048]{1,0:T(8,128)(2,1)} %w_out.3) | copy-start | bytes 3145732
  119.4 9.5 %copy-start.7 = (bf16[2048,128]{1,0:T(8,128)(2,1)S(1)}, bf16[2048,128]{1,0:T(8,128)(2,1)}, u32[]{:S(2)}) copy-start(bf16[2048,128]{1,0:T(8,128)(2,1)} %gate_w.1) | copy-start | bytes 1572868
  119.4 155.5 %all-to-all-start.1 = ((bf16[128,48,128]{2,1,0:T(8,128)(2,1)}), bf16[128,48,128]{2,1,0:T(8,128)(2,1)S(1)}, u32[]{:S(2)}, u32[]{:S(2)}) async-start(bf16[128,48,128]{2,1,0:T(8,128)(2,1)} %bitcast.14), calls=%async_computation.1 | async-start | bytes 3145728 | tf_op jit(solution)/shard_map/all_to_all | solution.py:675
  128.9 1.0 copy-start.8
  130.0 1.0 copy-start.9
  131.0 80.8 %copy-start.3 = (bf16[512,256]{1,0:T(8,128)(2,1)S(1)}, bf16[512,256]{1,0:T(8,128)(2,1)}, u32[]{:S(2)}) copy-start(bf16[512,256]{1,0:T(8,128)(2,1)} %v.3) | copy-start | bytes 786436
  131.0 80.8 %copy-start.10 = (bf16[512,128]{1,0:T(8,128)(2,1)S(1)}, bf16[512,128]{1,0:T(8,128)(2,1)}, u32[]{:S(2)}) copy-start(bf16[512,128]{1,0:T(8,128)(2,1)} %k.3) | copy-start | bytes 393220
  131.0 80.8 %copy-start.16 = (f32[512,2]{0,1:T(2,128)S(1)}, f32[512,2]{0,1:T(2,128)}, u32[]{:S(2)}) copy-start(f32[512,2]{0,1:T(2,128)} %param.20) | copy-start | bytes 12292
  131.0 127.5 %copy-start.18 = (f32[128,2]{0,1:T(2,128)S(1)}, f32[128,2]{0,1:T(2,128)}, u32[]{:S(2)}) copy-start(f32[128,2]{0,1:T(2,128)} %param.25) | copy-start | bytes 3076
  132.1 36.4 %collective-permute-start.11 = (bf16[6144,128]{1,0:T(8,128)(2,1)S(1)}, bf16[6144,128]{1,0:T(8,128)(2,1)}, u32[]{:S(2)}, u32[]{:S(2)}) collective-permute-start(bf16[6144,128]{1,0:T(8,128)(2,1)S(1)} %get-tuple-element.23.own), channel_id=1, source_target_pairs={{0,1},{1,2},{2,3},{3,0},{4,7},{5,4},{6,5},{7,6},{8,9},{9,10},{10,1... | collective-permute-start | bytes 4718600 | tf_op jit(solution)/shard_map/ppermute | solution.py:440
  134.6 1.2 copy-start.1
  135.8 70.1 %collective-permute-start.15 = (bf16[256,2048]{1,0:T(8,128)(2,1)S(1)}, bf16[256,2048]{1,0:T(8,128)(2,1)}, u32[]{:S(2)}, u32[]{:S(2)}) collective-permute-start(bf16[256,2048]{1,0:T(8,128)(2,1)S(1)} %copy-done), channel_id=1, source_target_pairs={{0,1},{1,2},{2,3},{3,0},{4,7},{5,4},{6,5},{7,6},{8,9},{9,10},{10,1... | collective-permute-start | bytes 3145736 | tf_op jit(solution)/shard_map/ppermute | solution.py:440
  136.4 73.7 %collective-permute-start.13 = (bf16[3072,128]{1,0:T(8,128)(2,1)S(1)}, bf16[3072,128]{1,0:T(8,128)(2,1)}, u32[]{:S(2)}, u32[]{:S(2)}) collective-permute-start(bf16[3072,128]{1,0:T(8,128)(2,1)S(1)} %get-tuple-element.24), channel_id=1, source_target_pairs={{0,2},{1,3},{2,0},{3,1},{4,6},{5,7},{6,4},{7,5},{8,10},{9,11},{10,... | collective-permute-start | bytes 2359304 | tf_op jit(solution)/shard_map/ppermute | solution.py:433
  168.4 99.2 %collective-permute-start.12 = (bf16[6144,128]{1,0:T(8,128)(2,1)}, bf16[6144,128]{1,0:T(8,128)(2,1)}, u32[]{:S(2)}, u32[]{:S(2)}) collective-permute-start(bf16[6144,128]{1,0:T(8,128)(2,1)} %collective-permute-done.11.near), channel_id=1, source_target_pairs={{0,4},{4,0},{1,5},{5,1},{2,6},{6,2},{3,7},{7,3},{8,12},{12,8},{9,1... | collective-permute-start | bytes 4718600 | tf_op jit(solution)/shard_map/ppermute | solution.py:433
  172.1 38.1 %collective-permute-start.17 = (bf16[128,2048]{1,0:T(8,128)(2,1)}, bf16[128,2048]{1,0:T(8,128)(2,1)}, u32[]{:S(2)}, u32[]{:S(2)}) collective-permute-start(bf16[128,2048]{1,0:T(8,128)(2,1)} %get-tuple-element.25), channel_id=1, source_target_pairs={{0,2},{1,3},{2,0},{3,1},{4,6},{5,7},{6,4},{7,5},{8,10},{9,11},{10,... | collective-permute-start | bytes 1572872 | tf_op jit(solution)/shard_map/ppermute | solution.py:433
  205.9 68.9 %collective-permute-start.16 = (bf16[256,2048]{1,0:T(8,128)(2,1)}, bf16[256,2048]{1,0:T(8,128)(2,1)}, u32[]{:S(2)}, u32[]{:S(2)}) collective-permute-start(bf16[256,2048]{1,0:T(8,128)(2,1)} %collective-permute-done.15.near_hbm), channel_id=1, source_target_pairs={{0,4},{4,0},{1,5},{5,1},{2,6},{6,2},{3,7},{7,3},{8,12},{12,8},{9,1... | collective-permute-start | bytes 3145736 | tf_op jit(solution)/shard_map/ppermute | solution.py:433
  210.1 57.2 %collective-permute-start.14 = (bf16[3072,128]{1,0:T(8,128)(2,1)}, bf16[3072,128]{1,0:T(8,128)(2,1)}, u32[]{:S(2)}, u32[]{:S(2)}) collective-permute-start(bf16[3072,128]{1,0:T(8,128)(2,1)} %collective-permute-done.13.mine), channel_id=1, source_target_pairs={{0,4},{4,0},{1,5},{5,1},{2,6},{6,2},{3,7},{7,3},{8,12},{12,8},{9,1... | collective-permute-start | bytes 2359304 | tf_op jit(solution)/shard_map/ppermute | solution.py:433
  210.2 64.7 %collective-permute-start.18 = (bf16[128,2048]{1,0:T(8,128)(2,1)}, bf16[128,2048]{1,0:T(8,128)(2,1)}, u32[]{:S(2)}, u32[]{:S(2)}) collective-permute-start(bf16[128,2048]{1,0:T(8,128)(2,1)} %collective-permute-done.17.mine_hbm), channel_id=1, source_target_pairs={{0,4},{4,0},{1,5},{5,1},{2,6},{6,2},{3,7},{7,3},{8,12},{12,8},{9,1... | collective-permute-start | bytes 1572872 | tf_op jit(solution)/shard_map/ppermute | solution.py:433
  212.7 1.9 collective-permute-start
  214.6 0.6 copy-start.13
  215.2 4.4 %collective-permute-start.1 = (bf16[80,128]{1,0:T(8,128)(2,1)S(1)}, bf16[80,128]{1,0:T(8,128)(2,1)S(1)}, u32[]{:S(2)}, u32[]{:S(2)}) collective-permute-start(bf16[80,128]{1,0:T(8,128)(2,1)S(1)} %shard_map.170.chip), channel_id=1, source_target_pairs={{0,8},{8,16},{16,24},{24,0},{1,9},{9,17},{17,25},{25,1},{2,10},{10... | collective-permute-start | bytes 61448 | tf_op jit(solution)/shard_map/ppermute | solution.py:433
  219.6 3.5 %collective-permute-start.2 = (bf16[80,128]{1,0:T(8,128)(2,1)S(1)}, bf16[80,128]{1,0:T(8,128)(2,1)S(1)}, u32[]{:S(2)}, u32[]{:S(2)}) collective-permute-start(bf16[80,128]{1,0:T(8,128)(2,1)S(1)} %shard_map.170.chip), channel_id=1, source_target_pairs={{0,16},{8,24},{16,0},{24,8},{1,17},{9,25},{17,1},{25,9},{2,18},{10... | collective-permute-start | bytes 61448 | tf_op jit(solution)/shard_map/ppermute | solution.py:433
  223.2 2.6 collective-permute-start.3
  225.9 6.7 %collective-permute-start.4 = (bf16[80,128]{1,0:T(8,128)(2,1)S(1)}, bf16[80,128]{1,0:T(8,128)(2,1)S(1)}, u32[]{:S(2)}, u32[]{:S(2)}) collective-permute-start(bf16[80,128]{1,0:T(8,128)(2,1)S(1)} %get-tuple-element.17), channel_id=1, source_target_pairs={{0,32},{32,64},{64,96},{96,0},{1,33},{33,65},{65,97},{97,1},{2,34}... | collective-permute-start | bytes 61448 | tf_op jit(solution)/shard_map/ppermute | solution.py:433
  232.5 11.3 %collective-permute-start.5 = (bf16[80,128]{1,0:T(8,128)(2,1)S(1)}, bf16[80,128]{1,0:T(8,128)(2,1)S(1)}, u32[]{:S(2)}, u32[]{:S(2)}) collective-permute-start(bf16[80,128]{1,0:T(8,128)(2,1)S(1)} %get-tuple-element.17), channel_id=1, source_target_pairs={{0,64},{32,96},{64,0},{96,32},{1,65},{33,97},{65,1},{97,33},{2,66}... | collective-permute-start | bytes 61448 | tf_op jit(solution)/shard_map/ppermute | solution.py:433
  243.9 6.5 %collective-permute-start.6 = (bf16[80,128]{1,0:T(8,128)(2,1)S(1)}, bf16[80,128]{1,0:T(8,128)(2,1)S(1)}, u32[]{:S(2)}, u32[]{:S(2)}) collective-permute-start(bf16[80,128]{1,0:T(8,128)(2,1)S(1)} %get-tuple-element.17), channel_id=1, source_target_pairs={{0,96},{32,0},{64,32},{96,64},{1,97},{33,1},{65,33},{97,65},{2,98}... | collective-permute-start | bytes 61448 | tf_op jit(solution)/shard_map/ppermute | solution.py:433
  251.0 8.7 %collective-permute-start.7 = (bf16[80,128]{1,0:T(8,128)(2,1)}, bf16[80,128]{1,0:T(8,128)(2,1)}, u32[]{:S(2)}, u32[]{:S(2)}) collective-permute-start(bf16[80,128]{1,0:T(8,128)(2,1)} %shard_map.172.mine), channel_id=1, source_target_pairs={{0,4},{4,0},{1,5},{5,1},{2,6},{6,2},{3,7},{7,3},{8,12},{12,8},{9,1... | collective-permute-start | bytes 61448 | tf_op jit(solution)/shard_map/ppermute | solution.py:433
  259.3 10.7 %copy-start.2 = (bf16[6144,128]{1,0:T(8,128)(2,1)S(1)}, bf16[6144,128]{1,0:T(8,128)(2,1)}, u32[]{:S(2)}) copy-start(bf16[6144,128]{1,0:T(8,128)(2,1)} %copy-done.1) | copy-start | bytes 4718596
  259.3 10.7 %copy-start.4 = (bf16[128,2048]{1,0:T(8,128)(2,1)S(1)}, bf16[128,2048]{1,0:T(8,128)(2,1)}, u32[]{:S(2)}) copy-start(bf16[128,2048]{1,0:T(8,128)(2,1)} %get-tuple-element.22.normed) | copy-start | bytes 1572868
  259.7 1.0 copy-start.14
  261.5 1.0 copy-start.12
  262.4 0.9 copy-start.15
  266.5 0.8 copy-start.5
  267.3 7.6 %collective-permute-start.10 = (bf16[128,256]{1,0:T(8,128)(2,1)S(1)}, bf16[128,256]{1,0:T(8,128)(2,1)S(1)}, u32[]{:S(2)}, u32[]{:S(2)}) collective-permute-start(bf16[128,256]{1,0:T(8,128)(2,1)S(1)} %get-tuple-element.21), channel_id=1, source_target_pairs={{0,2},{1,3},{2,0},{3,1},{4,6},{5,7},{6,4},{7,5},{8,10},{9,11},{10,... | collective-permute-start | bytes 196616 | tf_op jit(solution)/shard_map/ppermute | solution.py:433
  267.3 7.6 %collective-permute-start.8 = (bf16[128,256]{1,0:T(8,128)(2,1)S(1)}, bf16[128,256]{1,0:T(8,128)(2,1)S(1)}, u32[]{:S(2)}, u32[]{:S(2)}) collective-permute-start(bf16[128,256]{1,0:T(8,128)(2,1)S(1)} %get-tuple-element.19), channel_id=1, source_target_pairs={{0,1},{1,2},{2,3},{3,0},{4,5},{5,6},{6,7},{7,4},{8,9},{9,10},{10,1... | collective-permute-start | bytes 196616 | tf_op jit(solution)/shard_map/ppermute | solution.py:433
  267.6 7.2 %collective-permute-start.9 = (bf16[128,256]{1,0:T(8,128)(2,1)S(1)}, bf16[128,256]{1,0:T(8,128)(2,1)S(1)}, u32[]{:S(2)}, u32[]{:S(2)}) collective-permute-start(bf16[128,256]{1,0:T(8,128)(2,1)S(1)} %get-tuple-element.20), channel_id=1, source_target_pairs={{0,3},{1,0},{2,1},{3,2},{4,7},{5,4},{6,5},{7,6},{8,11},{9,8},{10,9... | collective-permute-start | bytes 196616 | tf_op jit(solution)/shard_map/ppermute | solution.py:433
  270.0 4.9 %copy-start.6 = (bf16[128,2048]{1,0:T(8,128)(2,1)S(1)}, bf16[128,2048]{1,0:T(8,128)(2,1)}, u32[]{:S(2)}) copy-start(bf16[128,2048]{1,0:T(8,128)(2,1)} %copy-done.5) | copy-start | bytes 1572868
  270.0 4.9 %copy-start.11 = (f32[128,2]{1,0:T(8,128)S(1)}, f32[128,2]{1,0:T(8,128)}, u32[]{:S(2)}) copy-start(f32[128,2]{1,0:T(8,128)} %copy.18.weight) | copy-start | bytes 3076
  270.0 4.9 %copy-start.17 = (s32[2,128]{1,0:T(2,128)S(1)}, s32[2,128]{1,0:T(2,128)}, u32[]{:S(2)}) copy-start(s32[2,128]{1,0:T(2,128)} %get-tuple-element.14.places) | copy-start | bytes 3076

commit v4 on v3

--- a/solution.py
+++ b/solution.py
@@ -10,7 +10,7 @@
 BLOCK = 128
 LANES = 128
 TILE = 16
-CHIPS = 4
+CHIPS = 2
 EP = ("ep_hi", "ep_lo", "ep_1")
 EP_TP = EP + ("tp",)
 GRP_EP = ("grp",) + EP
@@ -227,7 +227,13 @@
     return out
 
 
-def state_kernel(k, v, log_decay, cosine, sine, packed):
+def state_kernel(k_hbm, v_hbm, decay_hbm, cosine, sine, packed, k, v, log_decay, sems):
+    pairs = ((decay_hbm, log_decay), (k_hbm, k), (v_hbm, v))
+    copies = [pltpu.make_async_copy(a, b, sems.at[i]) for i, (a, b) in enumerate(pairs)]
+    for copy in copies:
+        copy.start()
+    for copy in copies:
+        copy.wait()
     heads = log_decay.shape[0]
     key_size = k.shape[1] // heads
     value_size = v.shape[1] // heads
@@ -589,12 +595,17 @@
     own = call(
         state_kernel,
         jax.ShapeDtypeStruct((heads * STATE_ROWS, value_size), BF16),
-        [VMEM] * 5,
+        [HBM] * 3 + [VMEM] * 2,
         VMEM,
-        [],
+        [
+            pltpu.VMEM(keys.shape, BF16),
+            pltpu.VMEM(values.shape, BF16),
+            pltpu.VMEM((heads, span), F32),
+            pltpu.SemaphoreType.DMA((3,)),
+        ],
         2 * span * LANES * 512,
         4 * span * LANES * 4,
-        12,
+        61,
     )(keys, values, log_decay.T, cosine, sine)
     other = moved_by(own, "ep_1", 1)
     chip = small(chip_kernel, packed_shape, [SMEM, VMEM, VMEM], VMEM)(core, own, other)

time: 280 us -> 305 us (1.089)
  starting transfers between devices: 46.7 us -> 62.4 us
  waiting for transfers between devices: 87.9 us -> 92.8 us
    ppermute x17 -> x19, starting transfers between devices: 34.1 us -> 49.7 us  [moved_by(): lax.ppermute(array, axis, [(s, (s + step) % count) for s in range(count)])]
    ppermute x17 -> x19, waiting for transfers between devices: 22.1 us -> 27.9 us  [moved_by(): lax.ppermute(array, axis, [(s, (s + step) % count) for s in range(count)])]
  transfers between devices with their start and end apart: 20 -> 22, of which waited for: 10 -> 12; matrix products, arithmetic and copies ran while one was open for 1% -> 1% of each run, Pallas kernels for 4% -> 4%
where the time goes in v4:
time: 305 us; the launch traced here: 304 us
  blocking collectives  107 us (35%)
  waiting for transfers between devices  92.8 us (30%)
  starting transfers between devices  62.4 us (20%)
  Pallas kernels  28.4 us (9%)
  local copies, waits for them, and re-layouts  10.9 us (4%)
    all_to_all x1, blocking collectives, per_device(): lax.all_to_all(outbound.reshape(experts, capacity * TILE, LANES), EP_TP,...  107 us
    ppermute x2, waiting for transfers between devices, outward(): return lax.ppermute(array, ('ep_1', 'tp'), pairs)  64.9 us
    ppermute x19, starting transfers between devices, moved_by(): lax.ppermute(array, axis, [(s, (s + step) % count) for s in range(count)])  49.7 us
    ppermute x19, waiting for transfers between devices, moved_by(): lax.ppermute(array, axis, [(s, (s + step) % count) for s in range(count)])  27.9 us
    unnamed x39, local copies, waits for them, and re-layouts  10.8 us
    all_to_all x1, starting transfers between devices, per_device(): lax.all_to_all(answers.reshape(experts, capacity * TILE, LANES), EP_TP, s...  9.48 us
    pallas_call x1, Pallas kernels, per_device(): call(expert_kernel, jax.ShapeDtypeStruct((tile_rows, LANES), BF16), [HBM]...  7.14 us
  transfers between devices with their start and end apart: 22, of which 12 were waited for; matrix products, arithmetic and copies ran while one was open for 1% of the time, Pallas kernels for 4%

profile of v4, /device:TPU:33, one launch (start us, length us, event | category | flops | bytes accessed | tf_op | source)
XLA Modules:
  0.0 304.3 jit_solution(4203588156269350877)
XLA Ops:
  0.6 4.6 %shard_map.167 = (bf16[128,2048]{1,0:T(8,128)(2,1)}, bf16[6144,128]{1,0:T(8,128)(2,1)}, s32[2,128]{1,0:T(2,128)}) custom-call(s32[2,128]{1,0:T(2,128)} %bitcast.18, bf16[128,2048]{1,0:T(8,128)(2,1)} %x_hbm.1, f32[1,2048]{1,0:T(1,128)} %bitcast.17), custom_call_target="tpu_custom_call" | custom-call | flops 134217728 | bytes 1048576 | tf_op jit(solution)/shard_map/pallas_call | solution.py:558
  5.2 107.0 %all_to_all.10 = bf16[128,48,128]{2,1,0:T(8,128)(2,1)} all-to-all(bf16[128,48,128]{2,1,0:T(8,128)(2,1)} %bitcast.16), channel_id=1, replica_groups=mesh['grp'=2,'ep_hi'=8,'ep_lo'=2,'ep_1'=2,'tp'=4] {'ep_hi','ep_lo','ep_1..., dimensions={0} | all-to-all | bytes 3145728 | tf_op jit(solution)/shard_map/all_to_all | solution.py:580
  112.2 7.1 %shard_map.168 = bf16[6144,128]{1,0:T(8,128)(2,1)} custom-call(bf16[6144,128]{1,0:T(8,128)(2,1)} %bitcast.15, bf16[1,2048,512]{2,1,0:T(8,128)(2,1)} %gate_hbm.1, bf16[1,2048,512]{2,1,0:T(8,128)(2,1)} %up_hbm.1, bf16[1,512,2048]{2,1,0:T(8,128)(2,1)} %down_hbm.1), custom_call_target="tpu_custom_call" | custom-call | flops 2415919104 | bytes 6291456 | tf_op jit(solution)/shard_map/pallas_call | solution.py:666
  119.4 9.5 %all-to-all-start.1 = ((bf16[128,48,128]{2,1,0:T(8,128)(2,1)}), bf16[128,48,128]{2,1,0:T(8,128)(2,1)S(1)}, u32[]{:S(2)}, u32[]{:S(2)}) async-start(bf16[128,48,128]{2,1,0:T(8,128)(2,1)} %bitcast.14), calls=%async_computation.1 | async-start | bytes 3145728 | tf_op jit(solution)/shard_map/all_to_all | solution.py:686
  128.9 1.0 copy-done.9
  130.0 1.0 copy-done.10
  131.0 1.0 copy-done.11
  132.0 1.1 shard_map.175
  133.1 2.6 collective-permute-start.13
  135.7 1.2 copy-done.3
  136.8 0.6 collective-permute-start.17
  137.5 31.8 %collective-permute-done.13.near = bf16[6144,128]{1,0:T(8,128)(2,1)} collective-permute-done((bf16[6144,128]{1,0:T(8,128)(2,1)S(1)}, bf16[6144,128]{1,0:T(8,128)(2,1)}, u32[]{:S(2)}, u32[]{:S(2)}) %collective-permute-start.13) | collective-permute-done | bytes 1572896 | tf_op jit(solution)/shard_map/ppermute | solution.py:446
  169.3 4.3 %collective-permute-start.14 = (bf16[6144,128]{1,0:T(8,128)(2,1)}, bf16[6144,128]{1,0:T(8,128)(2,1)}, u32[]{:S(2)}, u32[]{:S(2)}) collective-permute-start(bf16[6144,128]{1,0:T(8,128)(2,1)} %collective-permute-done.13.near), channel_id=1, source_target_pairs={{0,4},{4,0},{1,5},{5,1},{2,6},{6,2},{3,7},{7,3},{8,12},{12,8},{9,1... | collective-permute-start | bytes 4718600 | tf_op jit(solution)/shard_map/ppermute | solution.py:439
  173.7 33.1 %collective-permute-done.17.near_hbm = bf16[256,2048]{1,0:T(8,128)(2,1)} collective-permute-done((bf16[256,2048]{1,0:T(8,128)(2,1)S(1)}, bf16[256,2048]{1,0:T(8,128)(2,1)}, u32[]{:S(2)}, u32[]{:S(2)}) %collective-permute-start.17) | collective-permute-done | bytes 1048608 | tf_op jit(solution)/shard_map/ppermute | solution.py:446
  206.7 4.2 %collective-permute-start.18 = (bf16[256,2048]{1,0:T(8,128)(2,1)}, bf16[256,2048]{1,0:T(8,128)(2,1)}, u32[]{:S(2)}, u32[]{:S(2)}) collective-permute-start(bf16[256,2048]{1,0:T(8,128)(2,1)} %collective-permute-done.17.near_hbm), channel_id=1, source_target_pairs={{0,4},{4,0},{1,5},{5,1},{2,6},{6,2},{3,7},{7,3},{8,12},{12,8},{9,1... | collective-permute-start | bytes 3145736 | tf_op jit(solution)/shard_map/ppermute | solution.py:439
  211.1 0.6 collective-permute-start.20
  211.7 1.8 multiply_sine_fusion
  213.5 3.6 %shard_map.169.own = bf16[160,128]{1,0:T(8,128)(2,1)} custom-call(bf16[512,128]{1,0:T(8,128)(2,1)} %k.1, bf16[512,256]{1,0:T(8,128)(2,1)} %v.1, f32[2,512]{1,0:T(2,128)} %bitcast.12, f32[512,128]{1,0:T(8,128)} %get-tuple-element.27.cosine, f32[512,128]{1,0:T(8,128)} %get-tuple-element.26.sine), custom_call_target="tpu_custom_call" | custom-call | flops 67108864 | bytes 1048576 | tf_op jit(solution)/shard_map/pallas_call | solution.py:595
  217.1 0.2 collective-permute-start
  217.3 1.4 collective-permute-done.other
  218.6 0.8 copy-done.14
  219.6 2.6 collective-permute-done.1.refs_0_
  222.2 0.6 collective-permute-start.2
  222.8 4.2 %collective-permute-done.2.refs_0_ = bf16[80,128]{1,0:T(8,128)(2,1)S(1)} collective-permute-done((bf16[80,128]{1,0:T(8,128)(2,1)S(1)}, bf16[80,128]{1,0:T(8,128)(2,1)S(1)}, u32[]{:S(2)}, u32[]{:S(2)}) %collective-permute-start.2) | collective-permute-done | bytes 20512 | tf_op jit(solution)/shard_map/ppermute | solution.py:439
  227.1 3.9 %collective-permute-start.3 = (bf16[80,128]{1,0:T(8,128)(2,1)S(1)}, bf16[80,128]{1,0:T(8,128)(2,1)S(1)}, u32[]{:S(2)}, u32[]{:S(2)}) collective-permute-start(bf16[80,128]{1,0:T(8,128)(2,1)S(1)} %get-tuple-element.17), channel_id=1, source_target_pairs={{0,32},{16,48},{32,64},{48,80},{64,96},{80,112},{96,0},{112,16},{1... | collective-permute-start | bytes 61448 | tf_op jit(solution)/shard_map/ppermute | solution.py:439
  231.0 2.6 collective-permute-done.3.refs_1_
  233.6 5.1 %collective-permute-start.4 = (bf16[80,128]{1,0:T(8,128)(2,1)S(1)}, bf16[80,128]{1,0:T(8,128)(2,1)S(1)}, u32[]{:S(2)}, u32[]{:S(2)}) collective-permute-start(bf16[80,128]{1,0:T(8,128)(2,1)S(1)} %get-tuple-element.17), channel_id=1, source_target_pairs={{0,48},{16,64},{32,80},{48,96},{64,112},{80,0},{96,16},{112,32},{1... | collective-permute-start | bytes 61448 | tf_op jit(solution)/shard_map/ppermute | solution.py:439
  238.7 4.8 %collective-permute-done.4.refs_2_ = bf16[80,128]{1,0:T(8,128)(2,1)S(1)} collective-permute-done((bf16[80,128]{1,0:T(8,128)(2,1)S(1)}, bf16[80,128]{1,0:T(8,128)(2,1)S(1)}, u32[]{:S(2)}, u32[]{:S(2)}) %collective-permute-start.4) | collective-permute-done | bytes 20512 | tf_op jit(solution)/shard_map/ppermute | solution.py:439
  243.5 8.5 %collective-permute-start.5 = (bf16[80,128]{1,0:T(8,128)(2,1)S(1)}, bf16[80,128]{1,0:T(8,128)(2,1)S(1)}, u32[]{:S(2)}, u32[]{:S(2)}) collective-permute-start(bf16[80,128]{1,0:T(8,128)(2,1)S(1)} %get-tuple-element.17), channel_id=1, source_target_pairs={{0,64},{16,80},{32,96},{48,112},{64,0},{80,16},{96,32},{112,48},{1... | collective-permute-start | bytes 61448 | tf_op jit(solution)/shard_map/ppermute | solution.py:439
  252.0 3.2 %collective-permute-done.5.refs_3_ = bf16[80,128]{1,0:T(8,128)(2,1)S(1)} collective-permute-done((bf16[80,128]{1,0:T(8,128)(2,1)S(1)}, bf16[80,128]{1,0:T(8,128)(2,1)S(1)}, u32[]{:S(2)}, u32[]{:S(2)}) %collective-permute-start.5) | collective-permute-done | bytes 20512 | tf_op jit(solution)/shard_map/ppermute | solution.py:439
  255.2 4.2 %collective-permute-start.6 = (bf16[80,128]{1,0:T(8,128)(2,1)S(1)}, bf16[80,128]{1,0:T(8,128)(2,1)S(1)}, u32[]{:S(2)}, u32[]{:S(2)}) collective-permute-start(bf16[80,128]{1,0:T(8,128)(2,1)S(1)} %get-tuple-element.17), channel_id=1, source_target_pairs={{0,80},{16,96},{32,112},{48,0},{64,16},{80,32},{96,48},{112,64},{1... | collective-permute-start | bytes 61448 | tf_op jit(solution)/shard_map/ppermute | solution.py:439
  259.4 4.2 %collective-permute-done.6.refs_4_ = bf16[80,128]{1,0:T(8,128)(2,1)S(1)} collective-permute-done((bf16[80,128]{1,0:T(8,128)(2,1)S(1)}, bf16[80,128]{1,0:T(8,128)(2,1)S(1)}, u32[]{:S(2)}, u32[]{:S(2)}) %collective-permute-start.6) | collective-permute-done | bytes 20512 | tf_op jit(solution)/shard_map/ppermute | solution.py:439
  263.5 4.1 %collective-permute-start.7 = (bf16[80,128]{1,0:T(8,128)(2,1)S(1)}, bf16[80,128]{1,0:T(8,128)(2,1)S(1)}, u32[]{:S(2)}, u32[]{:S(2)}) collective-permute-start(bf16[80,128]{1,0:T(8,128)(2,1)S(1)} %get-tuple-element.17), channel_id=1, source_target_pairs={{0,96},{16,112},{32,0},{48,16},{64,32},{80,48},{96,64},{112,80},{1... | collective-permute-start | bytes 61448 | tf_op jit(solution)/shard_map/ppermute | solution.py:439
  267.7 2.4 collective-permute-done.7.refs_5_
  270.1 2.0 collective-permute-start.8
  272.1 1.7 collective-permute-done.8.refs_6_
  273.8 9.1 %collective-permute-start.9 = (bf16[80,128]{1,0:T(8,128)(2,1)S(1)}, bf16[80,128]{1,0:T(8,128)(2,1)S(1)}, u32[]{:S(2)}, u32[]{:S(2)}) collective-permute-start(bf16[80,128]{1,0:T(8,128)(2,1)S(1)} %shard_map.172.mine), channel_id=1, source_target_pairs={{0,4},{4,0},{1,5},{5,1},{2,6},{6,2},{3,7},{7,3},{8,12},{12,8},{9,1... | collective-permute-start | bytes 61448 | tf_op jit(solution)/shard_map/ppermute | solution.py:439
  283.0 0.7 collective-permute-done.9.theirs
  283.8 0.9 copy-done.2
  284.8 0.9 copy-done.5
  285.7 0.9 copy-done.13
  286.7 0.9 copy-done.15
  287.6 3.2 %shard_map.174 = (bf16[128,2048]{1,0:T(8,128)(2,1)S(1)}, bf16[128,256]{1,0:T(8,128)(2,1)S(1)}, bf16[128,256]{1,0:T(8,128)(2,1)S(1)}, bf16[128,256]{1,0:T(8,128)(2,1)S(1)}) custom-call(s32[1]{0:T(128)} %bitcast.7.seat, bf16[512,128]{1,0:T(8,128)(2,1)S(1)} %copy-done.15, bf16[512,128]{1,0:T(8,128)(2,1)S(1)} %copy-done.12, bf16[512,256]{1,0:T(8,128)(2,1)S(1)} %copy-done.5, ...), custom_call_target="tpu_custom_call" | custom-call | flops 262144000 | bytes 5242880 | tf_op jit(solution)/shard_map/pallas_call | solution.py:695
  290.7 0.8 copy-done.7
  291.5 2.7 collective-permute-start.11
  294.2 4.8 %shard_map.176.shared_hbm = f32[128,2048]{1,0:T(8,128)S(1)} custom-call(s32[1]{0:T(128)} %bitcast.2.core, bf16[128,2048]{1,0:T(8,128)(2,1)S(1)} %copy-done.6, bf16[6144,128]{1,0:T(8,128)(2,1)S(1)} %copy-done.4, bf16[6144,128]{1,0:T(8,128)(2,1)} %collective-permute-done.13.near, bf16[6144,128]{1,0:T(8,128)(2,1)} %collective-permute-done.14.near_other, ...), custom_call_target="tpu_custom_call" | custom-call | flops 805306368 | bytes 5242880 | tf_op jit(solution)/shard_map/pallas_call | solution.py:651
  299.1 1.0 copy-done.8
  300.1 4.0 %shard_map.177 = (bf16[128,2048]{1,0:T(8,128)(2,1)}, bf16[128,2048]{1,0:T(8,128)(2,1)}) custom-call(s32[2,128]{1,0:T(2,128)S(1)} %copy-done.17, s32[1]{0:T(128)} %bitcast.2.core, bf16[6144,128]{1,0:T(8,128)(2,1)S(1)} %bitcast.11, f32[128,2]{1,0:T(8,128)S(1)} %copy.18.weight, bf16[128,2048]{1,0:T(8,128)(2,1)S(1)} %copy-done.8, ...), custom_call_target="tpu_custom_call" | custom-call | flops 786432000 | bytes 5242880 | tf_op jit(solution)/shard_map/pallas_call | solution.py:707
  (52 shorter events, 0.7 us)
Async XLA Ops:
  119.4 9.5 %copy-start = (bf16[256,2048]{1,0:T(8,128)(2,1)S(1)}, bf16[256,2048]{1,0:T(8,128)(2,1)}, u32[]{:S(2)}) copy-start(bf16[256,2048]{1,0:T(8,128)(2,1)} %w_out.3) | copy-start | bytes 3145732
  119.4 179.7 %all-to-all-start.1 = ((bf16[128,48,128]{2,1,0:T(8,128)(2,1)}), bf16[128,48,128]{2,1,0:T(8,128)(2,1)S(1)}, u32[]{:S(2)}, u32[]{:S(2)}) async-start(bf16[128,48,128]{2,1,0:T(8,128)(2,1)} %bitcast.14), calls=%async_computation.1 | async-start | bytes 3145728 | tf_op jit(solution)/shard_map/all_to_all | solution.py:686
  128.9 1.0 copy-start.9
  130.0 1.0 copy-start.10
  131.0 1.0 copy-start.11
  133.1 149.8 %copy-start.18 = (f32[128,2]{0,1:T(2,128)S(1)}, f32[128,2]{0,1:T(2,128)}, u32[]{:S(2)}) copy-start(f32[128,2]{0,1:T(2,128)} %param.25) | copy-start | bytes 3076
  133.1 150.7 %copy-start.12 = (bf16[512,128]{1,0:T(8,128)(2,1)S(1)}, bf16[512,128]{1,0:T(8,128)(2,1)}, u32[]{:S(2)}) copy-start(bf16[512,128]{1,0:T(8,128)(2,1)} %k.1) | copy-start | bytes 393220
  133.1 150.7 %copy-start.16 = (f32[512,2]{0,1:T(2,128)S(1)}, f32[512,2]{0,1:T(2,128)}, u32[]{:S(2)}) copy-start(f32[512,2]{0,1:T(2,128)} %param.20) | copy-start | bytes 12292
  133.1 36.2 %collective-permute-start.13 = (bf16[6144,128]{1,0:T(8,128)(2,1)S(1)}, bf16[6144,128]{1,0:T(8,128)(2,1)}, u32[]{:S(2)}, u32[]{:S(2)}) collective-permute-start(bf16[6144,128]{1,0:T(8,128)(2,1)S(1)} %get-tuple-element.23.own), channel_id=1, source_target_pairs={{0,1},{1,2},{2,3},{3,0},{4,7},{5,4},{6,5},{7,6},{8,9},{9,10},{10,1... | collective-permute-start | bytes 4718600 | tf_op jit(solution)/shard_map/ppermute | solution.py:446
  135.7 1.2 copy-start.3
  136.8 69.9 %collective-permute-start.17 = (bf16[256,2048]{1,0:T(8,128)(2,1)S(1)}, bf16[256,2048]{1,0:T(8,128)(2,1)}, u32[]{:S(2)}, u32[]{:S(2)}) collective-permute-start(bf16[256,2048]{1,0:T(8,128)(2,1)S(1)} %copy-done), channel_id=1, source_target_pairs={{0,1},{1,2},{2,3},{3,0},{4,7},{5,4},{6,5},{7,6},{8,9},{9,10},{10,1... | collective-permute-start | bytes 3145736 | tf_op jit(solution)/shard_map/ppermute | solution.py:446
  137.4 73.6 %collective-permute-start.15 = (bf16[3072,128]{1,0:T(8,128)(2,1)S(1)}, bf16[3072,128]{1,0:T(8,128)(2,1)}, u32[]{:S(2)}, u32[]{:S(2)}) collective-permute-start(bf16[3072,128]{1,0:T(8,128)(2,1)S(1)} %get-tuple-element.24), channel_id=1, source_target_pairs={{0,2},{1,3},{2,0},{3,1},{4,6},{5,7},{6,4},{7,5},{8,10},{9,11},{10,... | collective-permute-start | bytes 2359304 | tf_op jit(solution)/shard_map/ppermute | solution.py:439
  169.3 124.9 %collective-permute-start.14 = (bf16[6144,128]{1,0:T(8,128)(2,1)}, bf16[6144,128]{1,0:T(8,128)(2,1)}, u32[]{:S(2)}, u32[]{:S(2)}) collective-permute-start(bf16[6144,128]{1,0:T(8,128)(2,1)} %collective-permute-done.13.near), channel_id=1, source_target_pairs={{0,4},{4,0},{1,5},{5,1},{2,6},{6,2},{3,7},{7,3},{8,12},{12,8},{9,1... | collective-permute-start | bytes 4718600 | tf_op jit(solution)/shard_map/ppermute | solution.py:439
  173.7 37.4 %collective-permute-start.19 = (bf16[128,2048]{1,0:T(8,128)(2,1)}, bf16[128,2048]{1,0:T(8,128)(2,1)}, u32[]{:S(2)}, u32[]{:S(2)}) collective-permute-start(bf16[128,2048]{1,0:T(8,128)(2,1)} %get-tuple-element.25), channel_id=1, source_target_pairs={{0,2},{1,3},{2,0},{3,1},{4,6},{5,7},{6,4},{7,5},{8,10},{9,11},{10,... | collective-permute-start | bytes 1572872 | tf_op jit(solution)/shard_map/ppermute | solution.py:439
  206.7 92.3 %collective-permute-start.18 = (bf16[256,2048]{1,0:T(8,128)(2,1)}, bf16[256,2048]{1,0:T(8,128)(2,1)}, u32[]{:S(2)}, u32[]{:S(2)}) collective-permute-start(bf16[256,2048]{1,0:T(8,128)(2,1)} %collective-permute-done.17.near_hbm), channel_id=1, source_target_pairs={{0,4},{4,0},{1,5},{5,1},{2,6},{6,2},{3,7},{7,3},{8,12},{12,8},{9,1... | collective-permute-start | bytes 3145736 | tf_op jit(solution)/shard_map/ppermute | solution.py:439
  211.0 80.6 %collective-permute-start.16 = (bf16[3072,128]{1,0:T(8,128)(2,1)}, bf16[3072,128]{1,0:T(8,128)(2,1)}, u32[]{:S(2)}, u32[]{:S(2)}) collective-permute-start(bf16[3072,128]{1,0:T(8,128)(2,1)} %collective-permute-done.15.mine), channel_id=1, source_target_pairs={{0,4},{4,0},{1,5},{5,1},{2,6},{6,2},{3,7},{7,3},{8,12},{12,8},{9,1... | collective-permute-start | bytes 2359304 | tf_op jit(solution)/shard_map/ppermute | solution.py:439
  211.1 88.0 %collective-permute-start.20 = (bf16[128,2048]{1,0:T(8,128)(2,1)}, bf16[128,2048]{1,0:T(8,128)(2,1)}, u32[]{:S(2)}, u32[]{:S(2)}) collective-permute-start(bf16[128,2048]{1,0:T(8,128)(2,1)} %collective-permute-done.19.mine_hbm), channel_id=1, source_target_pairs={{0,4},{4,0},{1,5},{5,1},{2,6},{6,2},{3,7},{7,3},{8,12},{12,8},{9,1... | collective-permute-start | bytes 1572872 | tf_op jit(solution)/shard_map/ppermute | solution.py:439
  213.5 70.3 %copy-start.1 = (f32[512,128]{1,0:T(8,128)S(1)}, f32[512,128]{1,0:T(8,128)}, u32[]{:S(2)}) copy-start(f32[512,128]{1,0:T(8,128)} %get-tuple-element.26.sine) | copy-start | bytes 786436
  217.1 1.6 collective-permute-start
  218.6 0.8 copy-start.14
  219.4 2.8 collective-permute-start.1
  222.2 4.9 %collective-permute-start.2 = (bf16[80,128]{1,0:T(8,128)(2,1)S(1)}, bf16[80,128]{1,0:T(8,128)(2,1)S(1)}, u32[]{:S(2)}, u32[]{:S(2)}) collective-permute-start(bf16[80,128]{1,0:T(8,128)(2,1)S(1)} %get-tuple-element.17), channel_id=1, source_target_pairs={{0,16},{16,32},{32,48},{48,64},{64,80},{80,96},{96,112},{112,0},{1... | collective-permute-start | bytes 61448 | tf_op jit(solution)/shard_map/ppermute | solution.py:439
  227.1 6.5 %collective-permute-start.3 = (bf16[80,128]{1,0:T(8,128)(2,1)S(1)}, bf16[80,128]{1,0:T(8,128)(2,1)S(1)}, u32[]{:S(2)}, u32[]{:S(2)}) collective-permute-start(bf16[80,128]{1,0:T(8,128)(2,1)S(1)} %get-tuple-element.17), channel_id=1, source_target_pairs={{0,32},{16,48},{32,64},{48,80},{64,96},{80,112},{96,0},{112,16},{1... | collective-permute-start | bytes 61448 | tf_op jit(solution)/shard_map/ppermute | solution.py:439
  233.6 9.9 %collective-permute-start.4 = (bf16[80,128]{1,0:T(8,128)(2,1)S(1)}, bf16[80,128]{1,0:T(8,128)(2,1)S(1)}, u32[]{:S(2)}, u32[]{:S(2)}) collective-permute-start(bf16[80,128]{1,0:T(8,128)(2,1)S(1)} %get-tuple-element.17), channel_id=1, source_target_pairs={{0,48},{16,64},{32,80},{48,96},{64,112},{80,0},{96,16},{112,32},{1... | collective-permute-start | bytes 61448 | tf_op jit(solution)/shard_map/ppermute | solution.py:439
  243.5 11.7 %collective-permute-start.5 = (bf16[80,128]{1,0:T(8,128)(2,1)S(1)}, bf16[80,128]{1,0:T(8,128)(2,1)S(1)}, u32[]{:S(2)}, u32[]{:S(2)}) collective-permute-start(bf16[80,128]{1,0:T(8,128)(2,1)S(1)} %get-tuple-element.17), channel_id=1, source_target_pairs={{0,64},{16,80},{32,96},{48,112},{64,0},{80,16},{96,32},{112,48},{1... | collective-permute-start | bytes 61448 | tf_op jit(solution)/shard_map/ppermute | solution.py:439
  255.2 8.3 %collective-permute-start.6 = (bf16[80,128]{1,0:T(8,128)(2,1)S(1)}, bf16[80,128]{1,0:T(8,128)(2,1)S(1)}, u32[]{:S(2)}, u32[]{:S(2)}) collective-permute-start(bf16[80,128]{1,0:T(8,128)(2,1)S(1)} %get-tuple-element.17), channel_id=1, source_target_pairs={{0,80},{16,96},{32,112},{48,0},{64,16},{80,32},{96,48},{112,64},{1... | collective-permute-start | bytes 61448 | tf_op jit(solution)/shard_map/ppermute | solution.py:439
  263.5 6.5 %collective-permute-start.7 = (bf16[80,128]{1,0:T(8,128)(2,1)S(1)}, bf16[80,128]{1,0:T(8,128)(2,1)S(1)}, u32[]{:S(2)}, u32[]{:S(2)}) collective-permute-start(bf16[80,128]{1,0:T(8,128)(2,1)S(1)} %get-tuple-element.17), channel_id=1, source_target_pairs={{0,96},{16,112},{32,0},{48,16},{64,32},{80,48},{96,64},{112,80},{1... | collective-permute-start | bytes 61448 | tf_op jit(solution)/shard_map/ppermute | solution.py:439
  270.1 3.6 %collective-permute-start.8 = (bf16[80,128]{1,0:T(8,128)(2,1)S(1)}, bf16[80,128]{1,0:T(8,128)(2,1)S(1)}, u32[]{:S(2)}, u32[]{:S(2)}) collective-permute-start(bf16[80,128]{1,0:T(8,128)(2,1)S(1)} %get-tuple-element.17), channel_id=1, source_target_pairs={{0,112},{16,0},{32,16},{48,32},{64,48},{80,64},{96,80},{112,96},{1... | collective-permute-start | bytes 61448 | tf_op jit(solution)/shard_map/ppermute | solution.py:439
  273.8 10.0 %collective-permute-start.9 = (bf16[80,128]{1,0:T(8,128)(2,1)S(1)}, bf16[80,128]{1,0:T(8,128)(2,1)S(1)}, u32[]{:S(2)}, u32[]{:S(2)}) collective-permute-start(bf16[80,128]{1,0:T(8,128)(2,1)S(1)} %shard_map.172.mine), channel_id=1, source_target_pairs={{0,4},{4,0},{1,5},{5,1},{2,6},{6,2},{3,7},{7,3},{8,12},{12,8},{9,1... | collective-permute-start | bytes 61448 | tf_op jit(solution)/shard_map/ppermute | solution.py:439
  283.8 1.0 copy-start.2
  284.8 0.9 copy-start.5
  285.7 0.9 copy-start.13
  286.7 0.9 copy-start.15
  287.6 6.7 %copy-start.4 = (bf16[6144,128]{1,0:T(8,128)(2,1)S(1)}, bf16[6144,128]{1,0:T(8,128)(2,1)}, u32[]{:S(2)}) copy-start(bf16[6144,128]{1,0:T(8,128)(2,1)} %copy-done.3) | copy-start | bytes 4718596
  287.6 6.7 %copy-start.6 = (bf16[128,2048]{1,0:T(8,128)(2,1)S(1)}, bf16[128,2048]{1,0:T(8,128)(2,1)}, u32[]{:S(2)}) copy-start(bf16[128,2048]{1,0:T(8,128)(2,1)} %get-tuple-element.22.normed) | copy-start | bytes 1572868
  290.7 0.8 copy-start.7
  291.5 7.5 %collective-permute-start.10 = (bf16[128,256]{1,0:T(8,128)(2,1)S(1)}, bf16[128,256]{1,0:T(8,128)(2,1)S(1)}, u32[]{:S(2)}, u32[]{:S(2)}) collective-permute-start(bf16[128,256]{1,0:T(8,128)(2,1)S(1)} %get-tuple-element.19), channel_id=1, source_target_pairs={{0,1},{1,2},{2,3},{3,0},{4,5},{5,6},{6,7},{7,4},{8,9},{9,10},{10,1... | collective-permute-start | bytes 196616 | tf_op jit(solution)/shard_map/ppermute | solution.py:439
  291.5 7.5 %collective-permute-start.11 = (bf16[128,256]{1,0:T(8,128)(2,1)S(1)}, bf16[128,256]{1,0:T(8,128)(2,1)S(1)}, u32[]{:S(2)}, u32[]{:S(2)}) collective-permute-start(bf16[128,256]{1,0:T(8,128)(2,1)S(1)} %get-tuple-element.20), channel_id=1, source_target_pairs={{0,3},{1,0},{2,1},{3,2},{4,7},{5,4},{6,5},{7,6},{8,11},{9,8},{10,9... | collective-permute-start | bytes 196616 | tf_op jit(solution)/shard_map/ppermute | solution.py:439
  294.2 4.8 %collective-permute-start.12 = (bf16[128,256]{1,0:T(8,128)(2,1)S(1)}, bf16[128,256]{1,0:T(8,128)(2,1)S(1)}, u32[]{:S(2)}, u32[]{:S(2)}) collective-permute-start(bf16[128,256]{1,0:T(8,128)(2,1)S(1)} %get-tuple-element.21), channel_id=1, source_target_pairs={{0,2},{1,3},{2,0},{3,1},{4,6},{5,7},{6,4},{7,5},{8,10},{9,11},{10,... | collective-permute-start | bytes 196616 | tf_op jit(solution)/shard_map/ppermute | solution.py:439
  294.2 4.9 %copy-start.17 = (s32[2,128]{1,0:T(2,128)S(1)}, s32[2,128]{1,0:T(2,128)}, u32[]{:S(2)}) copy-start(s32[2,128]{1,0:T(2,128)} %get-tuple-element.14.places) | copy-start | bytes 3076
  299.1 1.0 copy-start.8

commit v5 on v4

--- a/solution.py
+++ b/solution.py
@@ -227,20 +227,37 @@
     return out
 
 
-def state_kernel(k_hbm, v_hbm, decay_hbm, cosine, sine, packed, k, v, log_decay, sems):
+def state_kernel(first, k_hbm, v_hbm, decay_hbm, frequency, packed, k, v, log_decay, sems):
     pairs = ((decay_hbm, log_decay), (k_hbm, k), (v_hbm, v))
     copies = [pltpu.make_async_copy(a, b, sems.at[i]) for i, (a, b) in enumerate(pairs)]
     for copy in copies:
         copy.start()
+    half = k.shape[1] // log_decay.shape[0] // 2
+    groups = LANES // half
+    depth = k.shape[0] // groups
+    lane = lax.broadcasted_iota(jnp.int32, (depth, LANES), 1)
+    spots = first[0] + lax.broadcasted_iota(jnp.int32, (depth, LANES), 0) + lane // half * depth
+    angles = spots.astype(F32) * frequency[...]
+
+    def spread(packed):
+        found = []
+        for b in range(groups):
+            part = jnp.where(lane // half == b, packed, 0.0)
+            shift = half
+            while shift < LANES:
+                part = part + pltpu.roll(part, shift, 1)
+                shift *= 2
+            found.append(part)
+        return jnp.concatenate(found, axis=0)
+
+    cosine, sine = spread(jnp.cos(angles)), spread(jnp.sin(angles))
     for copy in copies:
         copy.wait()
     heads = log_decay.shape[0]
     key_size = k.shape[1] // heads
     value_size = v.shape[1] // heads
     span = k.shape[0]
-    k_rot = (rotated(k[...], cosine[...], sine[...], key_size // 2) * key_size ** (-0.5)).astype(
-        BF16
-    )
+    k_rot = (rotated(k[...], cosine, sine, key_size // 2) * key_size ** (-0.5)).astype(BF16)
     above = jnp.where(lower(BLOCK, True), 1.0, 0.0)
     after = jnp.zeros((1, heads), F32)
     tails = [None] * (span // BLOCK)
@@ -587,15 +604,17 @@
 
     half = key_size // 2
     frequency = ROPE_BASE ** (-jnp.arange(half, dtype=F32) / half)
-    spots = lax.axis_index(EP) * span + jnp.arange(span, dtype=jnp.int32)
-    angles = spots.astype(F32)[:, None] * jnp.tile(frequency, LANES // half)[None, :]
+    frequency = jnp.tile(frequency, LANES // half)[None, :]
+    first = lax.axis_index(EP) * span
+    spots = first + jnp.arange(span, dtype=jnp.int32)
+    angles = spots.astype(F32)[:, None] * frequency
     cosine = jnp.cos(angles)
     sine = jnp.sin(angles)
 
     own = call(
         state_kernel,
         jax.ShapeDtypeStruct((heads * STATE_ROWS, value_size), BF16),
-        [HBM] * 3 + [VMEM] * 2,
+        [SMEM] + [HBM] * 3 + [VMEM],
         VMEM,
         [
             pltpu.VMEM(keys.shape, BF16),
@@ -606,7 +625,7 @@
         2 * span * LANES * 512,
         4 * span * LANES * 4,
         61,
-    )(keys, values, log_decay.T, cosine, sine)
+    )(first.reshape(1).astype(jnp.int32), keys, values, log_decay.T, frequency)
     other = moved_by(own, "ep_1", 1)
     chip = small(chip_kernel, packed_shape, [SMEM, VMEM, VMEM], VMEM)(core, own, other)
     low_seat = lax.axis_index("ep_lo").reshape(1).astype(jnp.int32)

time: 305 us -> 302 us (level)
  starting transfers between devices: 62.4 us -> 53.1 us
  waiting for transfers between devices: 92.8 us -> 101 us
    ppermute x19, starting transfers between devices: 49.7 us -> 40.5 us  [moved_by(): lax.ppermute(array, axis, [(s, (s + step) % count) for s in range(count)])]
    ppermute x19, waiting for transfers between devices: 27.9 us -> 35.8 us  [moved_by(): lax.ppermute(array, axis, [(s, (s + step) % count) for s in range(count)])]
    unnamed x39 -> x35, local copies, waits for them, and re-layouts: 10.8 us -> 9.14 us
  transfers between devices with their start and end apart: 22 -> 22, of which waited for: 12 -> 11; matrix products, arithmetic and copies ran while one was open for 1% -> 1% of each run, Pallas kernels for 4% -> 4%
where the time goes in v5:
time: 302 us; the launch traced here: 301 us
  blocking collectives  107 us (35%)
  waiting for transfers between devices  101 us (33%)
  starting transfers between devices  53.1 us (18%)
  Pallas kernels  28 us (9%)
  local copies, waits for them, and re-layouts  9.9 us (3%)
    all_to_all x1, blocking collectives, per_device(): lax.all_to_all(outbound.reshape(experts, capacity * TILE, LANES), EP_TP,...  107 us
    ppermute x2, waiting for transfers between devices, outward(): return lax.ppermute(array, ('ep_1', 'tp'), pairs)  64.9 us
    ppermute x19, starting transfers between devices, moved_by(): lax.ppermute(array, axis, [(s, (s + step) % count) for s in range(count)])  40.5 us
    ppermute x19, waiting for transfers between devices, moved_by(): lax.ppermute(array, axis, [(s, (s + step) % count) for s in range(count)])  35.8 us
    all_to_all x1, starting transfers between devices, per_device(): lax.all_to_all(answers.reshape(experts, capacity * TILE, LANES), EP_TP, s...  9.48 us
    unnamed x35, local copies, waits for them, and re-layouts  9.14 us
    pallas_call x1, Pallas kernels, per_device(): call(expert_kernel, jax.ShapeDtypeStruct((tile_rows, LANES), BF16), [HBM]...  7.13 us
  transfers between devices with their start and end apart: 22, of which 11 were waited for; matrix products, arithmetic and copies ran while one was open for 1% of the time, Pallas kernels for 4%

profile of v5, /device:TPU:33, one launch (start us, length us, event | category | flops | bytes accessed | tf_op | source)
XLA Modules:
  0.0 300.8 jit_solution(1197930769200684840)
XLA Ops:
  0.6 4.6 %shard_map.167 = (bf16[128,2048]{1,0:T(8,128)(2,1)}, bf16[6144,128]{1,0:T(8,128)(2,1)}, s32[2,128]{1,0:T(2,128)}) custom-call(s32[2,128]{1,0:T(2,128)} %bitcast.19, bf16[128,2048]{1,0:T(8,128)(2,1)} %x_hbm.1, f32[1,2048]{1,0:T(1,128)} %bitcast.18), custom_call_target="tpu_custom_call" | custom-call | flops 134217728 | bytes 1048576 | tf_op jit(solution)/shard_map/pallas_call | solution.py:575
  5.2 107.0 %all_to_all.10 = bf16[128,48,128]{2,1,0:T(8,128)(2,1)} all-to-all(bf16[128,48,128]{2,1,0:T(8,128)(2,1)} %bitcast.17), channel_id=1, replica_groups=mesh['grp'=2,'ep_hi'=8,'ep_lo'=2,'ep_1'=2,'tp'=4] {'ep_hi','ep_lo','ep_1..., dimensions={0} | all-to-all | bytes 3145728 | tf_op jit(solution)/shard_map/all_to_all | solution.py:597
  112.2 7.1 %shard_map.168 = bf16[6144,128]{1,0:T(8,128)(2,1)} custom-call(bf16[6144,128]{1,0:T(8,128)(2,1)} %bitcast.16, bf16[1,2048,512]{2,1,0:T(8,128)(2,1)} %gate_hbm.1, bf16[1,2048,512]{2,1,0:T(8,128)(2,1)} %up_hbm.1, bf16[1,512,2048]{2,1,0:T(8,128)(2,1)} %down_hbm.1), custom_call_target="tpu_custom_call" | custom-call | flops 2415919104 | bytes 6291456 | tf_op jit(solution)/shard_map/pallas_call | solution.py:685
  119.4 9.5 %all-to-all-start.1 = ((bf16[128,48,128]{2,1,0:T(8,128)(2,1)}), bf16[128,48,128]{2,1,0:T(8,128)(2,1)S(1)}, u32[]{:S(2)}, u32[]{:S(2)}) async-start(bf16[128,48,128]{2,1,0:T(8,128)(2,1)} %bitcast.15), calls=%async_computation.1 | async-start | bytes 3145728 | tf_op jit(solution)/shard_map/all_to_all | solution.py:705
  128.9 1.0 copy-done.7
  129.9 1.0 copy-done.8
  131.0 1.0 copy-done.9
  132.0 1.1 shard_map.175
  133.1 2.6 collective-permute-start.13
  135.7 1.2 copy-done.1
  136.8 0.6 collective-permute-start.17
  137.4 0.1 collective-permute-start.15
  137.5 31.8 %collective-permute-done.13.near = bf16[6144,128]{1,0:T(8,128)(2,1)} collective-permute-done((bf16[6144,128]{1,0:T(8,128)(2,1)S(1)}, bf16[6144,128]{1,0:T(8,128)(2,1)}, u32[]{:S(2)}, u32[]{:S(2)}) %collective-permute-start.13) | collective-permute-done | bytes 1572896 | tf_op jit(solution)/shard_map/ppermute | solution.py:463
  169.3 4.3 %collective-permute-start.14 = (bf16[6144,128]{1,0:T(8,128)(2,1)}, bf16[6144,128]{1,0:T(8,128)(2,1)}, u32[]{:S(2)}, u32[]{:S(2)}) collective-permute-start(bf16[6144,128]{1,0:T(8,128)(2,1)} %collective-permute-done.13.near), channel_id=1, source_target_pairs={{0,4},{4,0},{1,5},{5,1},{2,6},{6,2},{3,7},{7,3},{8,12},{12,8},{9,1... | collective-permute-start | bytes 4718600 | tf_op jit(solution)/shard_map/ppermute | solution.py:456
  173.6 33.1 %collective-permute-done.17.near_hbm = bf16[256,2048]{1,0:T(8,128)(2,1)} collective-permute-done((bf16[256,2048]{1,0:T(8,128)(2,1)S(1)}, bf16[256,2048]{1,0:T(8,128)(2,1)}, u32[]{:S(2)}, u32[]{:S(2)}) %collective-permute-start.17) | collective-permute-done | bytes 1048608 | tf_op jit(solution)/shard_map/ppermute | solution.py:463
  206.7 4.2 %collective-permute-start.18 = (bf16[256,2048]{1,0:T(8,128)(2,1)}, bf16[256,2048]{1,0:T(8,128)(2,1)}, u32[]{:S(2)}, u32[]{:S(2)}) collective-permute-start(bf16[256,2048]{1,0:T(8,128)(2,1)} %collective-permute-done.17.near_hbm), channel_id=1, source_target_pairs={{0,4},{4,0},{1,5},{5,1},{2,6},{6,2},{3,7},{7,3},{8,12},{12,8},{9,1... | collective-permute-start | bytes 3145736 | tf_op jit(solution)/shard_map/ppermute | solution.py:456
  211.0 0.7 broadcast_in_dim_tile.3.frequency
  211.6 3.2 %shard_map.169.own = bf16[160,128]{1,0:T(8,128)(2,1)} custom-call(s32[1]{0:T(128)} %bitcast.11.first, bf16[512,128]{1,0:T(8,128)(2,1)} %k.1, bf16[512,256]{1,0:T(8,128)(2,1)} %v.1, f32[2,512]{1,0:T(2,128)} %bitcast.13, f32[1,128]{1,0:T(1,128)} %broadcast_in_dim_tile.3.frequency), custom_call_target="tpu_custom_call" | custom-call | flops 67108864 | bytes 1048576 | tf_op jit(solution)/shard_map/pallas_call | solution.py:614
  214.8 0.6 collective-permute-start
  215.4 1.1 collective-permute-done.other
  216.5 0.8 copy-done.12
  217.3 0.1 collective-permute-start.1
  217.5 2.6 collective-permute-done.1.refs_0_
  220.1 0.1 collective-permute-start.2
  220.2 4.7 %collective-permute-done.2.refs_0_ = bf16[80,128]{1,0:T(8,128)(2,1)S(1)} collective-permute-done((bf16[80,128]{1,0:T(8,128)(2,1)S(1)}, bf16[80,128]{1,0:T(8,128)(2,1)S(1)}, u32[]{:S(2)}, u32[]{:S(2)}) %collective-permute-start.2) | collective-permute-done | bytes 20512 | tf_op jit(solution)/shard_map/ppermute | solution.py:456
  225.0 1.4 collective-permute-start.3
  226.4 5.1 %collective-permute-done.3.refs_1_ = bf16[80,128]{1,0:T(8,128)(2,1)S(1)} collective-permute-done((bf16[80,128]{1,0:T(8,128)(2,1)S(1)}, bf16[80,128]{1,0:T(8,128)(2,1)S(1)}, u32[]{:S(2)}, u32[]{:S(2)}) %collective-permute-start.3) | collective-permute-done | bytes 20512 | tf_op jit(solution)/shard_map/ppermute | solution.py:456
  231.5 2.6 collective-permute-start.4
  234.1 3.5 %collective-permute-start.20 = (bf16[128,2048]{1,0:T(8,128)(2,1)}, bf16[128,2048]{1,0:T(8,128)(2,1)}, u32[]{:S(2)}, u32[]{:S(2)}) collective-permute-start(bf16[128,2048]{1,0:T(8,128)(2,1)} %collective-permute-done.19.mine_hbm), channel_id=1, source_target_pairs={{0,4},{4,0},{1,5},{5,1},{2,6},{6,2},{3,7},{7,3},{8,12},{12,8},{9,1... | collective-permute-start | bytes 1572872 | tf_op jit(solution)/shard_map/ppermute | solution.py:456
  237.6 3.4 %collective-permute-done.4.refs_2_ = bf16[80,128]{1,0:T(8,128)(2,1)S(1)} collective-permute-done((bf16[80,128]{1,0:T(8,128)(2,1)S(1)}, bf16[80,128]{1,0:T(8,128)(2,1)S(1)}, u32[]{:S(2)}, u32[]{:S(2)}) %collective-permute-start.4) | collective-permute-done | bytes 20512 | tf_op jit(solution)/shard_map/ppermute | solution.py:456
  241.1 6.1 %collective-permute-start.5 = (bf16[80,128]{1,0:T(8,128)(2,1)S(1)}, bf16[80,128]{1,0:T(8,128)(2,1)S(1)}, u32[]{:S(2)}, u32[]{:S(2)}) collective-permute-start(bf16[80,128]{1,0:T(8,128)(2,1)S(1)} %get-tuple-element.17), channel_id=1, source_target_pairs={{0,64},{16,80},{32,96},{48,112},{64,0},{80,16},{96,32},{112,48},{1... | collective-permute-start | bytes 61448 | tf_op jit(solution)/shard_map/ppermute | solution.py:456
  247.2 5.2 %collective-permute-done.5.refs_3_ = bf16[80,128]{1,0:T(8,128)(2,1)S(1)} collective-permute-done((bf16[80,128]{1,0:T(8,128)(2,1)S(1)}, bf16[80,128]{1,0:T(8,128)(2,1)S(1)}, u32[]{:S(2)}, u32[]{:S(2)}) %collective-permute-start.5) | collective-permute-done | bytes 20512 | tf_op jit(solution)/shard_map/ppermute | solution.py:456
  252.4 2.9 collective-permute-start.6
  255.3 5.4 %collective-permute-done.6.refs_4_ = bf16[80,128]{1,0:T(8,128)(2,1)S(1)} collective-permute-done((bf16[80,128]{1,0:T(8,128)(2,1)S(1)}, bf16[80,128]{1,0:T(8,128)(2,1)S(1)}, u32[]{:S(2)}, u32[]{:S(2)}) %collective-permute-start.6) | collective-permute-done | bytes 20512 | tf_op jit(solution)/shard_map/ppermute | solution.py:456
  260.8 2.4 collective-permute-start.7
  263.1 4.5 %collective-permute-done.7.refs_5_ = bf16[80,128]{1,0:T(8,128)(2,1)S(1)} collective-permute-done((bf16[80,128]{1,0:T(8,128)(2,1)S(1)}, bf16[80,128]{1,0:T(8,128)(2,1)S(1)}, u32[]{:S(2)}, u32[]{:S(2)}) %collective-permute-start.7) | collective-permute-done | bytes 20512 | tf_op jit(solution)/shard_map/ppermute | solution.py:456
  267.7 3.6 %collective-permute-done.8.refs_6_ = bf16[80,128]{1,0:T(8,128)(2,1)S(1)} collective-permute-done((bf16[80,128]{1,0:T(8,128)(2,1)S(1)}, bf16[80,128]{1,0:T(8,128)(2,1)S(1)}, u32[]{:S(2)}, u32[]{:S(2)}) %collective-permute-start.8) | collective-permute-done | bytes 20512 | tf_op jit(solution)/shard_map/ppermute | solution.py:456
  271.4 9.2 %collective-permute-start.9 = (bf16[80,128]{1,0:T(8,128)(2,1)S(1)}, bf16[80,128]{1,0:T(8,128)(2,1)S(1)}, u32[]{:S(2)}, u32[]{:S(2)}) collective-permute-start(bf16[80,128]{1,0:T(8,128)(2,1)S(1)} %shard_map.172.mine), channel_id=1, source_target_pairs={{0,4},{4,0},{1,5},{5,1},{2,6},{6,2},{3,7},{7,3},{8,12},{12,8},{9,1... | collective-permute-start | bytes 61448 | tf_op jit(solution)/shard_map/ppermute | solution.py:456
  280.6 1.0 multiply_sine_fusion
  281.8 1.0 copy-done.3
  282.9 0.9 copy-done.11
  283.8 0.9 copy-done.13
  284.7 3.1 %shard_map.174 = (bf16[128,2048]{1,0:T(8,128)(2,1)S(1)}, bf16[128,256]{1,0:T(8,128)(2,1)S(1)}, bf16[128,256]{1,0:T(8,128)(2,1)S(1)}, bf16[128,256]{1,0:T(8,128)(2,1)S(1)}) custom-call(s32[1]{0:T(128)} %bitcast.7.seat, bf16[512,128]{1,0:T(8,128)(2,1)S(1)} %copy-done.13, bf16[512,128]{1,0:T(8,128)(2,1)S(1)} %copy-done.10, bf16[512,256]{1,0:T(8,128)(2,1)S(1)} %copy-done.3, ...), custom_call_target="tpu_custom_call" | custom-call | flops 262144000 | bytes 5242880 | tf_op jit(solution)/shard_map/pallas_call | solution.py:714
  287.9 0.1 collective-permute-start.10
  288.0 2.6 collective-permute-start.11
  290.7 4.8 %shard_map.176.shared_hbm = f32[128,2048]{1,0:T(8,128)S(1)} custom-call(s32[1]{0:T(128)} %bitcast.2.core, bf16[128,2048]{1,0:T(8,128)(2,1)S(1)} %copy-done.4, bf16[6144,128]{1,0:T(8,128)(2,1)S(1)} %copy-done.2, bf16[6144,128]{1,0:T(8,128)(2,1)} %collective-permute-done.13.near, bf16[6144,128]{1,0:T(8,128)(2,1)} %collective-permute-done.14.near_other, ...), custom_call_target="tpu_custom_call" | custom-call | flops 805306368 | bytes 5242880 | tf_op jit(solution)/shard_map/pallas_call | solution.py:670
  295.6 1.0 copy-done.6
  296.6 4.0 %shard_map.177 = (bf16[128,2048]{1,0:T(8,128)(2,1)}, bf16[128,2048]{1,0:T(8,128)(2,1)}) custom-call(s32[2,128]{1,0:T(2,128)S(1)} %copy-done.15, s32[1]{0:T(128)} %bitcast.2.core, bf16[6144,128]{1,0:T(8,128)(2,1)S(1)} %bitcast.12, f32[128,2]{1,0:T(8,128)S(1)} %copy.18.weight, bf16[128,2048]{1,0:T(8,128)(2,1)S(1)} %copy-done.6, ...), custom_call_target="tpu_custom_call" | custom-call | flops 786432000 | bytes 5242880 | tf_op jit(solution)/shard_map/pallas_call | solution.py:726
  (49 shorter events, 0.5 us)
Async XLA Ops:
  119.4 9.5 %copy-start = (bf16[256,2048]{1,0:T(8,128)(2,1)S(1)}, bf16[256,2048]{1,0:T(8,128)(2,1)}, u32[]{:S(2)}) copy-start(bf16[256,2048]{1,0:T(8,128)(2,1)} %w_out.3) | copy-start | bytes 3145732
  119.4 176.2 %all-to-all-start.1 = ((bf16[128,48,128]{2,1,0:T(8,128)(2,1)}), bf16[128,48,128]{2,1,0:T(8,128)(2,1)S(1)}, u32[]{:S(2)}, u32[]{:S(2)}) async-start(bf16[128,48,128]{2,1,0:T(8,128)(2,1)} %bitcast.15), calls=%async_computation.1 | async-start | bytes 3145728 | tf_op jit(solution)/shard_map/all_to_all | solution.py:705
  128.9 1.0 copy-start.7
  129.9 1.0 copy-start.8
  131.0 1.0 copy-start.9
  132.0 149.6 %copy-start.16 = (f32[128,2]{0,1:T(2,128)S(1)}, f32[128,2]{0,1:T(2,128)}, u32[]{:S(2)}) copy-start(f32[128,2]{0,1:T(2,128)} %param.25) | copy-start | bytes 3076
  132.0 149.8 %copy-start.10 = (bf16[512,128]{1,0:T(8,128)(2,1)S(1)}, bf16[512,128]{1,0:T(8,128)(2,1)}, u32[]{:S(2)}) copy-start(bf16[512,128]{1,0:T(8,128)(2,1)} %k.1) | copy-start | bytes 393220
  132.0 149.8 %copy-start.14 = (f32[512,2]{0,1:T(2,128)S(1)}, f32[512,2]{0,1:T(2,128)}, u32[]{:S(2)}) copy-start(f32[512,2]{0,1:T(2,128)} %param.20) | copy-start | bytes 12292
  133.1 36.2 %collective-permute-start.13 = (bf16[6144,128]{1,0:T(8,128)(2,1)S(1)}, bf16[6144,128]{1,0:T(8,128)(2,1)}, u32[]{:S(2)}, u32[]{:S(2)}) collective-permute-start(bf16[6144,128]{1,0:T(8,128)(2,1)S(1)} %get-tuple-element.23.own), channel_id=1, source_target_pairs={{0,1},{1,2},{2,3},{3,0},{4,7},{5,4},{6,5},{7,6},{8,9},{9,10},{10,1... | collective-permute-start | bytes 4718600 | tf_op jit(solution)/shard_map/ppermute | solution.py:463
  135.7 1.2 copy-start.1
  136.8 69.9 %collective-permute-start.17 = (bf16[256,2048]{1,0:T(8,128)(2,1)S(1)}, bf16[256,2048]{1,0:T(8,128)(2,1)}, u32[]{:S(2)}, u32[]{:S(2)}) collective-permute-start(bf16[256,2048]{1,0:T(8,128)(2,1)S(1)} %copy-done), channel_id=1, source_target_pairs={{0,1},{1,2},{2,3},{3,0},{4,7},{5,4},{6,5},{7,6},{8,9},{9,10},{10,1... | collective-permute-start | bytes 3145736 | tf_op jit(solution)/shard_map/ppermute | solution.py:463
  137.4 73.6 %collective-permute-start.15 = (bf16[3072,128]{1,0:T(8,128)(2,1)S(1)}, bf16[3072,128]{1,0:T(8,128)(2,1)}, u32[]{:S(2)}, u32[]{:S(2)}) collective-permute-start(bf16[3072,128]{1,0:T(8,128)(2,1)S(1)} %get-tuple-element.24), channel_id=1, source_target_pairs={{0,2},{1,3},{2,0},{3,1},{4,6},{5,7},{6,4},{7,5},{8,10},{9,11},{10,... | collective-permute-start | bytes 2359304 | tf_op jit(solution)/shard_map/ppermute | solution.py:456
  169.3 121.4 %collective-permute-start.14 = (bf16[6144,128]{1,0:T(8,128)(2,1)}, bf16[6144,128]{1,0:T(8,128)(2,1)}, u32[]{:S(2)}, u32[]{:S(2)}) collective-permute-start(bf16[6144,128]{1,0:T(8,128)(2,1)} %collective-permute-done.13.near), channel_id=1, source_target_pairs={{0,4},{4,0},{1,5},{5,1},{2,6},{6,2},{3,7},{7,3},{8,12},{12,8},{9,1... | collective-permute-start | bytes 4718600 | tf_op jit(solution)/shard_map/ppermute | solution.py:456
  173.6 60.5 %collective-permute-start.19 = (bf16[128,2048]{1,0:T(8,128)(2,1)}, bf16[128,2048]{1,0:T(8,128)(2,1)}, u32[]{:S(2)}, u32[]{:S(2)}) collective-permute-start(bf16[128,2048]{1,0:T(8,128)(2,1)} %get-tuple-element.25), channel_id=1, source_target_pairs={{0,2},{1,3},{2,0},{3,1},{4,6},{5,7},{6,4},{7,5},{8,10},{9,11},{10,... | collective-permute-start | bytes 1572872 | tf_op jit(solution)/shard_map/ppermute | solution.py:456
  206.7 88.8 %collective-permute-start.18 = (bf16[256,2048]{1,0:T(8,128)(2,1)}, bf16[256,2048]{1,0:T(8,128)(2,1)}, u32[]{:S(2)}, u32[]{:S(2)}) collective-permute-start(bf16[256,2048]{1,0:T(8,128)(2,1)} %collective-permute-done.17.near_hbm), channel_id=1, source_target_pairs={{0,4},{4,0},{1,5},{5,1},{2,6},{6,2},{3,7},{7,3},{8,12},{12,8},{9,1... | collective-permute-start | bytes 3145736 | tf_op jit(solution)/shard_map/ppermute | solution.py:456
  210.9 77.1 %collective-permute-start.16 = (bf16[3072,128]{1,0:T(8,128)(2,1)}, bf16[3072,128]{1,0:T(8,128)(2,1)}, u32[]{:S(2)}, u32[]{:S(2)}) collective-permute-start(bf16[3072,128]{1,0:T(8,128)(2,1)} %collective-permute-done.15.mine), channel_id=1, source_target_pairs={{0,4},{4,0},{1,5},{5,1},{2,6},{6,2},{3,7},{7,3},{8,12},{12,8},{9,1... | collective-permute-start | bytes 2359304 | tf_op jit(solution)/shard_map/ppermute | solution.py:456
  214.8 1.7 collective-permute-start
  216.5 0.8 copy-start.12
  217.3 2.8 collective-permute-start.1
  220.1 4.9 %collective-permute-start.2 = (bf16[80,128]{1,0:T(8,128)(2,1)S(1)}, bf16[80,128]{1,0:T(8,128)(2,1)S(1)}, u32[]{:S(2)}, u32[]{:S(2)}) collective-permute-start(bf16[80,128]{1,0:T(8,128)(2,1)S(1)} %get-tuple-element.17), channel_id=1, source_target_pairs={{0,16},{16,32},{32,48},{48,64},{64,80},{80,96},{96,112},{112,0},{1... | collective-permute-start | bytes 61448 | tf_op jit(solution)/shard_map/ppermute | solution.py:456
  225.0 6.5 %collective-permute-start.3 = (bf16[80,128]{1,0:T(8,128)(2,1)S(1)}, bf16[80,128]{1,0:T(8,128)(2,1)S(1)}, u32[]{:S(2)}, u32[]{:S(2)}) collective-permute-start(bf16[80,128]{1,0:T(8,128)(2,1)S(1)} %get-tuple-element.17), channel_id=1, source_target_pairs={{0,32},{16,48},{32,64},{48,80},{64,96},{80,112},{96,0},{112,16},{1... | collective-permute-start | bytes 61448 | tf_op jit(solution)/shard_map/ppermute | solution.py:456
  231.5 9.5 %collective-permute-start.4 = (bf16[80,128]{1,0:T(8,128)(2,1)S(1)}, bf16[80,128]{1,0:T(8,128)(2,1)S(1)}, u32[]{:S(2)}, u32[]{:S(2)}) collective-permute-start(bf16[80,128]{1,0:T(8,128)(2,1)S(1)} %get-tuple-element.17), channel_id=1, source_target_pairs={{0,48},{16,64},{32,80},{48,96},{64,112},{80,0},{96,16},{112,32},{1... | collective-permute-start | bytes 61448 | tf_op jit(solution)/shard_map/ppermute | solution.py:456
  234.1 61.4 %collective-permute-start.20 = (bf16[128,2048]{1,0:T(8,128)(2,1)}, bf16[128,2048]{1,0:T(8,128)(2,1)}, u32[]{:S(2)}, u32[]{:S(2)}) collective-permute-start(bf16[128,2048]{1,0:T(8,128)(2,1)} %collective-permute-done.19.mine_hbm), channel_id=1, source_target_pairs={{0,4},{4,0},{1,5},{5,1},{2,6},{6,2},{3,7},{7,3},{8,12},{12,8},{9,1... | collective-permute-start | bytes 1572872 | tf_op jit(solution)/shard_map/ppermute | solution.py:456
  241.1 11.3 %collective-permute-start.5 = (bf16[80,128]{1,0:T(8,128)(2,1)S(1)}, bf16[80,128]{1,0:T(8,128)(2,1)S(1)}, u32[]{:S(2)}, u32[]{:S(2)}) collective-permute-start(bf16[80,128]{1,0:T(8,128)(2,1)S(1)} %get-tuple-element.17), channel_id=1, source_target_pairs={{0,64},{16,80},{32,96},{48,112},{64,0},{80,16},{96,32},{112,48},{1... | collective-permute-start | bytes 61448 | tf_op jit(solution)/shard_map/ppermute | solution.py:456
  252.4 8.3 %collective-permute-start.6 = (bf16[80,128]{1,0:T(8,128)(2,1)S(1)}, bf16[80,128]{1,0:T(8,128)(2,1)S(1)}, u32[]{:S(2)}, u32[]{:S(2)}) collective-permute-start(bf16[80,128]{1,0:T(8,128)(2,1)S(1)} %get-tuple-element.17), channel_id=1, source_target_pairs={{0,80},{16,96},{32,112},{48,0},{64,16},{80,32},{96,48},{112,64},{1... | collective-permute-start | bytes 61448 | tf_op jit(solution)/shard_map/ppermute | solution.py:456
  260.8 6.8 %collective-permute-start.7 = (bf16[80,128]{1,0:T(8,128)(2,1)S(1)}, bf16[80,128]{1,0:T(8,128)(2,1)S(1)}, u32[]{:S(2)}, u32[]{:S(2)}) collective-permute-start(bf16[80,128]{1,0:T(8,128)(2,1)S(1)} %get-tuple-element.17), channel_id=1, source_target_pairs={{0,96},{16,112},{32,0},{48,16},{64,32},{80,48},{96,64},{112,80},{1... | collective-permute-start | bytes 61448 | tf_op jit(solution)/shard_map/ppermute | solution.py:456
  267.6 3.7 %collective-permute-start.8 = (bf16[80,128]{1,0:T(8,128)(2,1)S(1)}, bf16[80,128]{1,0:T(8,128)(2,1)S(1)}, u32[]{:S(2)}, u32[]{:S(2)}) collective-permute-start(bf16[80,128]{1,0:T(8,128)(2,1)S(1)} %get-tuple-element.17), channel_id=1, source_target_pairs={{0,112},{16,0},{32,16},{48,32},{64,48},{80,64},{96,80},{112,96},{1... | collective-permute-start | bytes 61448 | tf_op jit(solution)/shard_map/ppermute | solution.py:456
  271.4 10.4 %collective-permute-start.9 = (bf16[80,128]{1,0:T(8,128)(2,1)S(1)}, bf16[80,128]{1,0:T(8,128)(2,1)S(1)}, u32[]{:S(2)}, u32[]{:S(2)}) collective-permute-start(bf16[80,128]{1,0:T(8,128)(2,1)S(1)} %shard_map.172.mine), channel_id=1, source_target_pairs={{0,4},{4,0},{1,5},{5,1},{2,6},{6,2},{3,7},{7,3},{8,12},{12,8},{9,1... | collective-permute-start | bytes 61448 | tf_op jit(solution)/shard_map/ppermute | solution.py:456
  281.8 8.9 %copy-start.2 = (bf16[6144,128]{1,0:T(8,128)(2,1)S(1)}, bf16[6144,128]{1,0:T(8,128)(2,1)}, u32[]{:S(2)}) copy-start(bf16[6144,128]{1,0:T(8,128)(2,1)} %copy-done.1) | copy-start | bytes 4718596
  281.8 1.1 copy-start.3
  282.9 0.9 copy-start.11
  283.8 0.9 copy-start.13
  284.7 6.0 %copy-start.4 = (bf16[128,2048]{1,0:T(8,128)(2,1)S(1)}, bf16[128,2048]{1,0:T(8,128)(2,1)}, u32[]{:S(2)}) copy-start(bf16[128,2048]{1,0:T(8,128)(2,1)} %get-tuple-element.22.normed) | copy-start | bytes 1572868
  287.9 7.6 %copy-start.5 = (bf16[128,2048]{1,0:T(8,128)(2,1)}, bf16[128,2048]{1,0:T(8,128)(2,1)S(1)}, u32[]{:S(2)}) copy-start(bf16[128,2048]{1,0:T(8,128)(2,1)S(1)} %get-tuple-element.18.own) | copy-start | bytes 1572868
  287.9 7.6 %collective-permute-start.10 = (bf16[128,256]{1,0:T(8,128)(2,1)S(1)}, bf16[128,256]{1,0:T(8,128)(2,1)S(1)}, u32[]{:S(2)}, u32[]{:S(2)}) collective-permute-start(bf16[128,256]{1,0:T(8,128)(2,1)S(1)} %get-tuple-element.19), channel_id=1, source_target_pairs={{0,1},{1,2},{2,3},{3,0},{4,5},{5,6},{6,7},{7,4},{8,9},{9,10},{10,1... | collective-permute-start | bytes 196616 | tf_op jit(solution)/shard_map/ppermute | solution.py:456
  288.0 7.5 %collective-permute-start.11 = (bf16[128,256]{1,0:T(8,128)(2,1)S(1)}, bf16[128,256]{1,0:T(8,128)(2,1)S(1)}, u32[]{:S(2)}, u32[]{:S(2)}) collective-permute-start(bf16[128,256]{1,0:T(8,128)(2,1)S(1)} %get-tuple-element.20), channel_id=1, source_target_pairs={{0,3},{1,0},{2,1},{3,2},{4,7},{5,4},{6,5},{7,6},{8,11},{9,8},{10,9... | collective-permute-start | bytes 196616 | tf_op jit(solution)/shard_map/ppermute | solution.py:456
  290.7 4.8 %collective-permute-start.12 = (bf16[128,256]{1,0:T(8,128)(2,1)S(1)}, bf16[128,256]{1,0:T(8,128)(2,1)S(1)}, u32[]{:S(2)}, u32[]{:S(2)}) collective-permute-start(bf16[128,256]{1,0:T(8,128)(2,1)S(1)} %get-tuple-element.21), channel_id=1, source_target_pairs={{0,2},{1,3},{2,0},{3,1},{4,6},{5,7},{6,4},{7,5},{8,10},{9,11},{10,... | collective-permute-start | bytes 196616 | tf_op jit(solution)/shard_map/ppermute | solution.py:456
  290.7 4.9 %copy-start.15 = (s32[2,128]{1,0:T(2,128)S(1)}, s32[2,128]{1,0:T(2,128)}, u32[]{:S(2)}) copy-start(s32[2,128]{1,0:T(2,128)} %get-tuple-element.14.places) | copy-start | bytes 3076
  295.6 1.0 copy-start.6
